TPU v7x, 512 devices: a whole 4x8x8 slice. The times are simulated.
512 devices in a mesh: sp: 64 (over z, y), tp: 8 (over x, core).
Axes of the slice: x: 4, y: 8, z: 8, core: 2. Of those that a mesh axis runs over, the one named last changes fastest.
Arguments:
- layer_source_tokens: bfloat16 [2, 4096, 4096], P(None, 'sp'), may hold values from -6 to 6
- address_projection: bfloat16 [4096, 2048], P('sp', 'tp'), may hold values from -0.09375 to 0.09375
- content_projection: bfloat16 [4096, 2048], P('sp', 'tp'), may hold values from -0.09375 to 0.09375
- strength_projection: bfloat16 [4096, 16], replicated, may hold values from -0.09375 to 0.09375
- fading_driver_projection: bfloat16 [4096, 16], replicated, may hold values from -0.25 to 0.25
- strength_offset: float32 [16], P('tp'), may hold values from -2.5 to 1
- channel_fading_speed: float32 [16], P('tp')
- added_fading_exponent: float32 [2, 4096, 16], P(None, 'sp', 'tp'), may hold values from -0.7 to 0, as said below
- first_step_probe: bfloat16 [2, 2048], P(None, 'tp'), may hold values from -6 to 6
- first_step_address: bfloat16 [2, 2048], P(None, 'tp'), may hold values from -6 to 6
- first_step_content: bfloat16 [2, 2048], P(None, 'tp'), may hold values from -6 to 6
- first_step_outgate: bfloat16 [2, 2048], P(None, 'tp'), may hold values from -6 to 6
- first_step_strength_raw: float32 [2, 16], P(None, 'tp'), may hold values from -6 to 6
- channel_scaling_factor: float32 [128], replicated, may hold values from 0.1 to 1.9
- readout_projection: bfloat16 [2048, 4096], P('tp', 'sp'), may hold values from -0.125 to 0.125
Outputs:
- state_cache: bfloat16 [2, 16, 128, 128], P(None, 'tp')
- mixed_read: bfloat16 [2, 4096], P(None, 'sp')
- boundary_cache: bfloat16 [2, 64, 16, 128, 128], P(None, 'sp', 'tp')
Inputs may be any that keep to these rules, and one draw needn't show every extreme that they name: `added_fading_exponent`: zero at most positions.
All inputs are finite; a program needn't handle non-finite values.
Results may differ from a plain program's by a relative error of at most 0.017.
Values may be sent and summed in bfloat16 or wider, within the bound.
No kernel may reach another device: no remote copies, remote signals or barrier semaphores. Data moves between devices by JAX's collectives and lax.ppermute only.
A program may use at most 64 MiB of HBM per device.

v0:
```python
import jax
import jax.numpy as jnp
from jax import lax
from jax.sharding import Mesh
from jax.sharding import PartitionSpec as P

ADDRESS_WIDTH = 128
BLOCK = 64
SP = ("sp_0", "sp_1")


EPSILON = 1e-06
HIGHEST_ACCURACY = lax.Precision.HIGHEST


def in_one_piece(arrays, axis, dim, along):
    ends, at = ([], 0)
    for a in arrays[:-1]:
        at += a.shape[along]
        ends.append(at)
    both = jnp.concatenate(arrays, axis=along)
    return tuple(jnp.split(lax.all_gather(both, axis, axis=dim, tiled=True), ends, axis=along))


def nothing_yet(array, identity):
    return jax.tree.map(
        lambda part, zero: jnp.zeros_like(part) + jnp.asarray(zero, part.dtype), array, identity
    )


def prefix_by_axis(array, axes, combine, identity):
    before = start = nothing_yet(array, identity)
    so_far = array
    for axis in reversed(axes):
        peers, index = (lax.axis_size(axis), lax.axis_index(axis))
        pieces = jax.tree.map(
            lambda part, kind: lax.all_gather(part.astype(kind), axis),
            so_far,
            (jnp.bfloat16, jnp.bfloat16),
        )
        inside, so_far = (start, start)
        for k in range(peers):
            passed = k < index
            so_far = combine(
                so_far, jax.tree.map(lambda part, own: part[k].astype(own.dtype), pieces, array)
            )
            inside = jax.tree.map(lambda new, old: jnp.where(passed, new, old), so_far, inside)
        before = combine(inside, before)
    return before


def as_sent(array):
    return jax.tree.map(lambda a: a.astype(jnp.bfloat16) if a.dtype == jnp.float32 else a, array)


def picked(array, axis, root):
    return lax.dynamic_index_in_dim(lax.all_gather(array, axis), root, 0, keepdims=False)


def from_everyone(array, axis):
    copies = jnp.broadcast_to(array, (lax.axis_size(axis), *array.shape))
    return lax.all_to_all(copies, axis, split_axis=0, concat_axis=0, tiled=True)


def taken_together(array, axis):
    return from_everyone(array, axis).astype(jnp.float32).sum(axis=0)


def unit_inverse(lower_part):
    matrix_order = lower_part.shape[-1]
    identity = jnp.eye(matrix_order, dtype=jnp.float32)
    result = identity - lower_part
    power_term = lower_part
    reached = 2
    while reached < matrix_order:
        power_term = jnp.matmul(power_term, power_term, precision=HIGHEST_ACCURACY)
        result = jnp.matmul(result, identity + power_term, precision=HIGHEST_ACCURACY)
        reached = reached * 2
    return result


def build_arguments(
    address_vectors,
    content_vectors,
    outgate_raw_scores,
    strength_offset,
    channel_fading_speed,
    added_fading_exponent,
    channel_width,
):
    length = address_vectors.shape[0]
    attention_channels_total = channel_fading_speed.shape[0]
    address_token_slab = jax.nn.silu(address_vectors.astype(jnp.float32)).reshape(
        length, attention_channels_total, channel_width
    )
    address_token_slab = address_token_slab * lax.rsqrt(
        jnp.sum(address_token_slab * address_token_slab, axis=-1, keepdims=True) + EPSILON
    )
    content_token_slab = jax.nn.silu(content_vectors.astype(jnp.float32)).reshape(
        length, attention_channels_total, channel_width
    )
    strength_raw_expanded = outgate_raw_scores.astype(jnp.float32)
    storing_strength = jax.nn.sigmoid(
        strength_raw_expanded[:, :attention_channels_total] + strength_offset
    )
    fading_exponent = added_fading_exponent - channel_fading_speed * jax.nn.softplus(
        strength_raw_expanded[:, attention_channels_total:]
    )
    return (address_token_slab, content_token_slab, storing_strength, fading_exponent)


def range_map(address_token_slab, content_token_slab, storing_strength, fading_exponent, block):
    length, attention_channels_total, channel_width = address_token_slab.shape
    blocks = length // block

    def split_blocks(tensor):
        moved_axes = jnp.swapaxes(tensor, 0, 1)
        return moved_axes.reshape((attention_channels_total, blocks, block) + moved_axes.shape[2:])

    block_keys = split_blocks(address_token_slab)
    block_values = split_blocks(content_token_slab)
    block_beta = split_blocks(storing_strength)
    cumulative = jnp.cumsum(split_blocks(fading_exponent), axis=-1)
    positions = jnp.arange(block)
    strict = positions[:, None] > positions[None, :]
    spread_log = jnp.where(strict, cumulative[..., :, None] - cumulative[..., None, :], 0.0)
    scaled_keys = block_keys * block_beta[..., None]
    inner_prod = jnp.einsum("hnik,hnjk->hnij", scaled_keys, block_keys, precision=HIGHEST_ACCURACY)
    lower_part = jnp.where(strict, inner_prod * jnp.exp(spread_log), 0.0)
    inverse = unit_inverse(lower_part)
    targets = jnp.concatenate(
        [block_values * block_beta[..., None], scaled_keys * jnp.exp(cumulative)[..., None]],
        axis=-1,
    )
    solved = jnp.einsum("hnij,hnjk->hnik", inverse, targets, precision=HIGHEST_ACCURACY)
    updates = solved[..., :channel_width]
    key_weights = solved[..., channel_width:]
    tail_keys = block_keys * jnp.exp(cumulative[..., -1:] - cumulative)[..., None]
    last_decay = jnp.exp(cumulative[..., -1])
    identity = jnp.eye(channel_width, dtype=jnp.float32)

    def advance(state_pair, block_items):
        transition, carried_state = state_pair
        update_index, weight_index, tail_index, last_index = block_items
        fresh_value_rows = update_index - jnp.einsum(
            "xbg,xgp->xbp", weight_index, carried_state, precision=HIGHEST_ACCURACY
        )
        carried_state = carried_state * last_index[:, None, None] + jnp.einsum(
            "tjo,tjw->tow", tail_index, fresh_value_rows, precision=HIGHEST_ACCURACY
        )
        block_move = last_index[:, None, None] * identity - jnp.einsum(
            "hck,hcj->hkj", tail_index, weight_index, precision=HIGHEST_ACCURACY
        )
        transition = jnp.einsum("hij,hjk->hik", block_move, transition, precision=HIGHEST_ACCURACY)
        return ((transition, carried_state), None)

    initial = (
        jnp.broadcast_to(identity, (attention_channels_total, channel_width, channel_width)),
        jnp.zeros((attention_channels_total, channel_width, channel_width), jnp.float32),
    )
    block_items = (
        jnp.moveaxis(updates, 1, 0),
        jnp.moveaxis(key_weights, 1, 0),
        jnp.moveaxis(tail_keys, 1, 0),
        jnp.moveaxis(last_decay, 1, 0),
    )
    (transition, carried_state), _ = lax.scan(advance, initial, block_items)
    return (transition, carried_state)


def read_heads(
    state_cache,
    first_step_probe,
    first_step_address,
    first_step_content,
    first_step_outgate,
    first_step_strength_raw,
    channel_scaling_factor,
):
    seq_count, attention_channels_total, channel_width, _ = state_cache.shape
    carried_state = state_cache.astype(jnp.float32)

    def activate(tensor):
        return jax.nn.silu(tensor.astype(jnp.float32)).reshape(
            seq_count, attention_channels_total, channel_width
        )

    query_rows = activate(first_step_probe)
    address_token_slab = activate(first_step_address)
    address_token_slab = address_token_slab * lax.rsqrt(
        jnp.sum(address_token_slab * address_token_slab, axis=-1, keepdims=True) + EPSILON
    )
    content_token_slab = activate(first_step_content)
    storing_strength = jax.nn.sigmoid(first_step_strength_raw)
    recalled = jnp.einsum(
        "nhk,nhkv->nhv", address_token_slab, carried_state, precision=HIGHEST_ACCURACY
    )
    updated = (
        carried_state
        + storing_strength[..., None, None]
        * address_token_slab[..., :, None]
        * (content_token_slab - recalled)[..., None, :]
    )
    output = jnp.einsum("nhk,nhkv->nhv", query_rows, updated, precision=HIGHEST_ACCURACY)
    normed = (
        output
        * lax.rsqrt(jnp.mean(output * output, axis=-1, keepdims=True) + EPSILON)
        * channel_scaling_factor
    )
    gated_out = normed * activate(first_step_outgate)
    return gated_out.reshape(seq_count, attention_channels_total * channel_width).astype(
        jnp.bfloat16
    )


def matmul_maps(left, right):
    return jnp.einsum("shij,shjk->shik", left, right, precision=HIGHEST_ACCURACY)


def join_pairs(earlier, later):
    return (matmul_maps(later[0], earlier[0]), matmul_maps(later[0], earlier[1]) + later[1])


def per_device(
    layer_source_tokens,
    address_projection,
    content_projection,
    strength_projection,
    fading_driver_projection,
    strength_offset,
    channel_fading_speed,
    added_fading_exponent,
    first_step_probe,
    first_step_address,
    first_step_content,
    first_step_outgate,
    first_step_strength_raw,
    channel_scaling_factor,
    readout_projection,
):
    head_local = channel_fading_speed.shape[0]
    first_head = lax.axis_index("tp") * head_local
    beta_slice = lax.dynamic_slice_in_dim(strength_projection, first_head, head_local, 1)
    alpha_slice = lax.dynamic_slice_in_dim(fading_driver_projection, first_head, head_local, 1)
    seq_count, local_len, model_width = layer_source_tokens.shape
    flat_rows = layer_source_tokens.reshape(seq_count * local_len, model_width)
    pieces = in_one_piece((address_projection, content_projection), SP, 0, 1)
    key_sum = jnp.dot(flat_rows, pieces[0], preferred_element_type=jnp.float32)
    value_sum = jnp.dot(flat_rows, pieces[1], preferred_element_type=jnp.float32)
    beta_sum = jnp.dot(flat_rows, beta_slice, preferred_element_type=jnp.float32)
    alpha_sum = jnp.dot(flat_rows, alpha_slice, preferred_element_type=jnp.float32)
    outgate_raw_scores = (
        jnp.concatenate([beta_sum, alpha_sum], axis=1)
        .astype(jnp.bfloat16)
        .reshape(seq_count, local_len, -1)
    )
    address_vectors = key_sum.astype(jnp.bfloat16).reshape(seq_count, local_len, -1)
    content_vectors = value_sum.astype(jnp.bfloat16).reshape(seq_count, local_len, -1)
    transitions = []
    offsets = []
    for prompt_number in range(seq_count):
        address_token_slab, content_token_slab, storing_strength, fading_exponent = build_arguments(
            address_vectors[prompt_number],
            content_vectors[prompt_number],
            outgate_raw_scores[prompt_number],
            strength_offset,
            channel_fading_speed,
            added_fading_exponent[prompt_number],
            ADDRESS_WIDTH,
        )
        transition, carried_state = range_map(
            address_token_slab, content_token_slab, storing_strength, fading_exponent, BLOCK
        )
        transitions.append(transition)
        offsets.append(carried_state)
    transition = jnp.stack(transitions)
    offset = jnp.stack(offsets)
    identity = jnp.broadcast_to(jnp.eye(ADDRESS_WIDTH, dtype=jnp.float32), transition.shape)
    entered = prefix_by_axis(
        (transition, offset), SP, join_pairs, (identity, jnp.zeros_like(offset))
    )
    leaving = matmul_maps(transition, entered[1]) + offset
    final = picked(as_sent(leaving), SP, lax.axis_size(SP) - 1).astype(leaving.dtype)
    boundary_cache = leaving.astype(jnp.bfloat16)[:, None]
    state_cache = final.astype(jnp.bfloat16)
    heads_read = read_heads(
        state_cache,
        first_step_probe,
        first_step_address,
        first_step_content,
        first_step_outgate,
        first_step_strength_raw,
        channel_scaling_factor,
    )
    group_terms = jnp.dot(
        heads_read, readout_projection, preferred_element_type=jnp.float32
    ).astype(jnp.bfloat16)
    mixed_read = (
        taken_together(group_terms.astype(jnp.float32).astype(jnp.bfloat16), "tp")
        .astype(jnp.float32)
        .astype(jnp.bfloat16)
    )
    return (state_cache, mixed_read, boundary_cache)


def solution(mesh):
    finer = Mesh(mesh.devices.reshape(8, 8, mesh.shape["tp"]), ("sp_0", "sp_1", "tp"))
    return jax.shard_map(
        per_device,
        mesh=finer,
        in_specs=(
            P(None, SP, None),
            P(SP, "tp"),
            P(SP, "tp"),
            P(),
            P(),
            P("tp"),
            P("tp"),
            P(None, SP, "tp"),
            P(None, "tp"),
            P(None, "tp"),
            P(None, "tp"),
            P(None, "tp"),
            P(None, "tp"),
            P(),
            P("tp", SP),
        ),
        out_specs=(P(None, "tp", None, None), P(None, SP), P(None, SP, "tp", None, None)),
        check_vma=False,
    )
```

profile of v0, /device:TPU:1, one launch (start us, length us, event | category | flops | bytes accessed | tf_op | source)
XLA Modules:
  0.0 409.0 jit_solution(2410808542872508235)
XLA Ops:
  7.2 1.5 pad_maximum_fusion.2
  8.8 1.2 fusion.21
  10.0 1.2 fusion.20
  13.6 86.2 %all-gather.10.cloned.1.call-done = bf16[4096,512]{1,0:T(8,128)(2,1)} async-done(((bf16[64,512]{1,0:T(8,128)(2,1)}), bf16[4096,512]{1,0:T(8,128)(2,1)}) %all-gather.10.cloned.1.call-update) | async-done | bytes 4194320 | tf_op jit(solution)/shard_map/all_gather | solution.py:22
  99.8 2.2 fusion.15
  114.1 33.6 %all-gather.12.cloned.1.call-done = bf16[8,2,2,128,128]{4,3,2,1,0:T(8,128)(2,1)} async-done(((bf16[1,2,2,128,128]{4,3,2,1,0:T(8,128)(2,1)}), bf16[8,2,2,128,128]{4,3,2,1,0:T(8,128)(2,1)}) %all-gather.12.cloned.1.call-update) | async-done | bytes 1048592 | tf_op jit(solution)/shard_map/all_gather | solution.py:37
  147.7 1.3 fusion.57
  148.9 1.2 fusion.81
  150.1 1.2 fusion.80
  151.3 1.2 fusion.79
  152.5 1.2 fusion.78
  154.4 1.2 fusion.77
  156.3 1.2 fusion.76
  158.6 31.5 %all-gather.14.cloned.1.call-done = bf16[8,2,2,128,128]{4,3,2,1,0:T(8,128)(2,1)} async-done(((bf16[1,2,2,128,128]{4,3,2,1,0:T(8,128)(2,1)}), bf16[8,2,2,128,128]{4,3,2,1,0:T(8,128)(2,1)}) %all-gather.14.cloned.1.call-update) | async-done | bytes 1048592 | tf_op jit(solution)/shard_map/all_gather | solution.py:37
  193.1 1.3 convolution_add_fusion.15
  194.4 1.3 convolution_add_fusion.14
  195.7 1.3 convolution_add_fusion.13
  197.0 1.3 convolution_add_fusion.12
  198.3 1.3 convolution_add_fusion.11
  199.6 2.0 fusion.186
  202.4 31.3 %all-gather.16.cloned.1.call-done = bf16[16,2,128,128]{3,2,1,0:T(8,128)(2,1)} async-done(((bf16[2,2,128,128]{3,2,1,0:T(8,128)(2,1)}), bf16[16,2,128,128]{3,2,1,0:T(8,128)(2,1)}) %all-gather.16.cloned.1.call-update) | async-done | bytes 1048592 | tf_op jit(solution)/shard_map/all_gather | solution.py:37
  233.7 42.5 %all-gather.18.cloned.1.call-done = bf16[16,2,128,128]{3,2,1,0:T(8,128)(2,1)} async-done(((bf16[2,2,128,128]{3,2,1,0:T(8,128)(2,1)}), bf16[16,2,128,128]{3,2,1,0:T(8,128)(2,1)}) %all-gather.18.cloned.1.call-update) | async-done | bytes 1048592 | tf_op jit(solution)/shard_map/all_gather | solution.py:37
  276.2 1.2 convolution_add_fusion.7
  277.4 1.2 convolution_add_fusion.6
  278.7 1.4 convolution_add_fusion.5
  280.1 1.2 convolution_add_fusion.4
  281.4 1.2 convolution_add_fusion.3
  282.7 1.2 convolution_add_fusion.2
  284.0 1.2 convolution_add_fusion.1
  285.2 1.2 fusion.4
  288.8 101.3 %all-gather.20.cloned.1.call-done = bf16[128,2,128,128]{3,2,1,0:T(8,128)(2,1)} async-done(((bf16[2,2,128,128]{3,2,1,0:T(8,128)(2,1)}), bf16[128,2,128,128]{3,2,1,0:T(8,128)(2,1)}) %all-gather.20.cloned.1.call-update) | async-done | bytes 8388624 | tf_op jit(solution)/shard_map/all_gather | solution.py:57
  392.1 9.6 %all_to_all.5 = bf16[8,2,64]{2,1,0:T(2,128)(2,1)S(1)} all-to-all(bf16[8,2,64]{2,1,0:T(2,128)(2,1)S(1)} %broadcast_in_dim.45), channel_id=1, replica_groups=mesh['sp_0'=8,'sp_1'=8,'tp'=8] {'tp'}, dimensions={0} | all-to-all | bytes 4096 | tf_op jit(solution)/shard_map/all_to_all | solution.py:62
  (174 shorter events, 25.0 us)
Async XLA Ops:
  7.2 92.6 %all-gather.10.cloned.1.call-start = ((), (), s32[]{:S(2)}) async-start(), calls=%async_computation.1 | async-start | bytes 4259840 | tf_op jit(solution)/shard_map/all_gather | solution.py:22
  8.7 138.9 %all-gather.12.cloned.1.call-start = ((), (), s32[]{:S(2)}) async-start(), calls=%async_computation.2 | async-start | bytes 1179648 | tf_op jit(solution)/shard_map/all_gather | solution.py:37
  99.8 5.5 %copy-start.35 = (bf16[4096,512]{1,0:T(8,128)(2,1)S(1)}, bf16[4096,512]{1,0:T(8,128)(2,1)}, u32[]{:S(2)}) copy-start(bf16[4096,512]{1,0:T(8,128)(2,1)} %all-gather.10.cloned.1.call-done) | copy-start | bytes 12582916
  111.1 79.0 %all-gather.14.cloned.1.call-start = ((), (), s32[]{:S(2)}) async-start(), calls=%async_computation.3 | async-start | bytes 1179648 | tf_op jit(solution)/shard_map/all_gather | solution.py:37
  114.0 119.7 %all-gather.16.cloned.1.call-start = ((), (), s32[]{:S(2)}) async-start(), calls=%async_computation.4 | async-start | bytes 1179648 | tf_op jit(solution)/shard_map/all_gather | solution.py:37
  147.7 9.8 %copy-start.2 = (bf16[8,2,2,128,128]{4,3,2,1,0:T(8,128)(2,1)S(1)}, bf16[8,2,2,128,128]{4,3,2,1,0:T(8,128)(2,1)}, u32[]{:S(2)}) copy-start(bf16[8,2,2,128,128]{4,3,2,1,0:T(8,128)(2,1)} %all-gather.12.cloned.1.call-done) | copy-start | bytes 3145732
  158.5 117.7 %all-gather.18.cloned.1.call-start = ((), (), s32[]{:S(2)}) async-start(), calls=%async_computation.5 | async-start | bytes 1179648 | tf_op jit(solution)/shard_map/all_gather | solution.py:37
  193.1 8.5 %copy-start.5 = (f32[2,2,128,128]{3,2,1,0:T(8,128)}, f32[2,2,128,128]{3,2,1,0:T(8,128)S(1)}, u32[]{:S(2)}) copy-start(f32[2,2,128,128]{3,2,1,0:T(8,128)S(1)} %convolution_add_fusion.16) | copy-start | bytes 786436
  194.4 7.2 %copy-start.7 = (f32[2,2,128,128]{3,2,1,0:T(8,128)}, f32[2,2,128,128]{3,2,1,0:T(8,128)S(1)}, u32[]{:S(2)}) copy-start(f32[2,2,128,128]{3,2,1,0:T(8,128)S(1)} %convolution_add_fusion.15) | copy-start | bytes 786436
  195.7 5.9 %copy-start.9 = (f32[2,2,128,128]{3,2,1,0:T(8,128)}, f32[2,2,128,128]{3,2,1,0:T(8,128)S(1)}, u32[]{:S(2)}) copy-start(f32[2,2,128,128]{3,2,1,0:T(8,128)S(1)} %convolution_add_fusion.14) | copy-start | bytes 786436
  197.0 4.6 %copy-start.11 = (f32[2,2,128,128]{3,2,1,0:T(8,128)}, f32[2,2,128,128]{3,2,1,0:T(8,128)S(1)}, u32[]{:S(2)}) copy-start(f32[2,2,128,128]{3,2,1,0:T(8,128)S(1)} %convolution_add_fusion.13) | copy-start | bytes 786436
  201.7 188.5 %all-gather.20.cloned.1.call-start = ((), (), s32[]{:S(2)}) async-start(), calls=%async_computation.6 | async-start | bytes 8519680 | tf_op jit(solution)/shard_map/all_gather | solution.py:57
  233.7 48.9 %copy-start.1 = (bf16[16,2,128,128]{3,2,1,0:T(8,128)(2,1)S(1)}, bf16[16,2,128,128]{3,2,1,0:T(8,128)(2,1)}, u32[]{:S(2)}) copy-start(bf16[16,2,128,128]{3,2,1,0:T(8,128)(2,1)} %all-gather.16.cloned.1.call-done) | copy-start | bytes 3145732
  278.6 8.2 %copy-start.6 = (f32[2,2,128,128]{3,2,1,0:T(8,128)S(1)}, f32[2,2,128,128]{3,2,1,0:T(8,128)}, u32[]{:S(2)}) copy-start(f32[2,2,128,128]{3,2,1,0:T(8,128)} %copy-done.5) | copy-start | bytes 786436
  278.7 8.2 %copy-start.8 = (f32[2,2,128,128]{3,2,1,0:T(8,128)S(1)}, f32[2,2,128,128]{3,2,1,0:T(8,128)}, u32[]{:S(2)}) copy-start(f32[2,2,128,128]{3,2,1,0:T(8,128)} %copy-done.7) | copy-start | bytes 786436
  278.7 8.2 %copy-start.10 = (f32[2,2,128,128]{3,2,1,0:T(8,128)S(1)}, f32[2,2,128,128]{3,2,1,0:T(8,128)}, u32[]{:S(2)}) copy-start(f32[2,2,128,128]{3,2,1,0:T(8,128)} %copy-done.9) | copy-start | bytes 786436
  278.7 8.2 %copy-start.12 = (f32[2,2,128,128]{3,2,1,0:T(8,128)S(1)}, f32[2,2,128,128]{3,2,1,0:T(8,128)}, u32[]{:S(2)}) copy-start(f32[2,2,128,128]{3,2,1,0:T(8,128)} %copy-done.11) | copy-start | bytes 786436
  278.7 8.2 %copy-start.14 = (f32[2,2,128,128]{3,2,1,0:T(8,128)S(1)}, f32[2,2,128,128]{3,2,1,0:T(8,128)}, u32[]{:S(2)}) copy-start(f32[2,2,128,128]{3,2,1,0:T(8,128)} %copy-done.13) | copy-start | bytes 786436
  278.7 8.2 %copy-start.16 = (f32[2,2,128,128]{3,2,1,0:T(8,128)S(1)}, f32[2,2,128,128]{3,2,1,0:T(8,128)}, u32[]{:S(2)}) copy-start(f32[2,2,128,128]{3,2,1,0:T(8,128)} %copy-done.15) | copy-start | bytes 786436
  278.7 8.2 %copy-start.18 = (f32[2,2,128,128]{3,2,1,0:T(8,128)S(1)}, f32[2,2,128,128]{3,2,1,0:T(8,128)}, u32[]{:S(2)}) copy-start(f32[2,2,128,128]{3,2,1,0:T(8,128)} %copy-done.17) | copy-start | bytes 786436
  278.7 8.2 %copy-start.23 = (f32[2,2,128,128]{3,2,1,0:T(8,128)S(1)}, f32[2,2,128,128]{3,2,1,0:T(8,128)}, u32[]{:S(2)}) copy-start(f32[2,2,128,128]{3,2,1,0:T(8,128)} %get-tuple-element.93) | copy-start | bytes 786436
  282.6 4.7 %copy-start.20 = (f32[2,128,128]{2,1,0:T(8,128)S(1)}, f32[2,128,128]{2,1,0:T(8,128)}, u32[]{:S(2)}) copy-start(f32[2,128,128]{2,1,0:T(8,128)} %copy-done.19) | copy-start | bytes 393220
  282.6 4.7 %copy-start.22 = (f32[2,128,128]{2,1,0:T(8,128)S(1)}, f32[2,128,128]{2,1,0:T(8,128)}, u32[]{:S(2)}) copy-start(f32[2,128,128]{2,1,0:T(8,128)} %copy-done.21) | copy-start | bytes 393220
  282.7 4.7 %copy-start.25 = (f32[2,128,128]{2,1,0:T(8,128)S(1)}, f32[2,128,128]{2,1,0:T(8,128)}, u32[]{:S(2)}) copy-start(f32[2,128,128]{2,1,0:T(8,128)} %copy-done.24) | copy-start | bytes 393220
  282.7 4.7 %copy-start.27 = (f32[2,128,128]{2,1,0:T(8,128)S(1)}, f32[2,128,128]{2,1,0:T(8,128)}, u32[]{:S(2)}) copy-start(f32[2,128,128]{2,1,0:T(8,128)} %copy-done.26) | copy-start | bytes 393220
  283.9 4.6 %copy-start.30 = (bf16[2,256]{1,0:T(2,128)(2,1)S(1)}, bf16[2,256]{1,0:T(2,128)(2,1)}, u32[]{:S(2)}) copy-start(bf16[2,256]{1,0:T(2,128)(2,1)} %param.23) | copy-start | bytes 3076
  283.9 4.6 %copy-start.31 = (bf16[2,256]{1,0:T(2,128)(2,1)S(1)}, bf16[2,256]{1,0:T(2,128)(2,1)}, u32[]{:S(2)}) copy-start(bf16[2,256]{1,0:T(2,128)(2,1)} %param.25) | copy-start | bytes 3076
  284.0 4.6 %copy-start.32 = (bf16[2,256]{1,0:T(2,128)(2,1)S(1)}, bf16[2,256]{1,0:T(2,128)(2,1)}, u32[]{:S(2)}) copy-start(bf16[2,256]{1,0:T(2,128)(2,1)} %param.24) | copy-start | bytes 3076
  284.0 4.8 %copy-start.33 = (f32[2,2]{1,0:T(2,128)S(1)}, f32[2,2]{1,0:T(2,128)}, u32[]{:S(2)}) copy-start(f32[2,2]{1,0:T(2,128)} %param.27) | copy-start | bytes 52
  284.0 107.8 %copy-start.34 = (f32[128]{0:T(128)S(1)}, f32[128]{0:T(128)}, u32[]{:S(2)}) copy-start(f32[128]{0:T(128)} %param.28) | copy-start | bytes 1540
  284.0 107.9 %copy-start.36 = (bf16[256,64]{0,1:T(8,128)(2,1)S(1)}, bf16[256,64]{0,1:T(8,128)(2,1)}, u32[]{:S(2)}) copy-start(bf16[256,64]{0,1:T(8,128)(2,1)} %param.29) | copy-start | bytes 98308
  391.1 11.1 %copy-start.28 = (bf16[2,2,128,128]{3,2,1,0:T(8,128)(2,1)}, bf16[2,2,128,128]{3,2,1,0:T(8,128)(2,1)S(1)}, u32[]{:S(2)}) copy-start(bf16[2,2,128,128]{3,2,1,0:T(8,128)(2,1)S(1)} %slice.260) | copy-start | bytes 393220
  (11 other events, 16.9 us)
Sparse Core Ops, SparseCore 0:
  11.6 88.1 all-gather.9
  111.2 36.4 all-gather.11
  150.3 39.7 all-gather.13
  192.6 41.0 all-gather.15
  236.2 39.9 all-gather.17
  288.6 101.5 all-gather.19
where the time goes:
time: 410 us; the launch traced here: 409 us
  waiting for transfers between devices  326 us (80%)
  matrix products  46.1 us (11%)
  between operations  15.2 us (4%)
  blocking collectives  9.58 us (2%)
  other arithmetic  6.23 us (2%)
  local copies, waits for them, and re-layouts  5 us (1%)
    all_gather x4, waiting for transfers between devices, prefix_by_axis(): lax.all_gather(part.astype(kind), axis)  139 us
    all_gather x1, waiting for transfers between devices, picked(): lax.all_gather(array, axis)  101 us
    all_gather x1, waiting for transfers between devices, in_one_piece(): lax.all_gather(both, axis, axis=dim, tiled=True)  86.2 us
    dot_general x28, matrix products, matmul_maps(): jnp.einsum('shij,shjk->shik', left, right, precision=HIGHEST_ACCURACY)  32.4 us
    all_to_all x1, blocking collectives, from_everyone(): return lax.all_to_all(copies, axis, split_axis=0, concat_axis=0, tiled=True)  9.58 us
  transfers between devices with their start and end apart: 6, of which 6 were waited for; matrix products, arithmetic and copies ran while one was open for 7% of the time, Pallas kernels for 0%

commit v1 on v0

v1 whole, which is shorter than its diff:
```python
import jax
import jax.numpy as jnp
from jax import lax
from jax.sharding import Mesh
from jax.sharding import PartitionSpec as P

WIDTH = 128
SIDE = 8
EPSILON = 1e-06
BEST = lax.Precision.HIGHEST
SP = ("z", "y")


def exchange(messages, axis):
    return lax.all_to_all(messages, axis, split_axis=0, concat_axis=0, tiled=True)


def from_everyone(array, axis):
    return exchange(jnp.broadcast_to(array, (lax.axis_size(axis), *array.shape)), axis)


def unit_inverse(lower_part):
    order = lower_part.shape[-1]
    identity = jnp.eye(order, dtype=jnp.float32)
    result = identity - lower_part
    power = lower_part
    reached = 2
    while reached < order:
        power = jnp.matmul(power, power, precision=BEST)
        result = jnp.matmul(result, identity + power, precision=BEST)
        reached *= 2
    return result


def two_parts(values):
    high = lax.reduce_precision(values, 8, 7)
    return high.astype(jnp.bfloat16), (values - high).astype(jnp.bfloat16)


def range_maps(keys, values, beta, fading):
    block = keys.shape[1]
    cumulative = jnp.cumsum(fading, axis=-1)
    at = jnp.arange(block)
    strict = at[:, None] > at[None, :]
    spread = jnp.where(strict, cumulative[:, :, None] - cumulative[:, None, :], 0.0)
    scaled = keys * beta[..., None]
    inner = jnp.einsum("nik,njk->nij", scaled, keys, precision=BEST)
    inverse = unit_inverse(jnp.where(strict, inner * jnp.exp(spread), 0.0))
    targets = jnp.concatenate(
        [scaled * jnp.exp(cumulative)[..., None], values * beta[..., None]], axis=-1
    )
    solved = jnp.einsum("nij,njk->nik", inverse, targets, precision=BEST)
    last = cumulative[:, -1:]
    tail = keys * jnp.exp(last - cumulative)[..., None]
    moved = jnp.einsum("njk,njw->nkw", tail, solved, precision=BEST)
    identity = jnp.eye(WIDTH, dtype=jnp.float32)
    transition = jnp.exp(last)[..., None] * identity - moved[..., :WIDTH]
    return jnp.concatenate([transition, moved[..., WIDTH:]], axis=-1)


def then(earlier, later):
    both = jnp.matmul(later[..., :WIDTH], earlier, precision=BEST)
    return jnp.concatenate([both[..., :WIDTH], both[..., WIDTH:] + later[..., WIDTH:]], axis=-1)


def applied(maps, state):
    return jnp.matmul(maps[..., :WIDTH], state, precision=BEST) + maps[..., WIDTH:]


def read_heads(state_cache, probe, address, content, outgate, strength_raw, gain):
    prompts, heads, width, _ = state_cache.shape
    state = state_cache.astype(jnp.float32)

    def activate(tensor):
        return jax.nn.silu(tensor.astype(jnp.float32)).reshape(prompts, heads, width)

    query = activate(probe)
    key = activate(address)
    key = key * lax.rsqrt(jnp.sum(key * key, axis=-1, keepdims=True) + EPSILON)
    value = activate(content)
    strength = jax.nn.sigmoid(strength_raw)
    recalled = jnp.einsum("nhk,nhkv->nhv", key, state, precision=BEST)
    updated = state + strength[..., None, None] * key[..., :, None] * (value - recalled)[..., None, :]
    output = jnp.einsum("nhk,nhkv->nhv", query, updated, precision=BEST)
    normed = output * lax.rsqrt(jnp.mean(output * output, axis=-1, keepdims=True) + EPSILON) * gain
    return (normed * activate(outgate)).reshape(prompts, heads * width).astype(jnp.bfloat16)


def per_device(
    tokens,
    address_projection,
    content_projection,
    strength_projection,
    fading_driver_projection,
    strength_offset,
    fading_speed,
    added_fading,
    probe,
    address,
    content,
    outgate,
    strength_raw,
    gain,
    readout_projection,
):
    prompts, positions, model = tokens.shape
    heads = fading_speed.shape[0]
    rows = prompts * positions
    share = model // (SIDE * SIDE)
    z, y, tp = lax.axis_index("z"), lax.axis_index("y"), lax.axis_index("tp")
    half = SIDE // 2
    my_half = y % 2

    weights = jnp.concatenate(
        [
            part[:, head * WIDTH : (head + 1) * WIDTH]
            for head in range(heads)
            for part in (address_projection, content_projection)
        ],
        axis=1,
    )
    flat = tokens.reshape(rows, model)
    columns = flat.reshape(rows, SIDE, SIDE, share).transpose(2, 0, 1, 3).reshape(SIDE, rows, -1)
    line_tokens = exchange(columns, "y")
    line_weights = from_everyone(weights, "z").reshape(SIDE * share, -1)

    drivers = jnp.concatenate([strength_projection, fading_driver_projection], axis=1)
    logits = jnp.dot(flat, drivers, preferred_element_type=jnp.float32).astype(jnp.bfloat16)
    logits = logits.astype(jnp.float32).reshape(prompts, positions, 2, -1)
    mine = lax.dynamic_slice_in_dim(logits, tp * heads, heads, 3)
    beta = jax.nn.sigmoid(mine[:, :, 0] + strength_offset)
    fading = added_fading - fading_speed * jax.nn.softplus(mine[:, :, 1])
    gates = jnp.stack([*two_parts(beta), *two_parts(fading)])
    gates = gates.transpose(1, 3, 0, 2).reshape(prompts, heads, 1, 1, 4 * positions)

    partial = jnp.dot(
        line_tokens.reshape(SIDE * rows, -1), line_weights, preferred_element_type=jnp.float32
    ).astype(jnp.bfloat16)
    partial = partial.reshape(2, half, prompts, positions, heads, 2 * WIDTH)
    partial = partial.transpose(2, 4, 0, 1, 3, 5).reshape(
        prompts, heads, 2, half * positions, 2 * WIDTH
    )
    gates = jnp.broadcast_to(gates, (prompts, heads, 2, 16, 4 * positions))
    sent = jnp.concatenate([partial, gates], axis=3).reshape(SIDE, half * positions + 16, -1)
    got = exchange(sent, "y")

    sums = got[:, : half * positions].astype(jnp.float32).sum(axis=0)
    sums = sums.reshape(half, positions, 2 * WIDTH)
    gates = lax.dynamic_slice_in_dim(got[:, half * positions], my_half * half, half, 0)
    gates = gates.astype(jnp.float32).reshape(half, 4, positions)
    beta = gates[:, 0] + gates[:, 1]
    fading = gates[:, 2] + gates[:, 3]
    keys = jax.nn.silu(sums[..., :WIDTH])
    keys = keys * lax.rsqrt(jnp.sum(keys * keys, axis=-1, keepdims=True) + EPSILON)
    values = jax.nn.silu(sums[..., WIDTH:])
    maps = range_maps(keys, values, beta, fading)
    inside = [maps[0]]
    for j in range(1, half):
        inside.append(then(inside[-1], maps[j]))

    whole = inside[-1].astype(jnp.bfloat16)
    other = lax.ppermute(whole, "y", [(i, i ^ 1) for i in range(SIDE)])
    first = jnp.where(my_half == 0, whole, other).astype(jnp.float32)
    second = jnp.where(my_half == 0, other, whole).astype(jnp.float32)
    line = then(first, second).astype(jnp.bfloat16)
    lines = from_everyone(line, "z").astype(jnp.float32)
    state = jnp.zeros((WIDTH, WIDTH), jnp.float32)
    entering = state
    for k in range(SIDE):
        entering = jnp.where(z == k, state, entering)
        state = applied(lines[k], state) if k else lines[0][:, WIDTH:]
    entering = jnp.where(my_half == 0, entering, applied(first, entering))
    leaving = applied(jnp.stack(inside), entering).astype(jnp.bfloat16)

    final_half = lax.dynamic_slice_in_dim(
        state.astype(jnp.bfloat16), my_half * (WIDTH // 2), WIDTH // 2, 0
    )
    home = jnp.concatenate(
        [
            jnp.concatenate([leaving, leaving], axis=0),
            jnp.broadcast_to(final_half, (SIDE, *final_half.shape)),
        ],
        axis=1,
    )
    back = exchange(home, "y").reshape(prompts, heads, 2, WIDTH + WIDTH // 2, WIDTH)
    boundary = lax.dynamic_index_in_dim(back, y // half, 2, keepdims=False)[:, :, :WIDTH]
    state_cache = back[:, :, :, WIDTH:].reshape(prompts, heads, WIDTH, WIDTH)

    heads_read = read_heads(state_cache, probe, address, content, outgate, strength_raw, gain)
    terms = jnp.dot(heads_read, readout_projection, preferred_element_type=jnp.float32)
    mixed = from_everyone(terms.astype(jnp.bfloat16), "tp").astype(jnp.float32).sum(axis=0)
    return state_cache, mixed.astype(jnp.bfloat16), boundary[:, None]


def solution(mesh):
    finer = Mesh(mesh.devices.reshape(SIDE, SIDE, mesh.shape["tp"]), (*SP, "tp"))
    return jax.shard_map(
        per_device,
        mesh=finer,
        in_specs=(
            P(None, SP, None),
            P(SP, "tp"),
            P(SP, "tp"),
            P(),
            P(),
            P("tp"),
            P("tp"),
            P(None, SP, "tp"),
            P(None, "tp"),
            P(None, "tp"),
            P(None, "tp"),
            P(None, "tp"),
            P(None, "tp"),
            P(),
            P("tp", SP),
        ),
        out_specs=(P(None, "tp", None, None), P(None, SP), P(None, SP, "tp", None, None)),
        check_vma=False,
    )
```

time: 410 us -> 176 us (0.43)
  waiting for transfers between devices: 326 us -> 109 us
  starting transfers between devices: 0.43 us -> 39.7 us
  matrix products: 46.1 us -> 8.78 us
  between operations: 15.2 us -> 1.48 us
  blocking collectives: 9.58 us -> 0 us
  local copies, waits for them, and re-layouts: 5 us -> 11.5 us
    all_gather x6 -> x0, waiting for transfers between devices: 326 us -> none  [the longest x4 139 us: prefix_by_axis(): lax.all_gather(part.astype(kind), axis)]
    all_to_all x0 -> x6, waiting for transfers between devices: none -> 106 us  [exchange(): lax.all_to_all(messages, axis, split_axis=0, concat_axis=0, tiled=True)]
    all_to_all x0 -> x6, starting transfers between devices: none -> 37.8 us  [exchange(): lax.all_to_all(messages, axis, split_axis=0, concat_axis=0, tiled=True)]
    dot_general x66 -> x30, matrix products: 45.9 us -> 8.65 us  [the longest x9 1.8 us: applied(): jnp.matmul(maps[..., :WIDTH], state, precision=BEST) + maps[..., WIDTH:]]
    all_to_all x1 -> x0, blocking collectives: 9.58 us -> none  [from_everyone(): return lax.all_to_all(copies, axis, split_axis=0, concat_axis=0, tiled=True)]
  transfers between devices with their start and end apart: 6 -> 7, of which waited for: 6 -> 7; matrix products, arithmetic and copies ran while one was open for 7% -> 1% of each run, Pallas kernels for 0% -> 0%
where the time goes in v1:
time: 176 us; the launch traced here: 175 us
  waiting for transfers between devices  109 us (62%)
  starting transfers between devices  39.7 us (23%)
  local copies, waits for them, and re-layouts  11.5 us (7%)
  matrix products  8.78 us (5%)
  other arithmetic  4.24 us (2%)
    all_to_all x6, waiting for transfers between devices, exchange(): lax.all_to_all(messages, axis, split_axis=0, concat_axis=0, tiled=True)  106 us
    all_to_all x6, starting transfers between devices, exchange(): lax.all_to_all(messages, axis, split_axis=0, concat_axis=0, tiled=True)  37.8 us
  transfers between devices with their start and end apart: 7, of which 7 were waited for; matrix products, arithmetic and copies ran while one was open for 1% of the time, Pallas kernels for 0%

profile of v1, /device:TPU:1, one launch (start us, length us, event | category | flops | bytes accessed | tf_op | source)
XLA Modules:
  0.0 175.0 jit_solution(8623035142511396311)
XLA Ops:
  0.6 3.3 %reshape_reshape.3 = bf16[128,8,8,64]{3,2,1,0:T(8,128)(2,1)S(1)} reshape(bf16[2,64,4096]{2,1,0:T(8,128)(2,1)} %param.15) | data formatting | bytes 2097152 | tf_op jit(solution)/shard_map/reshape;reshape | solution.py:123
  4.0 2.9 %copy.36 = bf16[8,128,8,64]{1,3,2,0:T(8,128)(2,1)} copy(bf16[8,128,8,64]{3,0,2,1:T(8,128)(2,1)S(1)} %bitcast.140) | data formatting | bytes 2097152 | tf_op jit(solution)/shard_map/transpose | solution.py:123
  6.8 7.8 %all-to-all-start.1 = ((bf16[8,128,512]{1,2,0:T(8,128)(2,1)}), bf16[8,128,512]{1,2,0:T(8,128)(2,1)S(1)}, u32[]{:S(2)}, u32[]{:S(2)}) async-start(bf16[8,128,512]{1,2,0:T(8,128)(2,1)} %bitcast.142), calls=%async_computation.1 | async-start | bytes 2097152 | tf_op jit(solution)/shard_map/all_to_all | solution.py:15
  14.7 0.4 fusion.6
  15.3 26.6 %all-to-all-done.1 = bf16[8,128,512]{1,2,0:T(8,128)(2,1)S(1)} async-done(((bf16[8,128,512]{1,2,0:T(8,128)(2,1)}), bf16[8,128,512]{1,2,0:T(8,128)(2,1)S(1)}, u32[]{:S(2)}, u32[]{:S(2)}) %all-to-all-start.1) | async-done | bytes 1048608 | tf_op jit(solution)/shard_map/all_to_all | solution.py:15
  41.9 0.8 broadcast_in_dim.30
  42.7 11.9 %all-to-all-start = ((bf16[8,64,512]{2,1,0:T(8,128)(2,1)}), bf16[8,64,512]{2,1,0:T(8,128)(2,1)S(1)}, u32[]{:S(2)}, u32[]{:S(2)}) async-start(bf16[8,64,512]{2,1,0:T(8,128)(2,1)} %broadcast_in_dim.30), calls=%async_computation | async-start | bytes 1048576 | tf_op jit(solution)/shard_map/all_to_all | solution.py:15
  55.0 0.5 copy.37
  55.5 17.1 %all-to-all-done = bf16[8,64,512]{2,1,0:T(8,128)(2,1)S(1)} async-done(((bf16[8,64,512]{2,1,0:T(8,128)(2,1)}), bf16[8,64,512]{2,1,0:T(8,128)(2,1)S(1)}, u32[]{:S(2)}, u32[]{:S(2)}) %all-to-all-start) | async-done | bytes 524320 | tf_op jit(solution)/shard_map/all_to_all | solution.py:15
  72.6 0.8 fusion
  73.4 0.5 copy.38
  74.4 1.1 pad_maximum_fusion
  75.5 3.6 %all-to-all-start.2 = ((bf16[8,272,256]{2,1,0:T(8,128)(2,1)}), bf16[8,272,256]{2,1,0:T(8,128)(2,1)S(1)}, u32[]{:S(2)}, u32[]{:S(2)}) async-start(bf16[8,272,256]{2,1,0:T(8,128)(2,1)} %pad_maximum_fusion), calls=%async_computation.2 | async-start | bytes 2228224 | tf_op jit(solution)/shard_map/all_to_all | solution.py:15
  79.2 30.5 %all-to-all-done.2 = bf16[8,272,256]{2,1,0:T(8,128)(2,1)S(1)} async-done(((bf16[8,272,256]{2,1,0:T(8,128)(2,1)}), bf16[8,272,256]{2,1,0:T(8,128)(2,1)S(1)}, u32[]{:S(2)}, u32[]{:S(2)}) %all-to-all-start.2) | async-done | bytes 1114144 | tf_op jit(solution)/shard_map/all_to_all | solution.py:15
  110.6 0.5 fusion.2
  113.9 0.4 fusion.11
  114.3 0.7 fusion.39
  116.1 1.9 %collective-permute-start = (bf16[128,256]{1,0:T(8,128)(2,1)S(1)}, bf16[128,256]{1,0:T(8,128)(2,1)S(1)}, u32[]{:S(2)}, u32[]{:S(2)}) collective-permute-start(bf16[128,256]{1,0:T(8,128)(2,1)S(1)} %fusion.43), channel_id=1, source_target_pairs={{0,8},{8,0},{16,24},{24,16},{32,40},{40,32},{48,56},{56,48},{1,9},... | collective-permute-start | bytes 196616 | tf_op jit(solution)/shard_map/ppermute | solution.py:162
  118.1 3.0 %collective-permute-done = bf16[128,256]{1,0:T(8,128)(2,1)S(1)} collective-permute-done((bf16[128,256]{1,0:T(8,128)(2,1)S(1)}, bf16[128,256]{1,0:T(8,128)(2,1)S(1)}, u32[]{:S(2)}, u32[]{:S(2)}) %collective-permute-start) | collective-permute-done | bytes 65568 | tf_op jit(solution)/shard_map/ppermute | solution.py:162
  121.3 0.8 broadcast_in_dim.37
  122.1 3.5 %all-to-all-start.3 = ((bf16[8,128,256]{2,1,0:T(8,128)(2,1)}), bf16[8,128,256]{2,1,0:T(8,128)(2,1)S(1)}, u32[]{:S(2)}, u32[]{:S(2)}) async-start(bf16[8,128,256]{2,1,0:T(8,128)(2,1)} %broadcast_in_dim.37), calls=%async_computation.3 | async-start | bytes 1048576 | tf_op jit(solution)/shard_map/all_to_all | solution.py:15
  125.8 16.1 %all-to-all-done.3 = bf16[8,128,256]{2,1,0:T(8,128)(2,1)S(1)} async-done(((bf16[8,128,256]{2,1,0:T(8,128)(2,1)}), bf16[8,128,256]{2,1,0:T(8,128)(2,1)S(1)}, u32[]{:S(2)}, u32[]{:S(2)}) %all-to-all-start.3) | async-done | bytes 524320 | tf_op jit(solution)/shard_map/all_to_all | solution.py:15
  143.7 0.4 fusion.1
  144.1 0.8 pad_maximum_fusion.2
  144.9 3.5 %all-to-all-start.4 = ((bf16[8,192,128]{2,1,0:T(8,128)(2,1)}), bf16[8,192,128]{2,1,0:T(8,128)(2,1)S(1)}, u32[]{:S(2)}, u32[]{:S(2)}) async-start(bf16[8,192,128]{2,1,0:T(8,128)(2,1)} %pad_maximum_fusion.2), calls=%async_computation.4 | async-start | bytes 786432 | tf_op jit(solution)/shard_map/all_to_all | solution.py:15
  148.6 12.1 %all-to-all-done.4 = bf16[8,192,128]{2,1,0:T(8,128)(2,1)S(1)} async-done(((bf16[8,192,128]{2,1,0:T(8,128)(2,1)}), bf16[8,192,128]{2,1,0:T(8,128)(2,1)S(1)}, u32[]{:S(2)}, u32[]{:S(2)}) %all-to-all-start.4) | async-done | bytes 393248 | tf_op jit(solution)/shard_map/all_to_all | solution.py:15
  160.9 0.4 fusion.15
  161.6 0.6 broadcast_in_dim.73
  162.3 7.6 %all-to-all-start.5 = ((bf16[8,2,64]{2,1,0:T(2,128)(2,1)}), bf16[8,2,64]{2,1,0:T(2,128)(2,1)S(1)}, u32[]{:S(2)}, u32[]{:S(2)}) async-start(bf16[8,2,64]{2,1,0:T(2,128)(2,1)} %broadcast_in_dim.73), calls=%async_computation.5 | async-start | bytes 8192 | tf_op jit(solution)/shard_map/all_to_all | solution.py:15
  169.8 0.7 slice_bitcast_fusion
  170.5 3.9 %all-to-all-done.5 = bf16[8,2,64]{2,1,0:T(2,128)(2,1)S(1)} async-done(((bf16[8,2,64]{2,1,0:T(2,128)(2,1)}), bf16[8,2,64]{2,1,0:T(2,128)(2,1)S(1)}, u32[]{:S(2)}, u32[]{:S(2)}) %all-to-all-start.5) | async-done | bytes 2080 | tf_op jit(solution)/shard_map/all_to_all | solution.py:15
  174.4 0.5 reduce_sum.52
  (123 shorter events, 8.4 us)
Async XLA Ops:
  0.6 160.9 %copy-start = (bf16[256,64]{0,1:T(8,128)(2,1)S(1)}, bf16[256,64]{0,1:T(8,128)(2,1)}, u32[]{:S(2)}) copy-start(bf16[256,64]{0,1:T(8,128)(2,1)} %param.29) | copy-start | bytes 98308
  3.9 10.7 %copy-start.1 = (bf16[2,64,4096]{2,1,0:T(8,128)(2,1)S(1)}, bf16[2,64,4096]{2,1,0:T(8,128)(2,1)}, u32[]{:S(2)}) copy-start(bf16[2,64,4096]{2,1,0:T(8,128)(2,1)} %param.15) | copy-start | bytes 3145732
  3.9 10.7 %copy-start.3 = (bf16[4096,16]{0,1:T(8,128)(2,1)S(1)}, bf16[4096,16]{0,1:T(8,128)(2,1)}, u32[]{:S(2)}) copy-start(bf16[4096,16]{0,1:T(8,128)(2,1)} %param.19) | copy-start | bytes 393220
  3.9 10.7 %copy-start.4 = (bf16[4096,16]{0,1:T(8,128)(2,1)S(1)}, bf16[4096,16]{0,1:T(8,128)(2,1)}, u32[]{:S(2)}) copy-start(bf16[4096,16]{0,1:T(8,128)(2,1)} %param.18) | copy-start | bytes 393220
  6.8 8.4 %copy-start.5 = (bf16[64,256]{1,0:T(8,128)(2,1)S(1)}, bf16[64,256]{1,0:T(8,128)(2,1)}, u32[]{:S(2)}) copy-start(bf16[64,256]{1,0:T(8,128)(2,1)} %param.16) | copy-start | bytes 98308
  6.8 8.4 %copy-start.6 = (bf16[64,256]{1,0:T(8,128)(2,1)S(1)}, bf16[64,256]{1,0:T(8,128)(2,1)}, u32[]{:S(2)}) copy-start(bf16[64,256]{1,0:T(8,128)(2,1)} %param.17) | copy-start | bytes 98308
  6.8 35.1 %all-to-all-start.1 = ((bf16[8,128,512]{1,2,0:T(8,128)(2,1)}), bf16[8,128,512]{1,2,0:T(8,128)(2,1)S(1)}, u32[]{:S(2)}, u32[]{:S(2)}) async-start(bf16[8,128,512]{1,2,0:T(8,128)(2,1)} %bitcast.142), calls=%async_computation.1 | async-start | bytes 2097152 | tf_op jit(solution)/shard_map/all_to_all | solution.py:15
  14.6 40.1 %copy-start.7 = (f32[2,64,2]{1,2,0:T(2,128)S(1)}, f32[2,64,2]{1,2,0:T(2,128)}, u32[]{:S(2)}) copy-start(f32[2,64,2]{1,2,0:T(2,128)} %param.22) | copy-start | bytes 3076
  14.6 40.1 %copy-start.15 = (f32[2]{0:T(128)S(1)}, f32[2]{0:T(128)}, u32[]{:S(2)}) copy-start(f32[2]{0:T(128)} %param.21) | copy-start | bytes 28
  14.6 40.1 %copy-start.13 = (f32[2]{0:T(128)S(1)}, f32[2]{0:T(128)}, u32[]{:S(2)}) copy-start(f32[2]{0:T(128)} %param.20) | copy-start | bytes 28
  42.7 29.9 %all-to-all-start = ((bf16[8,64,512]{2,1,0:T(8,128)(2,1)}), bf16[8,64,512]{2,1,0:T(8,128)(2,1)S(1)}, u32[]{:S(2)}, u32[]{:S(2)}) async-start(bf16[8,64,512]{2,1,0:T(8,128)(2,1)} %broadcast_in_dim.30), calls=%async_computation | async-start | bytes 1048576 | tf_op jit(solution)/shard_map/all_to_all | solution.py:15
  75.5 34.2 %all-to-all-start.2 = ((bf16[8,272,256]{2,1,0:T(8,128)(2,1)}), bf16[8,272,256]{2,1,0:T(8,128)(2,1)S(1)}, u32[]{:S(2)}, u32[]{:S(2)}) async-start(bf16[8,272,256]{2,1,0:T(8,128)(2,1)} %pad_maximum_fusion), calls=%async_computation.2 | async-start | bytes 2228224 | tf_op jit(solution)/shard_map/all_to_all | solution.py:15
  115.0 3.0 %copy-start.8 = (bf16[2,256]{1,0:T(2,128)(2,1)S(1)}, bf16[2,256]{1,0:T(2,128)(2,1)}, u32[]{:S(2)}) copy-start(bf16[2,256]{1,0:T(2,128)(2,1)} %param.26) | copy-start | bytes 3076
  115.4 10.2 %copy-start.9 = (bf16[2,256]{1,0:T(2,128)(2,1)S(1)}, bf16[2,256]{1,0:T(2,128)(2,1)}, u32[]{:S(2)}) copy-start(bf16[2,256]{1,0:T(2,128)(2,1)} %param.23) | copy-start | bytes 3076
  115.5 10.2 %copy-start.10 = (bf16[2,256]{1,0:T(2,128)(2,1)S(1)}, bf16[2,256]{1,0:T(2,128)(2,1)}, u32[]{:S(2)}) copy-start(bf16[2,256]{1,0:T(2,128)(2,1)} %param.25) | copy-start | bytes 3076
  116.1 5.0 %collective-permute-start = (bf16[128,256]{1,0:T(8,128)(2,1)S(1)}, bf16[128,256]{1,0:T(8,128)(2,1)S(1)}, u32[]{:S(2)}, u32[]{:S(2)}) collective-permute-start(bf16[128,256]{1,0:T(8,128)(2,1)S(1)} %fusion.43), channel_id=1, source_target_pairs={{0,8},{8,0},{16,24},{24,16},{32,40},{40,32},{48,56},{56,48},{1,9},... | collective-permute-start | bytes 196616 | tf_op jit(solution)/shard_map/ppermute | solution.py:162
  122.1 19.8 %all-to-all-start.3 = ((bf16[8,128,256]{2,1,0:T(8,128)(2,1)}), bf16[8,128,256]{2,1,0:T(8,128)(2,1)S(1)}, u32[]{:S(2)}, u32[]{:S(2)}) async-start(bf16[8,128,256]{2,1,0:T(8,128)(2,1)} %broadcast_in_dim.37), calls=%async_computation.3 | async-start | bytes 1048576 | tf_op jit(solution)/shard_map/all_to_all | solution.py:15
  142.2 6.2 %copy-start.11 = (bf16[2,256]{1,0:T(2,128)(2,1)S(1)}, bf16[2,256]{1,0:T(2,128)(2,1)}, u32[]{:S(2)}) copy-start(bf16[2,256]{1,0:T(2,128)(2,1)} %param.24) | copy-start | bytes 3076
  142.2 6.3 %copy-start.12 = (f32[2,2]{1,0:T(2,128)S(1)}, f32[2,2]{1,0:T(2,128)}, u32[]{:S(2)}) copy-start(f32[2,2]{1,0:T(2,128)} %param.27) | copy-start | bytes 52
  142.7 18.7 %copy-start.14 = (f32[128]{0:T(128)S(1)}, f32[128]{0:T(128)}, u32[]{:S(2)}) copy-start(f32[128]{0:T(128)} %param.28) | copy-start | bytes 1540
  144.9 15.7 %all-to-all-start.4 = ((bf16[8,192,128]{2,1,0:T(8,128)(2,1)}), bf16[8,192,128]{2,1,0:T(8,128)(2,1)S(1)}, u32[]{:S(2)}, u32[]{:S(2)}) async-start(bf16[8,192,128]{2,1,0:T(8,128)(2,1)} %pad_maximum_fusion.2), calls=%async_computation.4 | async-start | bytes 786432 | tf_op jit(solution)/shard_map/all_to_all | solution.py:15
  160.7 14.3 %copy-start.2 = (bf16[2,2,2,64,128]{4,3,2,1,0:T(8,128)(2,1)}, bf16[2,2,2,64,128]{4,3,2,1,0:T(8,128)(2,1)S(1)}, u32[]{:S(2)}) copy-start(bf16[2,2,2,64,128]{4,3,2,1,0:T(8,128)(2,1)S(1)} %slice.371) | copy-start | bytes 393220
  162.3 12.2 %all-to-all-start.5 = ((bf16[8,2,64]{2,1,0:T(2,128)(2,1)}), bf16[8,2,64]{2,1,0:T(2,128)(2,1)S(1)}, u32[]{:S(2)}, u32[]{:S(2)}) async-start(bf16[8,2,64]{2,1,0:T(2,128)(2,1)} %broadcast_in_dim.73), calls=%async_computation.5 | async-start | bytes 8192 | tf_op jit(solution)/shard_map/all_to_all | solution.py:15

commit v2 on v1

--- a/solution.py
+++ b/solution.py
@@ -1,6 +1,8 @@
 import jax
 import jax.numpy as jnp
 from jax import lax
+from jax.experimental import pallas as pl
+from jax.experimental.pallas import tpu as pltpu
 from jax.sharding import Mesh
 from jax.sharding import PartitionSpec as P
 
@@ -9,6 +11,8 @@
 EPSILON = 1e-06
 BEST = lax.Precision.HIGHEST
 SP = ("z", "y")
+INTERPRET = False
+SMALL = pltpu.CompilerParams(vmem_limit_bytes=16 * 1024 * 1024)
 
 
 def exchange(messages, axis):
@@ -17,6 +21,64 @@
 
 def from_everyone(array, axis):
     return exchange(jnp.broadcast_to(array, (lax.axis_size(axis), *array.shape)), axis)
+
+
+def columns_body(tokens_ref, columns_ref):
+    share = tokens_ref.shape[1] // (SIDE * SIDE)
+    for to in range(SIDE):
+        at = [(k * SIDE + to) * share for k in range(SIDE)]
+        columns_ref[to] = jnp.concatenate([tokens_ref[:, a : a + share] for a in at], axis=1)
+
+
+def columns_by_owner(flat):
+    rows, model = flat.shape
+    step = rows // 4
+    return pl.pallas_call(
+        columns_body,
+        grid=(rows // step,),
+        in_specs=[pl.BlockSpec((step, model), lambda i: (i, 0))],
+        out_specs=pl.BlockSpec((SIDE, step, model // SIDE), lambda i: (0, i, 0)),
+        out_shape=jax.ShapeDtypeStruct((SIDE, rows, model // SIDE), flat.dtype),
+        interpret=INTERPRET,
+        compiler_params=SMALL,
+        name="columns",
+    )(flat)
+
+
+VMEM = pl.BlockSpec(memory_space=pltpu.VMEM)
+
+
+def partial_body(tokens_ref, weights_ref, gates_ref, sent_ref):
+    line, rows, _ = tokens_ref.shape
+    owners, halves, sent_rows, width = sent_ref.shape
+    ranges = line // halves
+    positions = (sent_rows - gates_ref.shape[2]) // ranges
+    prompts = rows // positions
+    heads = owners // prompts
+    for k in range(line):
+        half, j = k // ranges, k % ranges
+        part = jnp.dot(tokens_ref[k], weights_ref[...], preferred_element_type=jnp.float32)
+        part = part.astype(sent_ref.dtype)
+        for p in range(prompts):
+            for h in range(heads):
+                sent_ref[p * heads + h, half, j * positions : (j + 1) * positions, :] = part[
+                    p * positions : (p + 1) * positions, h * width : (h + 1) * width
+                ]
+    sent_ref[:, :, ranges * positions :, :] = gates_ref[...]
+
+
+def partial_projections(tokens, weights, gates, positions):
+    owners, halves, extra, width = gates.shape
+    sent_rows = tokens.shape[0] // halves * positions + extra
+    return pl.pallas_call(
+        partial_body,
+        in_specs=[VMEM, VMEM, VMEM],
+        out_specs=VMEM,
+        out_shape=jax.ShapeDtypeStruct((owners, halves, sent_rows, width), tokens.dtype),
+        interpret=INTERPRET,
+        compiler_params=SMALL,
+        name="partials",
+    )(tokens, weights, gates)
 
 
 def unit_inverse(lower_part):
@@ -120,9 +182,9 @@
         axis=1,
     )
     flat = tokens.reshape(rows, model)
-    columns = flat.reshape(rows, SIDE, SIDE, share).transpose(2, 0, 1, 3).reshape(SIDE, rows, -1)
+    columns = columns_by_owner(flat)
     line_tokens = exchange(columns, "y")
-    line_weights = from_everyone(weights, "z").reshape(SIDE * share, -1)
+    line_weights = lax.all_gather(weights, "z", axis=0, tiled=True)
 
     drivers = jnp.concatenate([strength_projection, fading_driver_projection], axis=1)
     logits = jnp.dot(flat, drivers, preferred_element_type=jnp.float32).astype(jnp.bfloat16)
@@ -133,15 +195,13 @@
     gates = jnp.stack([*two_parts(beta), *two_parts(fading)])
     gates = gates.transpose(1, 3, 0, 2).reshape(prompts, heads, 1, 1, 4 * positions)
 
-    partial = jnp.dot(
-        line_tokens.reshape(SIDE * rows, -1), line_weights, preferred_element_type=jnp.float32
-    ).astype(jnp.bfloat16)
-    partial = partial.reshape(2, half, prompts, positions, heads, 2 * WIDTH)
-    partial = partial.transpose(2, 4, 0, 1, 3, 5).reshape(
-        prompts, heads, 2, half * positions, 2 * WIDTH
-    )
     gates = jnp.broadcast_to(gates, (prompts, heads, 2, 16, 4 * positions))
-    sent = jnp.concatenate([partial, gates], axis=3).reshape(SIDE, half * positions + 16, -1)
+    sent = partial_projections(
+        line_tokens,
+        line_weights,
+        gates.reshape(prompts * heads, 2, 16, 4 * positions),
+        positions,
+    ).reshape(SIDE, half * positions + 16, 4 * positions)
     got = exchange(sent, "y")
 
     sums = got[:, : half * positions].astype(jnp.float32).sum(axis=0)

time: 176 us -> 149 us (0.85)
  waiting for transfers between devices: 109 us -> 60.7 us
  blocking collectives: 0 us -> 27.2 us
  local copies, waits for them, and re-layouts: 11.5 us -> 4.2 us
  Pallas kernels: 0 us -> 3.57 us
    all_to_all x6 -> x5, waiting for transfers between devices: 106 us -> 57.7 us  [exchange(): lax.all_to_all(messages, axis, split_axis=0, concat_axis=0, tiled=True)]
    all_gather x0 -> x1, blocking collectives: none -> 27.2 us  [per_device(): line_weights = lax.all_gather(weights, 'z', axis=0, tiled=True)]
    pallas_call x0 -> x2, Pallas kernels: none -> 3.57 us  [the longest x1 1.84 us: columns_by_owner(): pl.pallas_call(columns_body, grid=(rows // step,), in_specs=[pl.BlockSpec...]
    another operation x1 -> x0, local copies, waits for them, and re-layouts: 3.26 us -> none  [per_device(): flat.reshape(rows, SIDE, SIDE, share).transpose(2, 0, 1, 3)]
    transpose x2 -> x0, local copies, waits for them, and re-layouts: 3.06 us -> none  [the longest x1 2.87 us: per_device(): flat.reshape(rows, SIDE, SIDE, share).transpose(2, 0, 1, 3)]
    all_to_all x6 -> x5, starting transfers between devices: 37.8 us -> 37.8 us  [exchange(): lax.all_to_all(messages, axis, split_axis=0, concat_axis=0, tiled=True)]
  transfers between devices with their start and end apart: 7 -> 6, of which waited for: 7 -> 5; matrix products, arithmetic and copies ran while one was open for 1% -> 1% of each run, Pallas kernels for 0% -> 0%
where the time goes in v2:
time: 149 us; the launch traced here: 148 us
  waiting for transfers between devices  60.7 us (41%)
  starting transfers between devices  39.8 us (27%)
  blocking collectives  27.2 us (18%)
  matrix products  8.02 us (5%)
  local copies, waits for them, and re-layouts  4.2 us (3%)
  Pallas kernels  3.57 us (2%)
  other arithmetic  3.15 us (2%)
    all_to_all x5, waiting for transfers between devices, exchange(): lax.all_to_all(messages, axis, split_axis=0, concat_axis=0, tiled=True)  57.7 us
    all_to_all x5, starting transfers between devices, exchange(): lax.all_to_all(messages, axis, split_axis=0, concat_axis=0, tiled=True)  37.8 us
    all_gather x1, blocking collectives, per_device(): line_weights = lax.all_gather(weights, 'z', axis=0, tiled=True)  27.2 us
    ppermute x1, waiting for transfers between devices, per_device(): other = lax.ppermute(whole, 'y', [(i, i ^ 1) for i in range(SIDE)])  2.99 us
  transfers between devices with their start and end apart: 6, of which 5 were waited for; matrix products, arithmetic and copies ran while one was open for 1% of the time, Pallas kernels for 0%

profile of v2, /device:TPU:1, one launch (start us, length us, event | category | flops | bytes accessed | tf_op | source)
XLA Modules:
  0.0 148.0 jit_solution(3446032366654902813)
XLA Ops:
  0.7 1.2 copy-done.1
  1.9 1.8 %columns.1 = bf16[8,128,512]{2,1,0:T(8,128)(2,1)} custom-call(bf16[128,4096]{1,0:T(8,128)(2,1)S(1)} %bitcast.131), custom_call_target="tpu_custom_call" | custom-call | tf_op jit(solution)/shard_map/columns/pallas_call | solution.py:36
  3.7 7.8 %all-to-all-start = ((bf16[8,128,512]{2,1,0:T(8,128)(2,1)}), bf16[8,128,512]{2,1,0:T(8,128)(2,1)S(1)}, u32[]{:S(2)}, u32[]{:S(2)}) async-start(bf16[8,128,512]{2,1,0:T(8,128)(2,1)} %columns.1), calls=%async_computation | async-start | bytes 2097152 | tf_op jit(solution)/shard_map/all_to_all | solution.py:19
  11.6 0.4 fusion.5
  12.5 27.2 %all_gather.3.weights_ref = bf16[512,512]{1,0:T(8,128)(2,1)S(1)} all-gather(bf16[64,512]{1,0:T(8,128)(2,1)S(1)} %pad_maximum_fusion.8), channel_id=1, replica_groups=mesh['z'=8,'y'=8,'tp'=8] {'z'}, dimensions={0}, use_global_device_ids=true | all-gather | bytes 589824 | tf_op jit(solution)/shard_map/all_gather | solution.py:187
  39.8 1.7 %partials.1 = bf16[4,2,272,256]{3,2,1,0:T(8,128)(2,1)} custom-call(bf16[8,128,512]{2,1,0:T(8,128)(2,1)S(1)} %all-to-all-done.tokens_ref, bf16[512,512]{1,0:T(8,128)(2,1)S(1)} %all_gather.3.weights_ref, bf16[4,2,16,256]{3,2,1,0:T(8,128)(2,1)S(1)} %broadcast_in_dim.25.gates_ref), custom_call_target="tpu_custom_call" | custom-call | tf_op jit(solution)/shard_map/partials/pallas_call | solution.py:73
  41.5 6.3 %all-to-all-start.1 = ((bf16[8,272,256]{2,1,0:T(8,128)(2,1)}), bf16[8,272,256]{2,1,0:T(8,128)(2,1)S(1)}, u32[]{:S(2)}, u32[]{:S(2)}) async-start(bf16[8,272,256]{2,1,0:T(8,128)(2,1)} %bitcast.7), calls=%async_computation.1 | async-start | bytes 2228224 | tf_op jit(solution)/shard_map/all_to_all | solution.py:19
  47.9 26.4 %all-to-all-done.1 = bf16[8,272,256]{2,1,0:T(8,128)(2,1)S(1)} async-done(((bf16[8,272,256]{2,1,0:T(8,128)(2,1)}), bf16[8,272,256]{2,1,0:T(8,128)(2,1)S(1)}, u32[]{:S(2)}, u32[]{:S(2)}) %all-to-all-start.1) | async-done | bytes 1114144 | tf_op jit(solution)/shard_map/all_to_all | solution.py:19
  75.4 0.4 fusion.1
  76.4 0.3 fusion.35
  76.9 0.3 fusion.33
  77.4 0.3 fusion.31
  78.0 0.3 fusion.29
  78.5 0.4 fusion.10
  78.8 0.7 fusion.38
  79.7 0.3 fusion.25
  80.3 0.3 fusion.44
  80.6 1.9 %collective-permute-start = (bf16[128,256]{1,0:T(8,128)(2,1)S(1)}, bf16[128,256]{1,0:T(8,128)(2,1)S(1)}, u32[]{:S(2)}, u32[]{:S(2)}) collective-permute-start(bf16[128,256]{1,0:T(8,128)(2,1)S(1)} %fusion.42), channel_id=1, source_target_pairs={{0,8},{8,0},{16,24},{24,16},{32,40},{40,32},{48,56},{56,48},{1,9},... | collective-permute-start | bytes 196616 | tf_op jit(solution)/shard_map/ppermute | solution.py:222
  82.6 3.0 %collective-permute-done = bf16[128,256]{1,0:T(8,128)(2,1)S(1)} collective-permute-done((bf16[128,256]{1,0:T(8,128)(2,1)S(1)}, bf16[128,256]{1,0:T(8,128)(2,1)S(1)}, u32[]{:S(2)}, u32[]{:S(2)}) %collective-permute-start) | collective-permute-done | bytes 65568 | tf_op jit(solution)/shard_map/ppermute | solution.py:222
  85.9 0.8 broadcast_in_dim.28
  86.7 12.3 %all-to-all-start.2 = ((bf16[8,128,256]{2,1,0:T(8,128)(2,1)}), bf16[8,128,256]{2,1,0:T(8,128)(2,1)S(1)}, u32[]{:S(2)}, u32[]{:S(2)}) async-start(bf16[8,128,256]{2,1,0:T(8,128)(2,1)} %broadcast_in_dim.28), calls=%async_computation.2 | async-start | bytes 1048576 | tf_op jit(solution)/shard_map/all_to_all | solution.py:19
  99.2 15.7 %all-to-all-done.2 = bf16[8,128,256]{2,1,0:T(8,128)(2,1)S(1)} async-done(((bf16[8,128,256]{2,1,0:T(8,128)(2,1)}), bf16[8,128,256]{2,1,0:T(8,128)(2,1)S(1)}, u32[]{:S(2)}, u32[]{:S(2)}) %all-to-all-start.2) | async-done | bytes 524320 | tf_op jit(solution)/shard_map/all_to_all | solution.py:19
  116.7 0.4 fusion
  117.1 0.8 pad_maximum_fusion.1
  117.9 3.5 %all-to-all-start.3 = ((bf16[8,192,128]{2,1,0:T(8,128)(2,1)}), bf16[8,192,128]{2,1,0:T(8,128)(2,1)S(1)}, u32[]{:S(2)}, u32[]{:S(2)}) async-start(bf16[8,192,128]{2,1,0:T(8,128)(2,1)} %pad_maximum_fusion.1), calls=%async_computation.3 | async-start | bytes 786432 | tf_op jit(solution)/shard_map/all_to_all | solution.py:19
  121.6 11.7 %all-to-all-done.3 = bf16[8,192,128]{2,1,0:T(8,128)(2,1)S(1)} async-done(((bf16[8,192,128]{2,1,0:T(8,128)(2,1)}), bf16[8,192,128]{2,1,0:T(8,128)(2,1)S(1)}, u32[]{:S(2)}, u32[]{:S(2)}) %all-to-all-start.3) | async-done | bytes 393248 | tf_op jit(solution)/shard_map/all_to_all | solution.py:19
  133.5 0.4 fusion.14
  134.3 0.6 broadcast_in_dim.30
  134.9 8.0 %all-to-all-start.4 = ((bf16[8,2,64]{2,1,0:T(2,128)(2,1)}), bf16[8,2,64]{2,1,0:T(2,128)(2,1)S(1)}, u32[]{:S(2)}, u32[]{:S(2)}) async-start(bf16[8,2,64]{2,1,0:T(2,128)(2,1)} %broadcast_in_dim.30), calls=%async_computation.4 | async-start | bytes 8192 | tf_op jit(solution)/shard_map/all_to_all | solution.py:19
  142.9 0.7 slice_bitcast_fusion
  143.5 3.9 %all-to-all-done.4 = bf16[8,2,64]{2,1,0:T(2,128)(2,1)S(1)} async-done(((bf16[8,2,64]{2,1,0:T(2,128)(2,1)}), bf16[8,2,64]{2,1,0:T(2,128)(2,1)S(1)}, u32[]{:S(2)}, u32[]{:S(2)}) %all-to-all-start.4) | async-done | bytes 2080 | tf_op jit(solution)/shard_map/all_to_all | solution.py:19
  147.5 0.5 reduce_sum.52
  (115 shorter events, 6.4 us)
Async XLA Ops:
  0.6 133.5 %copy-start = (bf16[256,64]{0,1:T(8,128)(2,1)S(1)}, bf16[256,64]{0,1:T(8,128)(2,1)}, u32[]{:S(2)}) copy-start(bf16[256,64]{0,1:T(8,128)(2,1)} %param.29) | copy-start | bytes 98308
  0.6 1.2 copy-start.1
  3.7 7.8 %copy-start.2 = (bf16[2,64,4096]{2,1,0:T(8,128)(2,1)S(1)}, bf16[2,64,4096]{2,1,0:T(8,128)(2,1)}, u32[]{:S(2)}) copy-start(bf16[2,64,4096]{2,1,0:T(8,128)(2,1)} %param.15) | copy-start | bytes 3145732
  3.7 7.8 %copy-start.4 = (bf16[4096,16]{0,1:T(8,128)(2,1)S(1)}, bf16[4096,16]{0,1:T(8,128)(2,1)}, u32[]{:S(2)}) copy-start(bf16[4096,16]{0,1:T(8,128)(2,1)} %param.19) | copy-start | bytes 393220
  3.7 7.9 %copy-start.5 = (bf16[4096,16]{0,1:T(8,128)(2,1)S(1)}, bf16[4096,16]{0,1:T(8,128)(2,1)}, u32[]{:S(2)}) copy-start(bf16[4096,16]{0,1:T(8,128)(2,1)} %param.18) | copy-start | bytes 393220
  3.7 36.0 %all-to-all-start = ((bf16[8,128,512]{2,1,0:T(8,128)(2,1)}), bf16[8,128,512]{2,1,0:T(8,128)(2,1)S(1)}, u32[]{:S(2)}, u32[]{:S(2)}) async-start(bf16[8,128,512]{2,1,0:T(8,128)(2,1)} %columns.1), calls=%async_computation | async-start | bytes 2097152 | tf_op jit(solution)/shard_map/all_to_all | solution.py:19
  11.5 0.7 copy-start.8
  11.5 0.7 copy-start.16
  11.5 0.7 copy-start.14
  11.5 1.0 copy-start.6
  11.5 0.9 copy-start.7
  41.5 32.7 %all-to-all-start.1 = ((bf16[8,272,256]{2,1,0:T(8,128)(2,1)}), bf16[8,272,256]{2,1,0:T(8,128)(2,1)S(1)}, u32[]{:S(2)}, u32[]{:S(2)}) async-start(bf16[8,272,256]{2,1,0:T(8,128)(2,1)} %bitcast.7), calls=%async_computation.1 | async-start | bytes 2228224 | tf_op jit(solution)/shard_map/all_to_all | solution.py:19
  79.7 2.8 %copy-start.9 = (bf16[2,256]{1,0:T(2,128)(2,1)S(1)}, bf16[2,256]{1,0:T(2,128)(2,1)}, u32[]{:S(2)}) copy-start(bf16[2,256]{1,0:T(2,128)(2,1)} %param.24) | copy-start | bytes 3076
  80.6 5.0 %collective-permute-start = (bf16[128,256]{1,0:T(8,128)(2,1)S(1)}, bf16[128,256]{1,0:T(8,128)(2,1)S(1)}, u32[]{:S(2)}, u32[]{:S(2)}) collective-permute-start(bf16[128,256]{1,0:T(8,128)(2,1)S(1)} %fusion.42), channel_id=1, source_target_pairs={{0,8},{8,0},{16,24},{24,16},{32,40},{40,32},{48,56},{56,48},{1,9},... | collective-permute-start | bytes 196616 | tf_op jit(solution)/shard_map/ppermute | solution.py:222
  85.6 13.4 %copy-start.10 = (bf16[2,256]{1,0:T(2,128)(2,1)S(1)}, bf16[2,256]{1,0:T(2,128)(2,1)}, u32[]{:S(2)}) copy-start(bf16[2,256]{1,0:T(2,128)(2,1)} %param.25) | copy-start | bytes 3076
  85.7 13.4 %copy-start.11 = (bf16[2,256]{1,0:T(2,128)(2,1)S(1)}, bf16[2,256]{1,0:T(2,128)(2,1)}, u32[]{:S(2)}) copy-start(bf16[2,256]{1,0:T(2,128)(2,1)} %param.23) | copy-start | bytes 3076
  86.7 28.2 %all-to-all-start.2 = ((bf16[8,128,256]{2,1,0:T(8,128)(2,1)}), bf16[8,128,256]{2,1,0:T(8,128)(2,1)S(1)}, u32[]{:S(2)}, u32[]{:S(2)}) async-start(bf16[8,128,256]{2,1,0:T(8,128)(2,1)} %broadcast_in_dim.28), calls=%async_computation.2 | async-start | bytes 1048576 | tf_op jit(solution)/shard_map/all_to_all | solution.py:19
  116.7 4.7 %copy-start.12 = (bf16[2,256]{1,0:T(2,128)(2,1)S(1)}, bf16[2,256]{1,0:T(2,128)(2,1)}, u32[]{:S(2)}) copy-start(bf16[2,256]{1,0:T(2,128)(2,1)} %param.26) | copy-start | bytes 3076
  116.7 4.8 %copy-start.13 = (f32[2,2]{1,0:T(2,128)S(1)}, f32[2,2]{1,0:T(2,128)}, u32[]{:S(2)}) copy-start(f32[2,2]{1,0:T(2,128)} %param.27) | copy-start | bytes 52
  117.1 16.9 %copy-start.15 = (f32[128]{0:T(128)S(1)}, f32[128]{0:T(128)}, u32[]{:S(2)}) copy-start(f32[128]{0:T(128)} %param.28) | copy-start | bytes 1540
  117.9 15.3 %all-to-all-start.3 = ((bf16[8,192,128]{2,1,0:T(8,128)(2,1)}), bf16[8,192,128]{2,1,0:T(8,128)(2,1)S(1)}, u32[]{:S(2)}, u32[]{:S(2)}) async-start(bf16[8,192,128]{2,1,0:T(8,128)(2,1)} %pad_maximum_fusion.1), calls=%async_computation.3 | async-start | bytes 786432 | tf_op jit(solution)/shard_map/all_to_all | solution.py:19
  133.3 14.7 %copy-start.3 = (bf16[2,2,2,64,128]{4,3,2,1,0:T(8,128)(2,1)}, bf16[2,2,2,64,128]{4,3,2,1,0:T(8,128)(2,1)S(1)}, u32[]{:S(2)}) copy-start(bf16[2,2,2,64,128]{4,3,2,1,0:T(8,128)(2,1)S(1)} %slice.371) | copy-start | bytes 393220
  134.9 12.6 %all-to-all-start.4 = ((bf16[8,2,64]{2,1,0:T(2,128)(2,1)}), bf16[8,2,64]{2,1,0:T(2,128)(2,1)S(1)}, u32[]{:S(2)}, u32[]{:S(2)}) async-start(bf16[8,2,64]{2,1,0:T(2,128)(2,1)} %broadcast_in_dim.30), calls=%async_computation.4 | async-start | bytes 8192 | tf_op jit(solution)/shard_map/all_to_all | solution.py:19

commit v3 on v2

v3 whole, which is shorter than its diff:
```python
import jax
import jax.numpy as jnp
from jax import lax
from jax.experimental import pallas as pl
from jax.experimental.pallas import tpu as pltpu
from jax.sharding import Mesh
from jax.sharding import PartitionSpec as P

WIDTH = 128
SIDE = 8
EPSILON = 1e-06
BEST = lax.Precision.HIGHEST
SP = ("z", "y")
INTERPRET = False
SMALL = pltpu.CompilerParams(vmem_limit_bytes=16 * 1024 * 1024)


def exchange(messages, axis):
    return lax.all_to_all(messages, axis, split_axis=0, concat_axis=0, tiled=True)


def columns_body(tokens_ref, columns_ref):
    share = tokens_ref.shape[1] // (SIDE * SIDE)
    for to in range(SIDE):
        at = [(k * SIDE + to) * share for k in range(SIDE)]
        columns_ref[to] = jnp.concatenate([tokens_ref[:, a : a + share] for a in at], axis=1)


def columns_by_owner(flat):
    rows, model = flat.shape
    step = rows // 4
    return pl.pallas_call(
        columns_body,
        grid=(rows // step,),
        in_specs=[pl.BlockSpec((step, model), lambda i: (i, 0))],
        out_specs=pl.BlockSpec((SIDE, step, model // SIDE), lambda i: (0, i, 0)),
        out_shape=jax.ShapeDtypeStruct((SIDE, rows, model // SIDE), flat.dtype),
        interpret=INTERPRET,
        compiler_params=SMALL,
        name="columns",
    )(flat)


VMEM = pl.BlockSpec(memory_space=pltpu.VMEM)


def partial_body(tokens_ref, weights_ref, gates_ref, sent_ref):
    line, rows, _ = tokens_ref.shape
    owners, halves, sent_rows, width = sent_ref.shape
    ranges = line // halves
    positions = (sent_rows - gates_ref.shape[2]) // ranges
    prompts = rows // positions
    heads = owners // prompts
    for k in range(line):
        half, j = k // ranges, k % ranges
        part = jnp.dot(tokens_ref[k], weights_ref[...], preferred_element_type=jnp.float32)
        part = part.astype(sent_ref.dtype)
        for p in range(prompts):
            for h in range(heads):
                sent_ref[p * heads + h, half, j * positions : (j + 1) * positions, :] = part[
                    p * positions : (p + 1) * positions, h * width : (h + 1) * width
                ]
    sent_ref[:, :, ranges * positions :, :] = gates_ref[...]


def partial_projections(tokens, weights, gates, positions):
    owners, halves, extra, width = gates.shape
    sent_rows = tokens.shape[0] // halves * positions + extra
    return pl.pallas_call(
        partial_body,
        in_specs=[VMEM, VMEM, VMEM],
        out_specs=VMEM,
        out_shape=jax.ShapeDtypeStruct((owners, halves, sent_rows, width), tokens.dtype),
        interpret=INTERPRET,
        compiler_params=SMALL,
        name="partials",
    )(tokens, weights, gates)


def two_parts(values):
    high = lax.reduce_precision(values, 8, 7)
    return high.astype(jnp.bfloat16), (values - high).astype(jnp.bfloat16)


def best(left, right, dims=((1,), (0,))):
    return lax.dot_general(
        left, right, (dims, ((), ())), precision=BEST, preferred_element_type=jnp.float32
    )


def times(state, matrix):
    high = state.astype(jnp.bfloat16)
    low = (state - high.astype(jnp.float32)).astype(jnp.bfloat16)
    rows = state.shape[0]
    both = jnp.dot(
        jnp.concatenate([high, low], axis=0), matrix, preferred_element_type=jnp.float32
    )
    return both[:rows] + both[rows:]


def silu(x):
    return x / (1.0 + jnp.exp(-x))


def ranges_body(half_ref, got_ref, sent_ref, kept_ref):
    line, _, width = got_ref.shape
    wide = width // 2
    ranges = line // 2
    positions = sent_ref.shape[0] // (ranges * 3)
    count = ranges * positions
    half = half_ref[0]
    sums = got_ref[0, :count, :].astype(jnp.float32)
    for k in range(1, line):
        sums = sums + got_ref[k, :count, :].astype(jnp.float32)
    keys = silu(sums[:, :wide])
    keys = keys * lax.rsqrt(jnp.sum(keys * keys, axis=-1, keepdims=True) + EPSILON)
    values = silu(sums[:, wide:])
    gates = got_ref[pl.ds(half * ranges, ranges), count:, :wide].astype(jnp.float32)
    beta = gates[:, 0, :] + gates[:, 1, :]
    fading = gates[:, 2, :] + gates[:, 3, :]
    up_to = lax.broadcasted_iota(jnp.int32, (wide, wide), 0) <= lax.broadcasted_iota(
        jnp.int32, (wide, wide), 1
    )
    sums_to = best(jnp.concatenate([beta, fading], axis=0), up_to.astype(jnp.float32))[ranges:]
    columns = jnp.concatenate([beta, sums_to], axis=0).T
    row = lax.broadcasted_iota(jnp.int32, (positions, positions), 0)
    column = lax.broadcasted_iota(jnp.int32, (positions, positions), 1)
    strict = row > column
    unit = (
        lax.broadcasted_iota(jnp.int32, (wide, wide), 0)
        == lax.broadcasted_iota(jnp.int32, (wide, wide), 1)
    ).astype(jnp.float32)
    powers, solved, tails, lasts = [], [], [], []
    for j in range(ranges):
        at = slice(j * positions, (j + 1) * positions)
        b = columns[:positions, j : j + 1]
        total = columns[:positions, ranges + j : ranges + j + 1]
        last = total[positions - 1 :, :]
        across = sums_to[j : j + 1, :positions]
        scaled = keys[at] * b
        inner = best(scaled, keys[at], ((1,), (1,)))
        spread = jnp.exp(jnp.where(strict, total - across, 0.0))
        powers.append(jnp.where(strict, inner * spread, 0.0))
        solved.append(jnp.concatenate([scaled * jnp.exp(total), values[at] * b], axis=1))
        tails.append(keys[at] * jnp.exp(last - total))
        lasts.append(jnp.exp(last))
    for j in range(ranges):
        solved[j] = solved[j] - best(powers[j], solved[j])
    reached = 2
    while reached < positions:
        for j in range(ranges):
            powers[j] = best(powers[j], powers[j])
        for j in range(ranges):
            solved[j] = solved[j] + best(powers[j], solved[j])
        reached *= 2
    so_far = None
    for j in range(ranges):
        moved = best(solved[j], tails[j], ((0,), (0,)))
        step = lasts[j] * unit - moved[:wide]
        if so_far is None:
            so_far = jnp.concatenate([step, moved[wide:]], axis=0)
        else:
            both = best(so_far, step)
            so_far = jnp.concatenate([both[:wide], both[wide:] + moved[wide:]], axis=0)
        out = so_far.astype(jnp.bfloat16)
        low, high = out[wide : wide + positions], out[wide + positions :]
        sent_ref[j * wide : (j + 1) * wide, :] = out[:wide]
        at = slice(ranges * wide + j * positions, ranges * wide + (j + 1) * positions)
        sent_ref[at, :] = jnp.where(half == 0, high, low)
        kept_ref[j * wide : (j + 1) * wide, :] = out[:wide]
        kept_ref[at, :] = jnp.where(half == 0, low, high)


def line_body(half_ref, kept_ref, other_ref, sent_ref):
    count, wide = kept_ref.shape
    ranges = 2 * count // (3 * wide)
    rows = wide // 2
    mine_first = half_ref[0] == 0
    step = slice((ranges - 1) * wide, ranges * wide)
    kept = jnp.concatenate([kept_ref[step, :], kept_ref[count - rows :, :]], axis=0)
    other = jnp.concatenate([other_ref[step, :], other_ref[count - rows :, :]], axis=0)
    first = jnp.where(mine_first, kept, other)
    second = jnp.where(mine_first, other, kept)
    both = jnp.dot(first, second[:wide], preferred_element_type=jnp.float32)
    added = both[wide:] + second[wide:].astype(jnp.float32)
    out = jnp.concatenate([both[:wide], added], axis=0).astype(jnp.bfloat16)
    for k in range(sent_ref.shape[0]):
        sent_ref[k] = out


def scan_body(place_ref, lines_ref, kept_ref, other_ref, sent_ref):
    lines, _, wide = lines_ref.shape
    rows = wide // 2
    ranges = sent_ref.shape[0] // 2
    z, mine_first = place_ref[0], place_ref[1] == 0
    state = lines_ref[0, wide:, :].astype(jnp.float32)
    entering = jnp.zeros_like(state)
    for k in range(1, lines):
        entering = jnp.where(z == k, state, entering)
        state = times(state, lines_ref[k, :wide, :]) + lines_ref[k, wide:, :].astype(jnp.float32)
    final = state.astype(jnp.bfloat16)
    state = entering
    for h in range(2):
        begin = state
        for j in range(ranges):
            step = slice(j * wide, (j + 1) * wide)
            extra = slice(ranges * wide + j * rows, ranges * wide + (j + 1) * rows)
            use_kept = mine_first if h == 0 else jnp.logical_not(mine_first)
            matrix = jnp.where(use_kept, kept_ref[step, :], other_ref[step, :])
            added = jnp.where(use_kept, kept_ref[extra, :], other_ref[extra, :])
            state = times(begin, matrix) + added.astype(jnp.float32)
            sent_ref[h * ranges + j, :rows, :] = state.astype(jnp.bfloat16)
            sent_ref[h * ranges + j, rows:, :] = final


def read_body(
    strength_ref,
    back_ref,
    probe_ref,
    address_ref,
    content_ref,
    outgate_ref,
    gain_ref,
    readout_ref,
    sent_ref,
):
    wide = back_ref.shape[2]
    rows = wide // 2
    prompts, width = probe_ref.shape
    heads = width // wide
    read = []
    for p in range(prompts):
        for h in range(heads):
            at, n = slice(h * wide, (h + 1) * wide), 2 * (p * heads + h)
            state = jnp.concatenate([back_ref[n, rows:, :], back_ref[n + 1, rows:, :]], axis=0)
            query = silu(probe_ref[p : p + 1, at].astype(jnp.float32))
            key = silu(address_ref[p : p + 1, at].astype(jnp.float32))
            key = key * lax.rsqrt(jnp.sum(key * key, axis=-1, keepdims=True) + EPSILON)
            value = silu(content_ref[p : p + 1, at].astype(jnp.float32))
            strength = 1.0 / (1.0 + jnp.exp(-jnp.full((1, 1), strength_ref[p, h], jnp.float32)))
            pair = jnp.concatenate([key, query, jnp.zeros((6, wide), jnp.float32)], axis=0)
            found = best(pair, state.astype(jnp.float32), ((1,), (1,)))
            along = jnp.sum(key * query, axis=-1, keepdims=True)
            out = found[1:2] + strength * along * (value - found[0:1])
            out = out * lax.rsqrt(jnp.mean(out * out, axis=-1, keepdims=True) + EPSILON)
            read.append(out * gain_ref[...] * silu(outgate_ref[p : p + 1, at].astype(jnp.float32)))
    rows_of = [jnp.concatenate(read[p * heads : (p + 1) * heads], axis=1) for p in range(prompts)]
    heads_read = jnp.concatenate(rows_of, axis=0).astype(jnp.bfloat16)
    terms = jnp.dot(heads_read, readout_ref[...], preferred_element_type=jnp.float32)
    for k in range(sent_ref.shape[0]):
        sent_ref[k] = terms.astype(jnp.bfloat16)


SMEM = pl.BlockSpec(memory_space=pltpu.SMEM)


def local(body, name, shapes, *operands):
    out = [jax.ShapeDtypeStruct(shape, jnp.bfloat16) for shape in shapes]
    return pl.pallas_call(
        body,
        in_specs=[SMEM] + [VMEM] * (len(operands) - 1),
        out_specs=[VMEM] * len(out),
        out_shape=out,
        interpret=INTERPRET,
        compiler_params=SMALL,
        name=name,
    )(*operands)


def per_device(
    tokens,
    address_projection,
    content_projection,
    strength_projection,
    fading_driver_projection,
    strength_offset,
    fading_speed,
    added_fading,
    probe,
    address,
    content,
    outgate,
    strength_raw,
    gain,
    readout_projection,
):
    prompts, positions, model = tokens.shape
    heads = fading_speed.shape[0]
    rows = prompts * positions
    share = model // (SIDE * SIDE)
    z, y, tp = lax.axis_index("z"), lax.axis_index("y"), lax.axis_index("tp")
    half = SIDE // 2
    my_half = y % 2

    weights = jnp.concatenate(
        [
            part[:, head * WIDTH : (head + 1) * WIDTH]
            for head in range(heads)
            for part in (address_projection, content_projection)
        ],
        axis=1,
    )
    flat = tokens.reshape(rows, model)
    columns = columns_by_owner(flat)
    line_tokens = exchange(columns, "y")
    line_weights = lax.all_gather(weights, "z", axis=0, tiled=True)

    drivers = jnp.concatenate([strength_projection, fading_driver_projection], axis=1)
    logits = jnp.dot(flat, drivers, preferred_element_type=jnp.float32).astype(jnp.bfloat16)
    logits = logits.astype(jnp.float32).reshape(prompts, positions, 2, -1)
    mine = lax.dynamic_slice_in_dim(logits, tp * heads, heads, 3)
    beta = jax.nn.sigmoid(mine[:, :, 0] + strength_offset)
    fading = added_fading - fading_speed * jax.nn.softplus(mine[:, :, 1])
    gates = jnp.stack([*two_parts(beta), *two_parts(fading)])
    gates = jnp.pad(
        gates.transpose(1, 3, 0, 2), ((0, 0), (0, 0), (0, 12), (0, 2 * WIDTH - positions))
    )

    gates = jnp.broadcast_to(gates[:, :, None], (prompts, heads, 2, *gates.shape[2:]))
    sent = partial_projections(
        line_tokens,
        line_weights,
        gates.reshape(prompts * heads, *gates.shape[2:]),
        positions,
    )
    got = exchange(sent.reshape(SIDE, *sent.shape[2:]), "y")

    side = my_half.astype(jnp.int32).reshape(1)
    size = (half * (WIDTH + WIDTH // 2), WIDTH)
    given, kept = local(ranges_body, "ranges", [size, size], side, got)
    other = lax.ppermute(given, "y", [(i, i ^ 1) for i in range(SIDE)])
    (line,) = local(line_body, "line", [(SIDE, WIDTH + WIDTH // 2, WIDTH)], side, kept, other)
    lines = exchange(line, "z")
    place = jnp.stack([z, my_half]).astype(jnp.int32)
    (home,) = local(scan_body, "scan", [(SIDE, WIDTH, WIDTH)], place, lines, kept, other)

    back = exchange(home, "y")
    (terms,) = local(
        read_body,
        "read",
        [(lax.axis_size("tp"), prompts, readout_projection.shape[1])],
        strength_raw,
        back,
        probe,
        address,
        content,
        outgate,
        gain.reshape(1, WIDTH),
        readout_projection,
    )
    mixed = exchange(terms, "tp").astype(jnp.float32).sum(axis=0)
    states = back.reshape(prompts, heads, 2, 2, WIDTH // 2, WIDTH).transpose(3, 0, 1, 5, 2, 4)
    boundary, state_cache = states.reshape(2, prompts, heads, WIDTH, WIDTH)
    return state_cache, mixed.astype(jnp.bfloat16), boundary[:, None]


def solution(mesh):
    finer = Mesh(mesh.devices.reshape(SIDE, SIDE, mesh.shape["tp"]), (*SP, "tp"))
    return jax.shard_map(
        per_device,
        mesh=finer,
        in_specs=(
            P(None, SP, None),
            P(SP, "tp"),
            P(SP, "tp"),
            P(),
            P(),
            P("tp"),
            P("tp"),
            P(None, SP, "tp"),
            P(None, "tp"),
            P(None, "tp"),
            P(None, "tp"),
            P(None, "tp"),
            P(None, "tp"),
            P(),
            P("tp", SP),
        ),
        out_specs=(P(None, "tp", None, None), P(None, SP), P(None, SP, "tp", None, None)),
        check_vma=False,
    )
```

time: 149 us -> 144 us (0.966)
  Pallas kernels: 3.57 us -> 13 us
  matrix products: 8.02 us -> 0.44 us
  waiting for transfers between devices: 60.7 us -> 55.6 us
  other arithmetic: 3.15 us -> 0.8 us
  starting transfers between devices: 39.8 us -> 41.7 us
    pallas_call x0 -> x4, Pallas kernels: none -> 9.38 us  [local(): pl.pallas_call(body, in_specs=[SMEM] + [VMEM] * (len(operands) - 1), out_...]
    dot_general x29 -> x0, matrix products: 7.57 us -> none  [the longest x9 1.79 us: applied(): jnp.matmul(maps[..., :WIDTH], state, precision=BEST) + maps[..., WIDTH:]]
    all_to_all x5, waiting for transfers between devices: 57.7 us -> 51.1 us  [exchange(): lax.all_to_all(messages, axis, split_axis=0, concat_axis=0, tiled=True)]
    broadcast_in_dim x6 -> x1, local copies, waits for them, and re-layouts: 2.22 us -> 0.01 us  [per_device(): jnp.broadcast_to(gates[:, :, None], (prompts, heads, 2, *gates.shape[2:]))]
    all_to_all x5, starting transfers between devices: 37.8 us -> 39.8 us  [exchange(): lax.all_to_all(messages, axis, split_axis=0, concat_axis=0, tiled=True)]
    unnamed x34 -> x36, local copies, waits for them, and re-layouts: 1.33 us -> 2.97 us
    ppermute x1, waiting for transfers between devices: 2.99 us -> 4.49 us  [per_device(): other = lax.ppermute(given, 'y', [(i, i ^ 1) for i in range(SIDE)])]
  transfers between devices with their start and end apart: 6 -> 6, of which waited for: 5 -> 5; matrix products, arithmetic and copies ran while one was open for 1% -> 2% of each run, Pallas kernels for 0% -> 0%
where the time goes in v3:
time: 144 us; the launch traced here: 143 us
  waiting for transfers between devices  55.6 us (39%)
  starting transfers between devices  41.7 us (29%)
  blocking collectives  27.2 us (19%)
  Pallas kernels  13 us (9%)
  local copies, waits for them, and re-layouts  3.15 us (2%)
    all_to_all x5, waiting for transfers between devices, exchange(): lax.all_to_all(messages, axis, split_axis=0, concat_axis=0, tiled=True)  51.1 us
    all_to_all x5, starting transfers between devices, exchange(): lax.all_to_all(messages, axis, split_axis=0, concat_axis=0, tiled=True)  39.8 us
    all_gather x1, blocking collectives, per_device(): line_weights = lax.all_gather(weights, 'z', axis=0, tiled=True)  27.2 us
    pallas_call x4, Pallas kernels, local(): pl.pallas_call(body, in_specs=[SMEM] + [VMEM] * (len(operands) - 1), out_...  9.38 us
    ppermute x1, waiting for transfers between devices, per_device(): other = lax.ppermute(given, 'y', [(i, i ^ 1) for i in range(SIDE)])  4.49 us
    unnamed x36, local copies, waits for them, and re-layouts  2.97 us
  transfers between devices with their start and end apart: 6, of which 5 were waited for; matrix products, arithmetic and copies ran while one was open for 2% of the time, Pallas kernels for 0%

profile of v3, /device:TPU:1, one launch (start us, length us, event | category | flops | bytes accessed | tf_op | source)
XLA Modules:
  0.0 142.9 jit_solution(2598214203896903081)
XLA Ops:
  0.6 1.2 copy-done
  1.9 1.9 %columns.1 = bf16[8,128,512]{2,1,0:T(8,128)(2,1)} custom-call(bf16[128,4096]{1,0:T(8,128)(2,1)S(1)} %bitcast.41), custom_call_target="tpu_custom_call" | custom-call | tf_op jit(solution)/shard_map/columns/pallas_call | solution.py:32
  3.7 7.8 %all-to-all-start = ((bf16[8,128,512]{2,1,0:T(8,128)(2,1)}), bf16[8,128,512]{2,1,0:T(8,128)(2,1)S(1)}, u32[]{:S(2)}, u32[]{:S(2)}) async-start(bf16[8,128,512]{2,1,0:T(8,128)(2,1)} %columns.1), calls=%async_computation | async-start | bytes 2097152 | tf_op jit(solution)/shard_map/all_to_all | solution.py:19
  11.5 0.0 copy-start.15
  11.5 0.0 copy-start.14
  11.6 0.4 fusion.1
  12.0 0.1 reshape.81
  12.2 0.0 copy-done.13
  12.2 0.1 fusion.15
  12.3 0.1 reduce-precision_convert_fusion.1
  12.5 27.2 %all_gather.3.weights_ref = bf16[512,512]{1,0:T(8,128)(2,1)S(1)} all-gather(bf16[64,512]{1,0:T(8,128)(2,1)S(1)} %pad_maximum_fusion), channel_id=1, replica_groups=mesh['z'=8,'y'=8,'tp'=8] {'z'}, dimensions={0}, use_global_device_ids=true | all-gather | bytes 589824 | tf_op jit(solution)/shard_map/all_gather | solution.py:306
  39.7 1.7 %partials.1 = bf16[4,2,272,256]{3,2,1,0:T(8,128)(2,1)} custom-call(bf16[8,128,512]{2,1,0:T(8,128)(2,1)S(1)} %all-to-all-done.tokens_ref, bf16[512,512]{1,0:T(8,128)(2,1)S(1)} %all_gather.3.weights_ref, bf16[4,2,16,256]{3,2,1,0:T(8,128)(2,1)S(1)} %broadcast_in_dim.5.gates_ref), custom_call_target="tpu_custom_call" | custom-call | tf_op jit(solution)/shard_map/partials/pallas_call | solution.py:69
  41.5 6.3 %all-to-all-start.1 = ((bf16[8,272,256]{2,1,0:T(8,128)(2,1)}), bf16[8,272,256]{2,1,0:T(8,128)(2,1)S(1)}, u32[]{:S(2)}, u32[]{:S(2)}) async-start(bf16[8,272,256]{2,1,0:T(8,128)(2,1)} %bitcast.10), calls=%async_computation.1 | async-start | bytes 2228224 | tf_op jit(solution)/shard_map/all_to_all | solution.py:19
  47.8 26.4 %all-to-all-done.1.got_ref = bf16[8,272,256]{2,1,0:T(8,128)(2,1)S(1)} async-done(((bf16[8,272,256]{2,1,0:T(8,128)(2,1)}), bf16[8,272,256]{2,1,0:T(8,128)(2,1)S(1)}, u32[]{:S(2)}, u32[]{:S(2)}) %all-to-all-start.1) | async-done | bytes 1114144 | tf_op jit(solution)/shard_map/all_to_all | solution.py:19
  74.2 4.1 %ranges.1 = (bf16[768,128]{1,0:T(8,128)(2,1)S(1)}, bf16[768,128]{1,0:T(8,128)(2,1)S(1)}) custom-call(s32[1]{0:T(128)} %bitcast.1.half_ref, bf16[8,272,256]{2,1,0:T(8,128)(2,1)S(1)} %all-to-all-done.1.got_ref), custom_call_target="tpu_custom_call" | custom-call | tf_op jit(solution)/shard_map/ranges/pallas_call | solution.py:259
  78.4 1.9 %collective-permute-start = (bf16[768,128]{1,0:T(8,128)(2,1)S(1)}, bf16[768,128]{1,0:T(8,128)(2,1)S(1)}, u32[]{:S(2)}, u32[]{:S(2)}) collective-permute-start(bf16[768,128]{1,0:T(8,128)(2,1)S(1)} %get-tuple-element.6), channel_id=1, source_target_pairs={{0,8},{8,0},{16,24},{24,16},{32,40},{40,32},{48,56},{56,48},{1,9},... | collective-permute-start | bytes 589832 | tf_op jit(solution)/shard_map/ppermute | solution.py:331
  80.3 4.5 %collective-permute-done.other_ref = bf16[768,128]{1,0:T(8,128)(2,1)S(1)} collective-permute-done((bf16[768,128]{1,0:T(8,128)(2,1)S(1)}, bf16[768,128]{1,0:T(8,128)(2,1)S(1)}, u32[]{:S(2)}, u32[]{:S(2)}) %collective-permute-start) | collective-permute-done | bytes 196640 | tf_op jit(solution)/shard_map/ppermute | solution.py:331
  84.8 0.9 line.1
  85.7 14.0 %all-to-all-start.2 = ((bf16[8,192,128]{2,1,0:T(8,128)(2,1)}), bf16[8,192,128]{2,1,0:T(8,128)(2,1)S(1)}, u32[]{:S(2)}, u32[]{:S(2)}) async-start(bf16[8,192,128]{2,1,0:T(8,128)(2,1)} %line.1), calls=%async_computation.2 | async-start | bytes 786432 | tf_op jit(solution)/shard_map/all_to_all | solution.py:19
  99.7 0.0 copy-start.4
  99.7 0.1 pad_add_fusion.place_ref
  99.8 12.6 %all-to-all-done.2.lines_ref = bf16[8,192,128]{2,1,0:T(8,128)(2,1)S(1)} async-done(((bf16[8,192,128]{2,1,0:T(8,128)(2,1)}), bf16[8,192,128]{2,1,0:T(8,128)(2,1)S(1)}, u32[]{:S(2)}, u32[]{:S(2)}) %all-to-all-start.2) | async-done | bytes 393248 | tf_op jit(solution)/shard_map/all_to_all | solution.py:19
  112.4 2.4 %scan.1 = bf16[8,128,128]{2,1,0:T(8,128)(2,1)} custom-call(s32[2]{0:T(128)S(1)} %pad_add_fusion.place_ref, bf16[8,192,128]{2,1,0:T(8,128)(2,1)S(1)} %all-to-all-done.2.lines_ref, bf16[768,128]{1,0:T(8,128)(2,1)S(1)} %get-tuple-element.5.kept_ref, bf16[768,128]{1,0:T(8,128)(2,1)S(1)} %collective-permute-done.other_ref), custom_call_target="tpu_custom_call" | custom-call | tf_op jit(solution)/shard_map/scan/pallas_call | solution.py:259
  114.7 3.4 %all-to-all-start.3 = ((bf16[8,128,128]{2,1,0:T(8,128)(2,1)}), bf16[8,128,128]{2,1,0:T(8,128)(2,1)S(1)}, u32[]{:S(2)}, u32[]{:S(2)}) async-start(bf16[8,128,128]{2,1,0:T(8,128)(2,1)} %scan.1), calls=%async_computation.3 | async-start | bytes 524288 | tf_op jit(solution)/shard_map/all_to_all | solution.py:19
  118.2 0.1 copy.26.readout_ref
  118.3 9.2 %all-to-all-done.3.back_ref = bf16[8,128,128]{2,1,0:T(8,128)(2,1)S(1)} async-done(((bf16[8,128,128]{2,1,0:T(8,128)(2,1)}), bf16[8,128,128]{2,1,0:T(8,128)(2,1)S(1)}, u32[]{:S(2)}, u32[]{:S(2)}) %all-to-all-start.3) | async-done | bytes 262176 | tf_op jit(solution)/shard_map/all_to_all | solution.py:19
  127.5 1.9 %read.1 = bf16[8,2,64]{2,1,0:T(2,128)(2,1)} custom-call(f32[2,2]{1,0:T(2,128)S(1)} %copy-done.2, bf16[8,128,128]{2,1,0:T(8,128)(2,1)S(1)} %all-to-all-done.3.back_ref, bf16[2,256]{1,0:T(2,128)(2,1)S(1)} %copy-done.3, bf16[2,256]{1,0:T(2,128)(2,1)S(1)} %copy-done.4, bf16[2,256]{1,0:T(2,128)(2,1)S(1)} %copy-done.5, bf16[2,256]{1,0:T(2,128)(2,1)S(1)} %copy-done.6, ...), custom_call_target="tpu_custom_call" | custom-call | tf_op jit(solution)/shard_map/read/pallas_call | solution.py:259
  129.5 8.4 %all-to-all-start.4 = ((bf16[8,2,64]{2,1,0:T(2,128)(2,1)}), bf16[8,2,64]{2,1,0:T(2,128)(2,1)S(1)}, u32[]{:S(2)}, u32[]{:S(2)}) async-start(bf16[8,2,64]{2,1,0:T(2,128)(2,1)} %read.1), calls=%async_computation.4 | async-start | bytes 8192 | tf_op jit(solution)/shard_map/all_to_all | solution.py:19
  137.8 0.8 copy.27
  138.6 0.8 copy.28
  139.4 3.0 %all-to-all-done.4 = bf16[8,2,64]{2,1,0:T(2,128)(2,1)S(1)} async-done(((bf16[8,2,64]{2,1,0:T(2,128)(2,1)}), bf16[8,2,64]{2,1,0:T(2,128)(2,1)S(1)}, u32[]{:S(2)}, u32[]{:S(2)}) %all-to-all-start.4) | async-done | bytes 2080 | tf_op jit(solution)/shard_map/all_to_all | solution.py:19
  142.4 0.5 reduce_sum.12
  (39 shorter events, 0.2 us)
Async XLA Ops:
  0.6 1.2 copy-start
  3.7 7.8 %copy-start.1 = (bf16[2,64,4096]{2,1,0:T(8,128)(2,1)S(1)}, bf16[2,64,4096]{2,1,0:T(8,128)(2,1)}, u32[]{:S(2)}) copy-start(bf16[2,64,4096]{2,1,0:T(8,128)(2,1)} %param.15) | copy-start | bytes 3145732
  3.7 7.8 %copy-start.8 = (bf16[4096,16]{0,1:T(8,128)(2,1)S(1)}, bf16[4096,16]{0,1:T(8,128)(2,1)}, u32[]{:S(2)}) copy-start(bf16[4096,16]{0,1:T(8,128)(2,1)} %param.19) | copy-start | bytes 393220
  3.7 7.9 %copy-start.9 = (bf16[4096,16]{0,1:T(8,128)(2,1)S(1)}, bf16[4096,16]{0,1:T(8,128)(2,1)}, u32[]{:S(2)}) copy-start(bf16[4096,16]{0,1:T(8,128)(2,1)} %param.18) | copy-start | bytes 393220
  3.7 36.0 %all-to-all-start = ((bf16[8,128,512]{2,1,0:T(8,128)(2,1)}), bf16[8,128,512]{2,1,0:T(8,128)(2,1)S(1)}, u32[]{:S(2)}, u32[]{:S(2)}) async-start(bf16[8,128,512]{2,1,0:T(8,128)(2,1)} %columns.1), calls=%async_computation | async-start | bytes 2097152 | tf_op jit(solution)/shard_map/all_to_all | solution.py:19
  11.5 0.7 copy-start.13
  11.5 0.7 copy-start.15
  11.5 0.7 copy-start.14
  11.5 0.9 copy-start.11
  11.5 0.9 copy-start.12
  41.5 32.7 %all-to-all-start.1 = ((bf16[8,272,256]{2,1,0:T(8,128)(2,1)}), bf16[8,272,256]{2,1,0:T(8,128)(2,1)S(1)}, u32[]{:S(2)}, u32[]{:S(2)}) async-start(bf16[8,272,256]{2,1,0:T(8,128)(2,1)} %bitcast.10), calls=%async_computation.1 | async-start | bytes 2228224 | tf_op jit(solution)/shard_map/all_to_all | solution.py:19
  78.4 6.4 %collective-permute-start = (bf16[768,128]{1,0:T(8,128)(2,1)S(1)}, bf16[768,128]{1,0:T(8,128)(2,1)S(1)}, u32[]{:S(2)}, u32[]{:S(2)}) collective-permute-start(bf16[768,128]{1,0:T(8,128)(2,1)S(1)} %get-tuple-element.6), channel_id=1, source_target_pairs={{0,8},{8,0},{16,24},{24,16},{32,40},{40,32},{48,56},{56,48},{1,9},... | collective-permute-start | bytes 589832 | tf_op jit(solution)/shard_map/ppermute | solution.py:331
  85.7 32.4 %copy-start.10 = (bf16[256,64]{0,1:T(8,128)(2,1)S(1)}, bf16[256,64]{0,1:T(8,128)(2,1)}, u32[]{:S(2)}) copy-start(bf16[256,64]{0,1:T(8,128)(2,1)} %param.29) | copy-start | bytes 98308
  85.7 26.7 %all-to-all-start.2 = ((bf16[8,192,128]{2,1,0:T(8,128)(2,1)}), bf16[8,192,128]{2,1,0:T(8,128)(2,1)S(1)}, u32[]{:S(2)}, u32[]{:S(2)}) async-start(bf16[8,192,128]{2,1,0:T(8,128)(2,1)} %line.1), calls=%async_computation.2 | async-start | bytes 786432 | tf_op jit(solution)/shard_map/all_to_all | solution.py:19
  99.7 27.8 %copy-start.2 = (f32[2,2]{1,0:T(2,128)S(1)}, f32[2,2]{1,0:T(2,128)}, u32[]{:S(2)}) copy-start(f32[2,2]{1,0:T(2,128)} %strength_ref.1) | copy-start | bytes 52
  99.7 27.8 %copy-start.3 = (bf16[2,256]{1,0:T(2,128)(2,1)S(1)}, bf16[2,256]{1,0:T(2,128)(2,1)}, u32[]{:S(2)}) copy-start(bf16[2,256]{1,0:T(2,128)(2,1)} %probe_ref.1) | copy-start | bytes 3076
  99.7 27.8 %copy-start.4 = (bf16[2,256]{1,0:T(2,128)(2,1)S(1)}, bf16[2,256]{1,0:T(2,128)(2,1)}, u32[]{:S(2)}) copy-start(bf16[2,256]{1,0:T(2,128)(2,1)} %address_ref.1) | copy-start | bytes 3076
  99.7 27.8 %copy-start.5 = (bf16[2,256]{1,0:T(2,128)(2,1)S(1)}, bf16[2,256]{1,0:T(2,128)(2,1)}, u32[]{:S(2)}) copy-start(bf16[2,256]{1,0:T(2,128)(2,1)} %content_ref.1) | copy-start | bytes 3076
  99.7 27.8 %copy-start.6 = (bf16[2,256]{1,0:T(2,128)(2,1)S(1)}, bf16[2,256]{1,0:T(2,128)(2,1)}, u32[]{:S(2)}) copy-start(bf16[2,256]{1,0:T(2,128)(2,1)} %outgate_ref.1) | copy-start | bytes 3076
  99.7 27.8 %copy-start.7 = (f32[128]{0:T(128)S(1)}, f32[128]{0:T(128)}, u32[]{:S(2)}) copy-start(f32[128]{0:T(128)} %param.28) | copy-start | bytes 1540
  114.7 12.7 %all-to-all-start.3 = ((bf16[8,128,128]{2,1,0:T(8,128)(2,1)}), bf16[8,128,128]{2,1,0:T(8,128)(2,1)S(1)}, u32[]{:S(2)}, u32[]{:S(2)}) async-start(bf16[8,128,128]{2,1,0:T(8,128)(2,1)} %scan.1), calls=%async_computation.3 | async-start | bytes 524288 | tf_op jit(solution)/shard_map/all_to_all | solution.py:19
  129.5 12.9 %all-to-all-start.4 = ((bf16[8,2,64]{2,1,0:T(2,128)(2,1)}), bf16[8,2,64]{2,1,0:T(2,128)(2,1)S(1)}, u32[]{:S(2)}, u32[]{:S(2)}) async-start(bf16[8,2,64]{2,1,0:T(2,128)(2,1)} %read.1), calls=%async_computation.4 | async-start | bytes 8192 | tf_op jit(solution)/shard_map/all_to_all | solution.py:19

commit v4 on v3

--- a/solution.py
+++ b/solution.py
@@ -12,6 +12,7 @@
 BEST = lax.Precision.HIGHEST
 SP = ("z", "y")
 INTERPRET = False
+VMEM = pl.BlockSpec(memory_space=pltpu.VMEM)
 SMALL = pltpu.CompilerParams(vmem_limit_bytes=16 * 1024 * 1024)
 
 
@@ -19,29 +20,41 @@
     return lax.all_to_all(messages, axis, split_axis=0, concat_axis=0, tiled=True)
 
 
-def columns_body(tokens_ref, columns_ref):
-    share = tokens_ref.shape[1] // (SIDE * SIDE)
-    for to in range(SIDE):
-        at = [(k * SIDE + to) * share for k in range(SIDE)]
-        columns_ref[to] = jnp.concatenate([tokens_ref[:, a : a + share] for a in at], axis=1)
-
-
-def columns_by_owner(flat):
+def columns_body(tokens_ref, columns_ref, buffer_ref, arrived):
+    parts, step, model = buffer_ref.shape
+    share = model // (SIDE * SIDE)
+    reads = [
+        pltpu.make_async_copy(
+            tokens_ref.at[i * step : (i + 1) * step, :], buffer_ref.at[i], arrived.at[i]
+        )
+        for i in range(parts)
+    ]
+    for read in reads:
+        read.start()
+    for i in range(parts):
+        reads[i].wait()
+        rows = buffer_ref[i]
+        for to in range(SIDE):
+            at = [(k * SIDE + to) * share for k in range(SIDE)]
+            columns_ref[to, i * step : (i + 1) * step, :] = jnp.concatenate(
+                [rows[:, a : a + share] for a in at], axis=1
+            )
+
+
+def columns_by_owner(flat, parts=4):
     rows, model = flat.shape
-    step = rows // 4
     return pl.pallas_call(
         columns_body,
-        grid=(rows // step,),
-        in_specs=[pl.BlockSpec((step, model), lambda i: (i, 0))],
-        out_specs=pl.BlockSpec((SIDE, step, model // SIDE), lambda i: (0, i, 0)),
+        in_specs=[pl.BlockSpec(memory_space=pltpu.MemorySpace.HBM)],
+        out_specs=VMEM,
         out_shape=jax.ShapeDtypeStruct((SIDE, rows, model // SIDE), flat.dtype),
+        scratch_shapes=[
+            pltpu.VMEM((parts, rows // parts, model), flat.dtype),
+            pltpu.SemaphoreType.DMA((parts,)),
+        ],
         interpret=INTERPRET,
-        compiler_params=SMALL,
         name="columns",
     )(flat)
-
-
-VMEM = pl.BlockSpec(memory_space=pltpu.VMEM)
 
 
 def partial_body(tokens_ref, weights_ref, gates_ref, sent_ref):
@@ -88,14 +101,26 @@
     )
 
 
+def parts(x):
+    high = x.astype(jnp.bfloat16)
+    return high, (x - high.astype(jnp.float32)).astype(jnp.bfloat16)
+
+
 def times(state, matrix):
-    high = state.astype(jnp.bfloat16)
-    low = (state - high.astype(jnp.float32)).astype(jnp.bfloat16)
     rows = state.shape[0]
     both = jnp.dot(
-        jnp.concatenate([high, low], axis=0), matrix, preferred_element_type=jnp.float32
+        jnp.concatenate(parts(state), axis=0), matrix, preferred_element_type=jnp.float32
     )
     return both[:rows] + both[rows:]
+
+
+def near(left, right, dims=((1,), (0,))):
+    (a, b), (c, d) = parts(left), parts(right)
+
+    def dot(u, v):
+        return lax.dot_general(u, v, (dims, ((), ())), preferred_element_type=jnp.float32)
+
+    return dot(a, c) + (dot(a, d) + dot(b, c))
 
 
 def silu(x):
@@ -155,12 +180,12 @@
         reached *= 2
     so_far = None
     for j in range(ranges):
-        moved = best(solved[j], tails[j], ((0,), (0,)))
+        moved = near(solved[j], tails[j], ((0,), (0,)))
         step = lasts[j] * unit - moved[:wide]
         if so_far is None:
             so_far = jnp.concatenate([step, moved[wide:]], axis=0)
         else:
-            both = best(so_far, step)
+            both = near(so_far, step)
             so_far = jnp.concatenate([both[:wide], both[wide:] + moved[wide:]], axis=0)
         out = so_far.astype(jnp.bfloat16)
         low, high = out[wide : wide + positions], out[wide + positions :]
@@ -228,23 +253,37 @@
     rows = wide // 2
     prompts, width = probe_ref.shape
     heads = width // wide
-    read = []
-    for p in range(prompts):
-        for h in range(heads):
-            at, n = slice(h * wide, (h + 1) * wide), 2 * (p * heads + h)
-            state = jnp.concatenate([back_ref[n, rows:, :], back_ref[n + 1, rows:, :]], axis=0)
-            query = silu(probe_ref[p : p + 1, at].astype(jnp.float32))
-            key = silu(address_ref[p : p + 1, at].astype(jnp.float32))
-            key = key * lax.rsqrt(jnp.sum(key * key, axis=-1, keepdims=True) + EPSILON)
-            value = silu(content_ref[p : p + 1, at].astype(jnp.float32))
-            strength = 1.0 / (1.0 + jnp.exp(-jnp.full((1, 1), strength_ref[p, h], jnp.float32)))
-            pair = jnp.concatenate([key, query, jnp.zeros((6, wide), jnp.float32)], axis=0)
-            found = best(pair, state.astype(jnp.float32), ((1,), (1,)))
-            along = jnp.sum(key * query, axis=-1, keepdims=True)
-            out = found[1:2] + strength * along * (value - found[0:1])
-            out = out * lax.rsqrt(jnp.mean(out * out, axis=-1, keepdims=True) + EPSILON)
-            read.append(out * gain_ref[...] * silu(outgate_ref[p : p + 1, at].astype(jnp.float32)))
-    rows_of = [jnp.concatenate(read[p * heads : (p + 1) * heads], axis=1) for p in range(prompts)]
+    each = [(p, h) for p in range(prompts) for h in range(heads)]
+
+    def gathered(ref):
+        wanted = [ref[p : p + 1, h * wide : (h + 1) * wide] for p, h in each]
+        return jnp.concatenate(wanted, axis=0).astype(jnp.float32)
+
+    query = silu(gathered(probe_ref))
+    key = silu(gathered(address_ref))
+    key = key * lax.rsqrt(jnp.sum(key * key, axis=-1, keepdims=True) + EPSILON)
+    value = silu(gathered(content_ref))
+    strength = jnp.concatenate(
+        [jnp.full((1, 1), strength_ref[p, h], jnp.float32) for p, h in each], axis=0
+    )
+    strength = 1.0 / (1.0 + jnp.exp(-strength))
+    pair = jnp.concatenate([key, query], axis=0)
+    recalled, probed = [], []
+    for n in range(len(each)):
+        state = jnp.concatenate([back_ref[2 * n, rows:, :], back_ref[2 * n + 1, rows:, :]], axis=0)
+        found = best(pair, state.astype(jnp.float32), ((1,), (1,)))
+        recalled.append(found[n : n + 1])
+        probed.append(found[len(each) + n : len(each) + n + 1])
+    along = jnp.sum(key * query, axis=-1, keepdims=True)
+    out = jnp.concatenate(probed, axis=0) + strength * along * (
+        value - jnp.concatenate(recalled, axis=0)
+    )
+    out = out * lax.rsqrt(jnp.mean(out * out, axis=-1, keepdims=True) + EPSILON)
+    read = out * gain_ref[...] * silu(gathered(outgate_ref))
+    rows_of = [
+        jnp.concatenate([read[p * heads + h :][:1] for h in range(heads)], axis=1)
+        for p in range(prompts)
+    ]
     heads_read = jnp.concatenate(rows_of, axis=0).astype(jnp.bfloat16)
     terms = jnp.dot(heads_read, readout_ref[...], preferred_element_type=jnp.float32)
     for k in range(sent_ref.shape[0]):
@@ -313,7 +352,7 @@
     fading = added_fading - fading_speed * jax.nn.softplus(mine[:, :, 1])
     gates = jnp.stack([*two_parts(beta), *two_parts(fading)])
     gates = jnp.pad(
-        gates.transpose(1, 3, 0, 2), ((0, 0), (0, 0), (0, 12), (0, 2 * WIDTH - positions))
+        gates.transpose(1, 3, 0, 2), ((0, 0), (0, 0), (0, 4), (0, 2 * WIDTH - positions))
     )
 
     gates = jnp.broadcast_to(gates[:, :, None], (prompts, heads, 2, *gates.shape[2:]))

time: 144 us -> 142 us (0.986)
    unnamed x36 -> x34, local copies, waits for them, and re-layouts: 2.97 us -> 1.75 us
where the time goes in v4:
time: 142 us; the launch traced here: 141 us
  waiting for transfers between devices  55.1 us (39%)
  starting transfers between devices  41.7 us (29%)
  blocking collectives  27.2 us (19%)
  Pallas kernels  13.1 us (9%)
  local copies, waits for them, and re-layouts  1.93 us (1%)
    all_to_all x5, waiting for transfers between devices, exchange(): lax.all_to_all(messages, axis, split_axis=0, concat_axis=0, tiled=True)  50.6 us
    all_to_all x5, starting transfers between devices, exchange(): lax.all_to_all(messages, axis, split_axis=0, concat_axis=0, tiled=True)  39.7 us
    all_gather x1, blocking collectives, per_device(): line_weights = lax.all_gather(weights, 'z', axis=0, tiled=True)  27.2 us
    pallas_call x4, Pallas kernels, local(): pl.pallas_call(body, in_specs=[SMEM] + [VMEM] * (len(operands) - 1), out_...  8.87 us
    ppermute x1, waiting for transfers between devices, per_device(): other = lax.ppermute(given, 'y', [(i, i ^ 1) for i in range(SIDE)])  4.49 us
  transfers between devices with their start and end apart: 6, of which 5 were waited for; matrix products, arithmetic and copies ran while one was open for 2% of the time, Pallas kernels for 0%

profile of v4, /device:TPU:1, one launch (start us, length us, event | category | flops | bytes accessed | tf_op | source)
XLA Modules:
  0.0 141.2 jit_solution(611887070420256680)
XLA Ops:
  0.6 2.5 %columns.1 = bf16[8,128,512]{2,1,0:T(8,128)(2,1)} custom-call(bf16[128,4096]{1,0:T(8,128)(2,1)} %bitcast.43), custom_call_target="tpu_custom_call" | custom-call | tf_op jit(solution)/shard_map/columns/pallas_call | solution.py:46
  3.2 0.0 copy-start.6
  3.2 0.0 copy-start.7
  3.2 7.8 %all-to-all-start = ((bf16[8,128,512]{2,1,0:T(8,128)(2,1)}), bf16[8,128,512]{2,1,0:T(8,128)(2,1)S(1)}, u32[]{:S(2)}, u32[]{:S(2)}) async-start(bf16[8,128,512]{2,1,0:T(8,128)(2,1)} %columns.1), calls=%async_computation | async-start | bytes 2097152 | tf_op jit(solution)/shard_map/all_to_all | solution.py:20
  11.0 0.0 copy-start.10
  11.0 0.0 copy-start.11
  11.1 0.4 fusion.1
  11.5 0.1 reshape.81
  11.7 0.0 copy-done.12
  11.7 0.1 fusion.15
  11.8 0.1 reduce-precision_convert_fusion.1
  12.0 27.2 %all_gather.3.weights_ref = bf16[512,512]{1,0:T(8,128)(2,1)S(1)} all-gather(bf16[64,512]{1,0:T(8,128)(2,1)S(1)} %pad_maximum_fusion), channel_id=1, replica_groups=mesh['z'=8,'y'=8,'tp'=8] {'z'}, dimensions={0}, use_global_device_ids=true | all-gather | bytes 589824 | tf_op jit(solution)/shard_map/all_gather | solution.py:345
  39.2 1.7 %partials.1 = bf16[4,2,264,256]{3,2,1,0:T(8,128)(2,1)} custom-call(bf16[8,128,512]{2,1,0:T(8,128)(2,1)S(1)} %all-to-all-done.tokens_ref, bf16[512,512]{1,0:T(8,128)(2,1)S(1)} %all_gather.3.weights_ref, bf16[4,2,8,256]{3,2,1,0:T(8,128)(2,1)S(1)} %broadcast_in_dim.5.gates_ref), custom_call_target="tpu_custom_call" | custom-call | tf_op jit(solution)/shard_map/partials/pallas_call | solution.py:82
  40.9 6.3 %all-to-all-start.1 = ((bf16[8,264,256]{2,1,0:T(8,128)(2,1)}), bf16[8,264,256]{2,1,0:T(8,128)(2,1)S(1)}, u32[]{:S(2)}, u32[]{:S(2)}) async-start(bf16[8,264,256]{2,1,0:T(8,128)(2,1)} %bitcast.10), calls=%async_computation.1 | async-start | bytes 2162688 | tf_op jit(solution)/shard_map/all_to_all | solution.py:20
  47.3 25.8 %all-to-all-done.1.got_ref = bf16[8,264,256]{2,1,0:T(8,128)(2,1)S(1)} async-done(((bf16[8,264,256]{2,1,0:T(8,128)(2,1)}), bf16[8,264,256]{2,1,0:T(8,128)(2,1)S(1)}, u32[]{:S(2)}, u32[]{:S(2)}) %all-to-all-start.1) | async-done | bytes 1081376 | tf_op jit(solution)/shard_map/all_to_all | solution.py:20
  73.1 3.6 %ranges.1 = (bf16[768,128]{1,0:T(8,128)(2,1)S(1)}, bf16[768,128]{1,0:T(8,128)(2,1)S(1)}) custom-call(s32[1]{0:T(128)} %bitcast.1.half_ref, bf16[8,264,256]{2,1,0:T(8,128)(2,1)S(1)} %all-to-all-done.1.got_ref), custom_call_target="tpu_custom_call" | custom-call | tf_op jit(solution)/shard_map/ranges/pallas_call | solution.py:298
  76.7 1.9 %collective-permute-start = (bf16[768,128]{1,0:T(8,128)(2,1)S(1)}, bf16[768,128]{1,0:T(8,128)(2,1)S(1)}, u32[]{:S(2)}, u32[]{:S(2)}) collective-permute-start(bf16[768,128]{1,0:T(8,128)(2,1)S(1)} %get-tuple-element.6), channel_id=1, source_target_pairs={{0,8},{8,0},{16,24},{24,16},{32,40},{40,32},{48,56},{56,48},{1,9},... | collective-permute-start | bytes 589832 | tf_op jit(solution)/shard_map/ppermute | solution.py:370
  78.6 4.5 %collective-permute-done.other_ref = bf16[768,128]{1,0:T(8,128)(2,1)S(1)} collective-permute-done((bf16[768,128]{1,0:T(8,128)(2,1)S(1)}, bf16[768,128]{1,0:T(8,128)(2,1)S(1)}, u32[]{:S(2)}, u32[]{:S(2)}) %collective-permute-start) | collective-permute-done | bytes 196640 | tf_op jit(solution)/shard_map/ppermute | solution.py:370
  83.1 0.9 line.1
  84.0 13.9 %all-to-all-start.2 = ((bf16[8,192,128]{2,1,0:T(8,128)(2,1)}), bf16[8,192,128]{2,1,0:T(8,128)(2,1)S(1)}, u32[]{:S(2)}, u32[]{:S(2)}) async-start(bf16[8,192,128]{2,1,0:T(8,128)(2,1)} %line.1), calls=%async_computation.2 | async-start | bytes 786432 | tf_op jit(solution)/shard_map/all_to_all | solution.py:20
  97.9 0.1 pad_add_fusion.place_ref
  98.0 12.6 %all-to-all-done.2.lines_ref = bf16[8,192,128]{2,1,0:T(8,128)(2,1)S(1)} async-done(((bf16[8,192,128]{2,1,0:T(8,128)(2,1)}), bf16[8,192,128]{2,1,0:T(8,128)(2,1)S(1)}, u32[]{:S(2)}, u32[]{:S(2)}) %all-to-all-start.2) | async-done | bytes 393248 | tf_op jit(solution)/shard_map/all_to_all | solution.py:20
  110.6 2.4 %scan.1 = bf16[8,128,128]{2,1,0:T(8,128)(2,1)} custom-call(s32[2]{0:T(128)S(1)} %pad_add_fusion.place_ref, bf16[8,192,128]{2,1,0:T(8,128)(2,1)S(1)} %all-to-all-done.2.lines_ref, bf16[768,128]{1,0:T(8,128)(2,1)S(1)} %get-tuple-element.5.kept_ref, bf16[768,128]{1,0:T(8,128)(2,1)S(1)} %collective-permute-done.other_ref), custom_call_target="tpu_custom_call" | custom-call | tf_op jit(solution)/shard_map/scan/pallas_call | solution.py:298
  112.9 3.4 %all-to-all-start.3 = ((bf16[8,128,128]{2,1,0:T(8,128)(2,1)}), bf16[8,128,128]{2,1,0:T(8,128)(2,1)S(1)}, u32[]{:S(2)}, u32[]{:S(2)}) async-start(bf16[8,128,128]{2,1,0:T(8,128)(2,1)} %scan.1), calls=%async_computation.3 | async-start | bytes 524288 | tf_op jit(solution)/shard_map/all_to_all | solution.py:20
  116.4 0.1 copy.26.readout_ref
  116.5 9.2 %all-to-all-done.3.back_ref = bf16[8,128,128]{2,1,0:T(8,128)(2,1)S(1)} async-done(((bf16[8,128,128]{2,1,0:T(8,128)(2,1)}), bf16[8,128,128]{2,1,0:T(8,128)(2,1)S(1)}, u32[]{:S(2)}, u32[]{:S(2)}) %all-to-all-start.3) | async-done | bytes 262176 | tf_op jit(solution)/shard_map/all_to_all | solution.py:20
  125.7 2.0 %read.1 = bf16[8,2,64]{2,1,0:T(2,128)(2,1)} custom-call(f32[2,2]{1,0:T(2,128)S(1)} %copy-done, bf16[8,128,128]{2,1,0:T(8,128)(2,1)S(1)} %all-to-all-done.3.back_ref, bf16[2,256]{1,0:T(2,128)(2,1)S(1)} %copy-done.1, bf16[2,256]{1,0:T(2,128)(2,1)S(1)} %copy-done.2, bf16[2,256]{1,0:T(2,128)(2,1)S(1)} %copy-done.3, bf16[2,256]{1,0:T(2,128)(2,1)S(1)} %copy-done.4, ...), custom_call_target="tpu_custom_call" | custom-call | tf_op jit(solution)/shard_map/read/pallas_call | solution.py:298
  127.7 8.4 %all-to-all-start.4 = ((bf16[8,2,64]{2,1,0:T(2,128)(2,1)}), bf16[8,2,64]{2,1,0:T(2,128)(2,1)S(1)}, u32[]{:S(2)}, u32[]{:S(2)}) async-start(bf16[8,2,64]{2,1,0:T(2,128)(2,1)} %read.1), calls=%async_computation.4 | async-start | bytes 8192 | tf_op jit(solution)/shard_map/all_to_all | solution.py:20
  136.1 0.8 copy.27
  136.8 0.8 copy.28
  137.6 3.0 %all-to-all-done.4 = bf16[8,2,64]{2,1,0:T(2,128)(2,1)S(1)} async-done(((bf16[8,2,64]{2,1,0:T(2,128)(2,1)}), bf16[8,2,64]{2,1,0:T(2,128)(2,1)S(1)}, u32[]{:S(2)}, u32[]{:S(2)}) %all-to-all-start.4) | async-done | bytes 2080 | tf_op jit(solution)/shard_map/all_to_all | solution.py:20
  140.6 0.5 reduce_sum.12
  (37 shorter events, 0.2 us)
Async XLA Ops:
  3.2 7.9 %copy-start.6 = (bf16[2,64,4096]{2,1,0:T(8,128)(2,1)S(1)}, bf16[2,64,4096]{2,1,0:T(8,128)(2,1)}, u32[]{:S(2)}) copy-start(bf16[2,64,4096]{2,1,0:T(8,128)(2,1)} %param.15) | copy-start | bytes 3145732
  3.2 7.9 %copy-start.7 = (bf16[4096,16]{0,1:T(8,128)(2,1)S(1)}, bf16[4096,16]{0,1:T(8,128)(2,1)}, u32[]{:S(2)}) copy-start(bf16[4096,16]{0,1:T(8,128)(2,1)} %param.19) | copy-start | bytes 393220
  3.2 7.9 %copy-start.8 = (bf16[4096,16]{0,1:T(8,128)(2,1)S(1)}, bf16[4096,16]{0,1:T(8,128)(2,1)}, u32[]{:S(2)}) copy-start(bf16[4096,16]{0,1:T(8,128)(2,1)} %param.18) | copy-start | bytes 393220
  3.2 36.0 %all-to-all-start = ((bf16[8,128,512]{2,1,0:T(8,128)(2,1)}), bf16[8,128,512]{2,1,0:T(8,128)(2,1)S(1)}, u32[]{:S(2)}, u32[]{:S(2)}) async-start(bf16[8,128,512]{2,1,0:T(8,128)(2,1)} %columns.1), calls=%async_computation | async-start | bytes 2097152 | tf_op jit(solution)/shard_map/all_to_all | solution.py:20
  11.0 0.7 copy-start.12
  11.0 0.7 copy-start.14
  11.0 0.7 copy-start.13
  11.0 0.9 copy-start.10
  11.0 0.9 copy-start.11
  40.9 32.1 %all-to-all-start.1 = ((bf16[8,264,256]{2,1,0:T(8,128)(2,1)}), bf16[8,264,256]{2,1,0:T(8,128)(2,1)S(1)}, u32[]{:S(2)}, u32[]{:S(2)}) async-start(bf16[8,264,256]{2,1,0:T(8,128)(2,1)} %bitcast.10), calls=%async_computation.1 | async-start | bytes 2162688 | tf_op jit(solution)/shard_map/all_to_all | solution.py:20
  76.7 6.4 %collective-permute-start = (bf16[768,128]{1,0:T(8,128)(2,1)S(1)}, bf16[768,128]{1,0:T(8,128)(2,1)S(1)}, u32[]{:S(2)}, u32[]{:S(2)}) collective-permute-start(bf16[768,128]{1,0:T(8,128)(2,1)S(1)} %get-tuple-element.6), channel_id=1, source_target_pairs={{0,8},{8,0},{16,24},{24,16},{32,40},{40,32},{48,56},{56,48},{1,9},... | collective-permute-start | bytes 589832 | tf_op jit(solution)/shard_map/ppermute | solution.py:370
  84.0 32.3 %copy-start.9 = (bf16[256,64]{0,1:T(8,128)(2,1)S(1)}, bf16[256,64]{0,1:T(8,128)(2,1)}, u32[]{:S(2)}) copy-start(bf16[256,64]{0,1:T(8,128)(2,1)} %param.29) | copy-start | bytes 98308
  84.0 26.6 %all-to-all-start.2 = ((bf16[8,192,128]{2,1,0:T(8,128)(2,1)}), bf16[8,192,128]{2,1,0:T(8,128)(2,1)S(1)}, u32[]{:S(2)}, u32[]{:S(2)}) async-start(bf16[8,192,128]{2,1,0:T(8,128)(2,1)} %line.1), calls=%async_computation.2 | async-start | bytes 786432 | tf_op jit(solution)/shard_map/all_to_all | solution.py:20
  98.0 27.7 %copy-start = (f32[2,2]{1,0:T(2,128)S(1)}, f32[2,2]{1,0:T(2,128)}, u32[]{:S(2)}) copy-start(f32[2,2]{1,0:T(2,128)} %strength_ref.1) | copy-start | bytes 52
  98.0 27.7 %copy-start.1 = (bf16[2,256]{1,0:T(2,128)(2,1)S(1)}, bf16[2,256]{1,0:T(2,128)(2,1)}, u32[]{:S(2)}) copy-start(bf16[2,256]{1,0:T(2,128)(2,1)} %probe_ref.1) | copy-start | bytes 3076
  98.0 27.7 %copy-start.2 = (bf16[2,256]{1,0:T(2,128)(2,1)S(1)}, bf16[2,256]{1,0:T(2,128)(2,1)}, u32[]{:S(2)}) copy-start(bf16[2,256]{1,0:T(2,128)(2,1)} %address_ref.1) | copy-start | bytes 3076
  98.0 27.7 %copy-start.3 = (bf16[2,256]{1,0:T(2,128)(2,1)S(1)}, bf16[2,256]{1,0:T(2,128)(2,1)}, u32[]{:S(2)}) copy-start(bf16[2,256]{1,0:T(2,128)(2,1)} %content_ref.1) | copy-start | bytes 3076
  98.0 27.7 %copy-start.4 = (bf16[2,256]{1,0:T(2,128)(2,1)S(1)}, bf16[2,256]{1,0:T(2,128)(2,1)}, u32[]{:S(2)}) copy-start(bf16[2,256]{1,0:T(2,128)(2,1)} %outgate_ref.1) | copy-start | bytes 3076
  98.0 27.7 %copy-start.5 = (f32[128]{0:T(128)S(1)}, f32[128]{0:T(128)}, u32[]{:S(2)}) copy-start(f32[128]{0:T(128)} %param.28) | copy-start | bytes 1540
  112.9 12.7 %all-to-all-start.3 = ((bf16[8,128,128]{2,1,0:T(8,128)(2,1)}), bf16[8,128,128]{2,1,0:T(8,128)(2,1)S(1)}, u32[]{:S(2)}, u32[]{:S(2)}) async-start(bf16[8,128,128]{2,1,0:T(8,128)(2,1)} %scan.1), calls=%async_computation.3 | async-start | bytes 524288 | tf_op jit(solution)/shard_map/all_to_all | solution.py:20
  127.7 13.0 %all-to-all-start.4 = ((bf16[8,2,64]{2,1,0:T(2,128)(2,1)}), bf16[8,2,64]{2,1,0:T(2,128)(2,1)S(1)}, u32[]{:S(2)}, u32[]{:S(2)}) async-start(bf16[8,2,64]{2,1,0:T(2,128)(2,1)} %read.1), calls=%async_computation.4 | async-start | bytes 8192 | tf_op jit(solution)/shard_map/all_to_all | solution.py:20

commit v5 on v4

--- a/solution.py
+++ b/solution.py
@@ -10,7 +10,8 @@
 SIDE = 8
 EPSILON = 1e-06
 BEST = lax.Precision.HIGHEST
-SP = ("z", "y")
+Z = ("zh", "zl")
+SP = (*Z, "y")
 INTERPRET = False
 VMEM = pl.BlockSpec(memory_space=pltpu.VMEM)
 SMALL = pltpu.CompilerParams(vmem_limit_bytes=16 * 1024 * 1024)
@@ -327,7 +328,7 @@
     heads = fading_speed.shape[0]
     rows = prompts * positions
     share = model // (SIDE * SIDE)
-    z, y, tp = lax.axis_index("z"), lax.axis_index("y"), lax.axis_index("tp")
+    z, y, tp = lax.axis_index(Z), lax.axis_index("y"), lax.axis_index("tp")
     half = SIDE // 2
     my_half = y % 2
 
@@ -342,7 +343,10 @@
     flat = tokens.reshape(rows, model)
     columns = columns_by_owner(flat)
     line_tokens = exchange(columns, "y")
-    line_weights = lax.all_gather(weights, "z", axis=0, tiled=True)
+    beside = lax.ppermute(weights, "zl", [(0, 1), (1, 0)])
+    even = lax.axis_index("zl") == 0
+    both = [jnp.where(even, weights, beside), jnp.where(even, beside, weights)]
+    line_weights = lax.all_gather(jnp.concatenate(both), "zh", axis=0, tiled=True)
 
     drivers = jnp.concatenate([strength_projection, fading_driver_projection], axis=1)
     logits = jnp.dot(flat, drivers, preferred_element_type=jnp.float32).astype(jnp.bfloat16)
@@ -369,7 +373,7 @@
     given, kept = local(ranges_body, "ranges", [size, size], side, got)
     other = lax.ppermute(given, "y", [(i, i ^ 1) for i in range(SIDE)])
     (line,) = local(line_body, "line", [(SIDE, WIDTH + WIDTH // 2, WIDTH)], side, kept, other)
-    lines = exchange(line, "z")
+    lines = exchange(line, Z)
     place = jnp.stack([z, my_half]).astype(jnp.int32)
     (home,) = local(scan_body, "scan", [(SIDE, WIDTH, WIDTH)], place, lines, kept, other)
 
@@ -394,7 +398,7 @@
 
 
 def solution(mesh):
-    finer = Mesh(mesh.devices.reshape(SIDE, SIDE, mesh.shape["tp"]), (*SP, "tp"))
+    finer = Mesh(mesh.devices.reshape(SIDE // 2, 2, SIDE, mesh.shape["tp"]), (*SP, "tp"))
     return jax.shard_map(
         per_device,
         mesh=finer,

time: 142 us -> 146 us (1.028)
  waiting for transfers between devices: 55.1 us -> 69.1 us
  blocking collectives: 27.2 us -> 19.7 us
  starting transfers between devices: 41.7 us -> 38.3 us
    all_to_all x5, waiting for transfers between devices: 50.6 us -> 63.2 us  [exchange(): lax.all_to_all(messages, axis, split_axis=0, concat_axis=0, tiled=True)]
    all_to_all x5, starting transfers between devices: 39.7 us -> 31.6 us  [exchange(): lax.all_to_all(messages, axis, split_axis=0, concat_axis=0, tiled=True)]
    all_gather x1, blocking collectives: 27.2 us -> 19.7 us  [per_device(): lax.all_gather(jnp.concatenate(both), 'zh', axis=0, tiled=True)]
    ppermute x0 -> x1, starting transfers between devices: none -> 4.82 us  [per_device(): beside = lax.ppermute(weights, 'zl', [(0, 1), (1, 0)])]
  transfers between devices with their start and end apart: 6 -> 7, of which waited for: 5 -> 6; matrix products, arithmetic and copies ran while one was open for 2% -> 2% of each run, Pallas kernels for 0% -> 2%
where the time goes in v5:
time: 146 us; the launch traced here: 145 us
  waiting for transfers between devices  69.1 us (47%)
  starting transfers between devices  38.3 us (26%)
  blocking collectives  19.7 us (13%)
  Pallas kernels  13.1 us (9%)
  local copies, waits for them, and re-layouts  2.7 us (2%)
    all_to_all x5, waiting for transfers between devices, exchange(): lax.all_to_all(messages, axis, split_axis=0, concat_axis=0, tiled=True)  63.2 us
    all_to_all x5, starting transfers between devices, exchange(): lax.all_to_all(messages, axis, split_axis=0, concat_axis=0, tiled=True)  31.6 us
    all_gather x1, blocking collectives, per_device(): lax.all_gather(jnp.concatenate(both), 'zh', axis=0, tiled=True)  19.7 us
    pallas_call x4, Pallas kernels, local(): pl.pallas_call(body, in_specs=[SMEM] + [VMEM] * (len(operands) - 1), out_...  8.87 us
    ppermute x1, waiting for transfers between devices, per_device(): other = lax.ppermute(given, 'y', [(i, i ^ 1) for i in range(SIDE)])  5.94 us
    ppermute x1, starting transfers between devices, per_device(): beside = lax.ppermute(weights, 'zl', [(0, 1), (1, 0)])  4.82 us
  transfers between devices with their start and end apart: 7, of which 6 were waited for; matrix products, arithmetic and copies ran while one was open for 2% of the time, Pallas kernels for 2%

profile of v5, /device:TPU:1, one launch (start us, length us, event | category | flops | bytes accessed | tf_op | source)
XLA Modules:
  0.0 145.1 jit_solution(12355100499259578775)
XLA Ops:
  0.6 0.8 fusion.20
  1.4 4.8 %collective-permute-start = (bf16[64,512]{1,0:T(8,128)(2,1)S(1)}, bf16[64,512]{1,0:T(8,128)(2,1)S(1)}, u32[]{:S(2)}, u32[]{:S(2)}) collective-permute-start(bf16[64,512]{1,0:T(8,128)(2,1)S(1)} %pad_maximum_fusion.1), channel_id=1, source_target_pairs={{0,64},{64,0},{1,65},{65,1},{2,66},{66,2},{3,67},{67,3},{4,68},{68... | collective-permute-start | bytes 196616 | tf_op jit(solution)/shard_map/ppermute | solution.py:346
  6.2 2.5 %columns.1 = bf16[8,128,512]{2,1,0:T(8,128)(2,1)} custom-call(bf16[128,4096]{1,0:T(8,128)(2,1)} %bitcast.43), custom_call_target="tpu_custom_call" | custom-call | tf_op jit(solution)/shard_map/columns/pallas_call | solution.py:47
  8.8 0.0 copy-start.6
  8.8 7.0 %all-to-all-start = ((bf16[8,128,512]{2,1,0:T(8,128)(2,1)}), bf16[8,128,512]{2,1,0:T(8,128)(2,1)S(1)}, u32[]{:S(2)}, u32[]{:S(2)}) async-start(bf16[8,128,512]{2,1,0:T(8,128)(2,1)} %columns.1), calls=%async_computation | async-start | bytes 2097152 | tf_op jit(solution)/shard_map/all_to_all | solution.py:21
  15.9 0.4 fusion.1
  16.3 0.1 reshape.81
  16.4 0.0 copy-done.10
  16.5 0.1 fusion.15
  16.5 0.1 reduce-precision_convert_fusion.1
  16.8 19.7 %all_gather.3.weights_ref = bf16[512,512]{1,0:T(8,128)(2,1)S(1)} all-gather(bf16[128,512]{1,0:T(8,128)(2,1)S(1)} %pad_maximum_fusion), channel_id=1, replica_groups=mesh['zh'=4,'zl'=2,'y'=8,'tp'=8] {'zh'}, dimensions={0}, use_global_device_ids=true | all-gather | bytes 655360 | tf_op jit(solution)/shard_map/all_gather | solution.py:349
  36.4 8.5 %all-to-all-done.tokens_ref = bf16[8,128,512]{2,1,0:T(8,128)(2,1)S(1)} async-done(((bf16[8,128,512]{2,1,0:T(8,128)(2,1)}), bf16[8,128,512]{2,1,0:T(8,128)(2,1)S(1)}, u32[]{:S(2)}, u32[]{:S(2)}) %all-to-all-start) | async-done | bytes 1048608 | tf_op jit(solution)/shard_map/all_to_all | solution.py:21
  45.0 1.7 %partials.1 = bf16[4,2,264,256]{3,2,1,0:T(8,128)(2,1)} custom-call(bf16[8,128,512]{2,1,0:T(8,128)(2,1)S(1)} %all-to-all-done.tokens_ref, bf16[512,512]{1,0:T(8,128)(2,1)S(1)} %all_gather.3.weights_ref, bf16[4,2,8,256]{3,2,1,0:T(8,128)(2,1)S(1)} %broadcast_in_dim.5.gates_ref), custom_call_target="tpu_custom_call" | custom-call | tf_op jit(solution)/shard_map/partials/pallas_call | solution.py:83
  46.7 3.6 %all-to-all-start.1 = ((bf16[8,264,256]{2,1,0:T(8,128)(2,1)}), bf16[8,264,256]{2,1,0:T(8,128)(2,1)S(1)}, u32[]{:S(2)}, u32[]{:S(2)}) async-start(bf16[8,264,256]{2,1,0:T(8,128)(2,1)} %bitcast.10), calls=%async_computation.1 | async-start | bytes 2162688 | tf_op jit(solution)/shard_map/all_to_all | solution.py:21
  50.3 29.8 %all-to-all-done.1.got_ref = bf16[8,264,256]{2,1,0:T(8,128)(2,1)S(1)} async-done(((bf16[8,264,256]{2,1,0:T(8,128)(2,1)}), bf16[8,264,256]{2,1,0:T(8,128)(2,1)S(1)}, u32[]{:S(2)}, u32[]{:S(2)}) %all-to-all-start.1) | async-done | bytes 1081376 | tf_op jit(solution)/shard_map/all_to_all | solution.py:21
  80.1 3.6 %ranges.1 = (bf16[768,128]{1,0:T(8,128)(2,1)S(1)}, bf16[768,128]{1,0:T(8,128)(2,1)S(1)}) custom-call(s32[1]{0:T(128)} %bitcast.1.half_ref, bf16[8,264,256]{2,1,0:T(8,128)(2,1)S(1)} %all-to-all-done.1.got_ref), custom_call_target="tpu_custom_call" | custom-call | tf_op jit(solution)/shard_map/ranges/pallas_call | solution.py:299
  83.7 1.9 %collective-permute-start.1 = (bf16[768,128]{1,0:T(8,128)(2,1)S(1)}, bf16[768,128]{1,0:T(8,128)(2,1)S(1)}, u32[]{:S(2)}, u32[]{:S(2)}) collective-permute-start(bf16[768,128]{1,0:T(8,128)(2,1)S(1)} %get-tuple-element.6), channel_id=1, source_target_pairs={{0,8},{8,0},{16,24},{24,16},{32,40},{40,32},{48,56},{56,48},{1,9},... | collective-permute-start | bytes 589832 | tf_op jit(solution)/shard_map/ppermute | solution.py:374
  85.7 5.9 %collective-permute-done.1.other_ref = bf16[768,128]{1,0:T(8,128)(2,1)S(1)} collective-permute-done((bf16[768,128]{1,0:T(8,128)(2,1)S(1)}, bf16[768,128]{1,0:T(8,128)(2,1)S(1)}, u32[]{:S(2)}, u32[]{:S(2)}) %collective-permute-start.1) | collective-permute-done | bytes 196640 | tf_op jit(solution)/shard_map/ppermute | solution.py:374
  91.6 0.9 line.1
  92.5 9.3 %all-to-all-start.2 = ((bf16[8,192,128]{2,1,0:T(8,128)(2,1)}), bf16[8,192,128]{2,1,0:T(8,128)(2,1)S(1)}, u32[]{:S(2)}, u32[]{:S(2)}) async-start(bf16[8,192,128]{2,1,0:T(8,128)(2,1)} %line.1), calls=%async_computation.2 | async-start | bytes 786432 | tf_op jit(solution)/shard_map/all_to_all | solution.py:21
  101.8 0.1 pad_add_fusion.place_ref
  101.9 12.6 %all-to-all-done.2.lines_ref = bf16[8,192,128]{2,1,0:T(8,128)(2,1)S(1)} async-done(((bf16[8,192,128]{2,1,0:T(8,128)(2,1)}), bf16[8,192,128]{2,1,0:T(8,128)(2,1)S(1)}, u32[]{:S(2)}, u32[]{:S(2)}) %all-to-all-start.2) | async-done | bytes 393248 | tf_op jit(solution)/shard_map/all_to_all | solution.py:21
  114.5 2.4 %scan.1 = bf16[8,128,128]{2,1,0:T(8,128)(2,1)} custom-call(s32[2]{0:T(128)S(1)} %pad_add_fusion.place_ref, bf16[8,192,128]{2,1,0:T(8,128)(2,1)S(1)} %all-to-all-done.2.lines_ref, bf16[768,128]{1,0:T(8,128)(2,1)S(1)} %get-tuple-element.5.kept_ref, bf16[768,128]{1,0:T(8,128)(2,1)S(1)} %collective-permute-done.1.other_ref), custom_call_target="tpu_custom_call" | custom-call | tf_op jit(solution)/shard_map/scan/pallas_call | solution.py:299
  116.8 3.4 %all-to-all-start.3 = ((bf16[8,128,128]{2,1,0:T(8,128)(2,1)}), bf16[8,128,128]{2,1,0:T(8,128)(2,1)S(1)}, u32[]{:S(2)}, u32[]{:S(2)}) async-start(bf16[8,128,128]{2,1,0:T(8,128)(2,1)} %scan.1), calls=%async_computation.3 | async-start | bytes 524288 | tf_op jit(solution)/shard_map/all_to_all | solution.py:21
  120.3 0.1 copy.26.readout_ref
  120.4 9.2 %all-to-all-done.3.back_ref = bf16[8,128,128]{2,1,0:T(8,128)(2,1)S(1)} async-done(((bf16[8,128,128]{2,1,0:T(8,128)(2,1)}), bf16[8,128,128]{2,1,0:T(8,128)(2,1)S(1)}, u32[]{:S(2)}, u32[]{:S(2)}) %all-to-all-start.3) | async-done | bytes 262176 | tf_op jit(solution)/shard_map/all_to_all | solution.py:21
  129.6 2.0 %read.1 = bf16[8,2,64]{2,1,0:T(2,128)(2,1)} custom-call(f32[2,2]{1,0:T(2,128)S(1)} %copy-done, bf16[8,128,128]{2,1,0:T(8,128)(2,1)S(1)} %all-to-all-done.3.back_ref, bf16[2,256]{1,0:T(2,128)(2,1)S(1)} %copy-done.1, bf16[2,256]{1,0:T(2,128)(2,1)S(1)} %copy-done.2, bf16[2,256]{1,0:T(2,128)(2,1)S(1)} %copy-done.3, bf16[2,256]{1,0:T(2,128)(2,1)S(1)} %copy-done.4, ...), custom_call_target="tpu_custom_call" | custom-call | tf_op jit(solution)/shard_map/read/pallas_call | solution.py:299
  131.6 8.4 %all-to-all-start.4 = ((bf16[8,2,64]{2,1,0:T(2,128)(2,1)}), bf16[8,2,64]{2,1,0:T(2,128)(2,1)S(1)}, u32[]{:S(2)}, u32[]{:S(2)}) async-start(bf16[8,2,64]{2,1,0:T(2,128)(2,1)} %read.1), calls=%async_computation.4 | async-start | bytes 8192 | tf_op jit(solution)/shard_map/all_to_all | solution.py:21
  140.0 0.8 copy.27
  140.8 0.8 copy.28
  141.5 3.0 %all-to-all-done.4 = bf16[8,2,64]{2,1,0:T(2,128)(2,1)S(1)} async-done(((bf16[8,2,64]{2,1,0:T(2,128)(2,1)}), bf16[8,2,64]{2,1,0:T(2,128)(2,1)S(1)}, u32[]{:S(2)}, u32[]{:S(2)}) %all-to-all-start.4) | async-done | bytes 2080 | tf_op jit(solution)/shard_map/all_to_all | solution.py:21
  144.6 0.5 reduce_sum.12
  (37 shorter events, 0.2 us)
Async XLA Ops:
  1.4 15.3 %collective-permute-start = (bf16[64,512]{1,0:T(8,128)(2,1)S(1)}, bf16[64,512]{1,0:T(8,128)(2,1)S(1)}, u32[]{:S(2)}, u32[]{:S(2)}) collective-permute-start(bf16[64,512]{1,0:T(8,128)(2,1)S(1)} %pad_maximum_fusion.1), channel_id=1, source_target_pairs={{0,64},{64,0},{1,65},{65,1},{2,66},{66,2},{3,67},{67,3},{4,68},{68... | collective-permute-start | bytes 196616 | tf_op jit(solution)/shard_map/ppermute | solution.py:346
  8.8 7.0 %copy-start.6 = (bf16[2,64,4096]{2,1,0:T(8,128)(2,1)S(1)}, bf16[2,64,4096]{2,1,0:T(8,128)(2,1)}, u32[]{:S(2)}) copy-start(bf16[2,64,4096]{2,1,0:T(8,128)(2,1)} %param.15) | copy-start | bytes 3145732
  8.8 7.0 %copy-start.7 = (bf16[4096,16]{0,1:T(8,128)(2,1)S(1)}, bf16[4096,16]{0,1:T(8,128)(2,1)}, u32[]{:S(2)}) copy-start(bf16[4096,16]{0,1:T(8,128)(2,1)} %param.19) | copy-start | bytes 393220
  8.8 7.0 %copy-start.8 = (bf16[4096,16]{0,1:T(8,128)(2,1)S(1)}, bf16[4096,16]{0,1:T(8,128)(2,1)}, u32[]{:S(2)}) copy-start(bf16[4096,16]{0,1:T(8,128)(2,1)} %param.18) | copy-start | bytes 393220
  8.8 36.2 %all-to-all-start = ((bf16[8,128,512]{2,1,0:T(8,128)(2,1)}), bf16[8,128,512]{2,1,0:T(8,128)(2,1)S(1)}, u32[]{:S(2)}, u32[]{:S(2)}) async-start(bf16[8,128,512]{2,1,0:T(8,128)(2,1)} %columns.1), calls=%async_computation | async-start | bytes 2097152 | tf_op jit(solution)/shard_map/all_to_all | solution.py:21
  15.8 0.7 copy-start.10
  15.8 0.7 copy-start.12
  15.8 0.7 copy-start.11
  46.7 33.4 %all-to-all-start.1 = ((bf16[8,264,256]{2,1,0:T(8,128)(2,1)}), bf16[8,264,256]{2,1,0:T(8,128)(2,1)S(1)}, u32[]{:S(2)}, u32[]{:S(2)}) async-start(bf16[8,264,256]{2,1,0:T(8,128)(2,1)} %bitcast.10), calls=%async_computation.1 | async-start | bytes 2162688 | tf_op jit(solution)/shard_map/all_to_all | solution.py:21
  83.7 7.9 %collective-permute-start.1 = (bf16[768,128]{1,0:T(8,128)(2,1)S(1)}, bf16[768,128]{1,0:T(8,128)(2,1)S(1)}, u32[]{:S(2)}, u32[]{:S(2)}) collective-permute-start(bf16[768,128]{1,0:T(8,128)(2,1)S(1)} %get-tuple-element.6), channel_id=1, source_target_pairs={{0,8},{8,0},{16,24},{24,16},{32,40},{40,32},{48,56},{56,48},{1,9},... | collective-permute-start | bytes 589832 | tf_op jit(solution)/shard_map/ppermute | solution.py:374
  92.5 27.7 %copy-start.9 = (bf16[256,64]{0,1:T(8,128)(2,1)S(1)}, bf16[256,64]{0,1:T(8,128)(2,1)}, u32[]{:S(2)}) copy-start(bf16[256,64]{0,1:T(8,128)(2,1)} %param.29) | copy-start | bytes 98308
  92.5 22.0 %all-to-all-start.2 = ((bf16[8,192,128]{2,1,0:T(8,128)(2,1)}), bf16[8,192,128]{2,1,0:T(8,128)(2,1)S(1)}, u32[]{:S(2)}, u32[]{:S(2)}) async-start(bf16[8,192,128]{2,1,0:T(8,128)(2,1)} %line.1), calls=%async_computation.2 | async-start | bytes 786432 | tf_op jit(solution)/shard_map/all_to_all | solution.py:21
  101.9 27.7 %copy-start = (f32[2,2]{1,0:T(2,128)S(1)}, f32[2,2]{1,0:T(2,128)}, u32[]{:S(2)}) copy-start(f32[2,2]{1,0:T(2,128)} %strength_ref.1) | copy-start | bytes 52
  101.9 27.7 %copy-start.1 = (bf16[2,256]{1,0:T(2,128)(2,1)S(1)}, bf16[2,256]{1,0:T(2,128)(2,1)}, u32[]{:S(2)}) copy-start(bf16[2,256]{1,0:T(2,128)(2,1)} %probe_ref.1) | copy-start | bytes 3076
  101.9 27.7 %copy-start.2 = (bf16[2,256]{1,0:T(2,128)(2,1)S(1)}, bf16[2,256]{1,0:T(2,128)(2,1)}, u32[]{:S(2)}) copy-start(bf16[2,256]{1,0:T(2,128)(2,1)} %address_ref.1) | copy-start | bytes 3076
  101.9 27.7 %copy-start.3 = (bf16[2,256]{1,0:T(2,128)(2,1)S(1)}, bf16[2,256]{1,0:T(2,128)(2,1)}, u32[]{:S(2)}) copy-start(bf16[2,256]{1,0:T(2,128)(2,1)} %content_ref.1) | copy-start | bytes 3076
  101.9 27.7 %copy-start.4 = (bf16[2,256]{1,0:T(2,128)(2,1)S(1)}, bf16[2,256]{1,0:T(2,128)(2,1)}, u32[]{:S(2)}) copy-start(bf16[2,256]{1,0:T(2,128)(2,1)} %outgate_ref.1) | copy-start | bytes 3076
  101.9 27.7 %copy-start.5 = (f32[128]{0:T(128)S(1)}, f32[128]{0:T(128)}, u32[]{:S(2)}) copy-start(f32[128]{0:T(128)} %param.28) | copy-start | bytes 1540
  116.8 12.7 %all-to-all-start.3 = ((bf16[8,128,128]{2,1,0:T(8,128)(2,1)}), bf16[8,128,128]{2,1,0:T(8,128)(2,1)S(1)}, u32[]{:S(2)}, u32[]{:S(2)}) async-start(bf16[8,128,128]{2,1,0:T(8,128)(2,1)} %scan.1), calls=%async_computation.3 | async-start | bytes 524288 | tf_op jit(solution)/shard_map/all_to_all | solution.py:21
  131.6 13.0 %all-to-all-start.4 = ((bf16[8,2,64]{2,1,0:T(2,128)(2,1)}), bf16[8,2,64]{2,1,0:T(2,128)(2,1)S(1)}, u32[]{:S(2)}, u32[]{:S(2)}) async-start(bf16[8,2,64]{2,1,0:T(2,128)(2,1)} %read.1), calls=%async_computation.4 | async-start | bytes 8192 | tf_op jit(solution)/shard_map/all_to_all | solution.py:21

commit v6 on v5

--- a/solution.py
+++ b/solution.py
@@ -21,12 +21,14 @@
     return lax.all_to_all(messages, axis, split_axis=0, concat_axis=0, tiled=True)
 
 
-def columns_body(tokens_ref, columns_ref, buffer_ref, arrived):
+def columns_body(prompt_ref, tokens_ref, columns_ref, buffer_ref, arrived):
     parts, step, model = buffer_ref.shape
     share = model // (SIDE * SIDE)
     reads = [
         pltpu.make_async_copy(
-            tokens_ref.at[i * step : (i + 1) * step, :], buffer_ref.at[i], arrived.at[i]
+            tokens_ref.at[prompt_ref[0], i * step : (i + 1) * step, :],
+            buffer_ref.at[i],
+            arrived.at[i],
         )
         for i in range(parts)
     ]
@@ -42,53 +44,52 @@
             )
 
 
-def columns_by_owner(flat, parts=4):
-    rows, model = flat.shape
+def columns_by_owner(prompt, tokens, parts=2):
+    _, rows, model = tokens.shape
     return pl.pallas_call(
         columns_body,
-        in_specs=[pl.BlockSpec(memory_space=pltpu.MemorySpace.HBM)],
+        in_specs=[
+            pl.BlockSpec(memory_space=pltpu.SMEM),
+            pl.BlockSpec(memory_space=pltpu.MemorySpace.HBM),
+        ],
         out_specs=VMEM,
-        out_shape=jax.ShapeDtypeStruct((SIDE, rows, model // SIDE), flat.dtype),
+        out_shape=jax.ShapeDtypeStruct((SIDE, rows, model // SIDE), tokens.dtype),
         scratch_shapes=[
-            pltpu.VMEM((parts, rows // parts, model), flat.dtype),
+            pltpu.VMEM((parts, rows // parts, model), tokens.dtype),
             pltpu.SemaphoreType.DMA((parts,)),
         ],
         interpret=INTERPRET,
         name="columns",
-    )(flat)
-
-
-def partial_body(tokens_ref, weights_ref, gates_ref, sent_ref):
-    line, rows, _ = tokens_ref.shape
-    owners, halves, sent_rows, width = sent_ref.shape
+    )(prompt, tokens)
+
+
+def partial_body(prompt_ref, mine_ref, other_ref, weights_ref, gates_ref, sent_ref):
+    line, positions, share = mine_ref.shape
+    prompts, heads, halves, _, width = sent_ref.shape
     ranges = line // halves
-    positions = (sent_rows - gates_ref.shape[2]) // ranges
-    prompts = rows // positions
-    heads = owners // prompts
-    for k in range(line):
-        half, j = k // ranges, k % ranges
-        part = jnp.dot(tokens_ref[k], weights_ref[...], preferred_element_type=jnp.float32)
-        part = part.astype(sent_ref.dtype)
-        for p in range(prompts):
+    for tokens_ref, p in ((mine_ref, prompt_ref[0]), (other_ref, 1 - prompt_ref[0])):
+        for half in range(halves):
+            rows = tokens_ref[half * ranges : (half + 1) * ranges].reshape(-1, share)
+            part = jnp.dot(rows, weights_ref[...], preferred_element_type=jnp.float32)
+            part = part.astype(sent_ref.dtype)
             for h in range(heads):
-                sent_ref[p * heads + h, half, j * positions : (j + 1) * positions, :] = part[
-                    p * positions : (p + 1) * positions, h * width : (h + 1) * width
-                ]
-    sent_ref[:, :, ranges * positions :, :] = gates_ref[...]
-
-
-def partial_projections(tokens, weights, gates, positions):
-    owners, halves, extra, width = gates.shape
-    sent_rows = tokens.shape[0] // halves * positions + extra
+                sent_ref[p, h, half, : ranges * positions, :] = part[:, h * width : (h + 1) * width]
+    sent_ref[:, :, :, ranges * positions :, :] = gates_ref[...]
+
+
+def partial_projections(prompt, mine, other, weights, gates):
+    prompts, heads, halves, extra, width = gates.shape
+    line, positions, _ = mine.shape
+    sent_rows = line // halves * positions + extra
     return pl.pallas_call(
         partial_body,
-        in_specs=[VMEM, VMEM, VMEM],
+        in_specs=[pl.BlockSpec(memory_space=pltpu.SMEM), VMEM, VMEM, VMEM, VMEM],
         out_specs=VMEM,
-        out_shape=jax.ShapeDtypeStruct((owners, halves, sent_rows, width), tokens.dtype),
+        out_shape=jax.ShapeDtypeStruct((prompts, heads, halves, sent_rows, width), mine.dtype),
         interpret=INTERPRET,
         compiler_params=SMALL,
         name="partials",
-    )(tokens, weights, gates)
+    )(prompt, mine, other, weights, gates)
 
 
 def two_parts(values):
@@ -341,32 +342,29 @@
         axis=1,
     )
     flat = tokens.reshape(rows, model)
-    columns = columns_by_owner(flat)
-    line_tokens = exchange(columns, "y")
+    prompt = (tp % 2).astype(jnp.int32).reshape(1)
+    mine = exchange(columns_by_owner(prompt, tokens), "y")
     beside = lax.ppermute(weights, "zl", [(0, 1), (1, 0)])
     even = lax.axis_index("zl") == 0
     both = [jnp.where(even, weights, beside), jnp.where(even, beside, weights)]
     line_weights = lax.all_gather(jnp.concatenate(both), "zh", axis=0, tiled=True)
+    mine, line_weights = lax.optimization_barrier((mine, line_weights))
+    other = lax.ppermute(mine, "tp", [(i, i ^ 1) for i in range(lax.axis_size("tp"))])
 
     drivers = jnp.concatenate([strength_projection, fading_driver_projection], axis=1)
     logits = jnp.dot(flat, drivers, preferred_element_type=jnp.float32).astype(jnp.bfloat16)
     logits = logits.astype(jnp.float32).reshape(prompts, positions, 2, -1)
-    mine = lax.dynamic_slice_in_dim(logits, tp * heads, heads, 3)
-    beta = jax.nn.sigmoid(mine[:, :, 0] + strength_offset)
-    fading = added_fading - fading_speed * jax.nn.softplus(mine[:, :, 1])
+    own = lax.dynamic_slice_in_dim(logits, tp * heads, heads, 3)
+    beta = jax.nn.sigmoid(own[:, :, 0] + strength_offset)
+    fading = added_fading - fading_speed * jax.nn.softplus(own[:, :, 1])
     gates = jnp.stack([*two_parts(beta), *two_parts(fading)])
     gates = jnp.pad(
         gates.transpose(1, 3, 0, 2), ((0, 0), (0, 0), (0, 4), (0, 2 * WIDTH - positions))
     )
 
     gates = jnp.broadcast_to(gates[:, :, None], (prompts, heads, 2, *gates.shape[2:]))
-    sent = partial_projections(
-        line_tokens,
-        line_weights,
-        gates.reshape(prompts * heads, *gates.shape[2:]),
-        positions,
-    )
-    got = exchange(sent.reshape(SIDE, *sent.shape[2:]), "y")
+    sent = partial_projections(prompt, mine, other, line_weights, gates)
+    got = exchange(sent.reshape(SIDE, *sent.shape[3:]), "y")
 
     side = my_half.astype(jnp.int32).reshape(1)
     size = (half * (WIDTH + WIDTH // 2), WIDTH)

time: 146 us -> 144 us (0.986)
  starting transfers between devices: 38.3 us -> 44.6 us
  waiting for transfers between devices: 69.1 us -> 63.2 us
    all_to_all x5, waiting for transfers between devices: 63.2 us -> 54.7 us  [exchange(): lax.all_to_all(messages, axis, split_axis=0, concat_axis=0, tiled=True)]
    ppermute x0 -> x1, starting transfers between devices: none -> 6.09 us  [per_device(): lax.ppermute(mine, 'tp', [(i, i ^ 1) for i in range(lax.axis_size('tp'))])]
  transfers between devices with their start and end apart: 7 -> 8, of which waited for: 6 -> 7; matrix products, arithmetic and copies ran while one was open for 2% -> 2% of each run, Pallas kernels for 2% -> 0%
where the time goes in v6:
time: 144 us
  waiting for transfers between devices  63.2 us (44%)
  starting transfers between devices  44.6 us (31%)
  blocking collectives  18.8 us (13%)
  Pallas kernels  12.7 us (9%)
  local copies, waits for them, and re-layouts  1.91 us (1%)
    all_to_all x5, waiting for transfers between devices, exchange(): lax.all_to_all(messages, axis, split_axis=0, concat_axis=0, tiled=True)  54.7 us
    all_to_all x5, starting transfers between devices, exchange(): lax.all_to_all(messages, axis, split_axis=0, concat_axis=0, tiled=True)  32.5 us
    all_gather x1, blocking collectives, per_device(): lax.all_gather(jnp.concatenate(both), 'zh', axis=0, tiled=True)  18.8 us
    pallas_call x4, Pallas kernels, local(): pl.pallas_call(body, in_specs=[SMEM] + [VMEM] * (len(operands) - 1), out_...  8.85 us
    ppermute x1, starting transfers between devices, per_device(): lax.ppermute(mine, 'tp', [(i, i ^ 1) for i in range(lax.axis_size('tp'))])  6.09 us
    ppermute x1, waiting for transfers between devices, per_device(): other = lax.ppermute(given, 'y', [(i, i ^ 1) for i in range(SIDE)])  5.93 us
    ppermute x1, starting transfers between devices, per_device(): beside = lax.ppermute(weights, 'zl', [(0, 1), (1, 0)])  4 us
  transfers between devices with their start and end apart: 8, of which 7 were waited for; matrix products, arithmetic and copies ran while one was open for 2% of the time, Pallas kernels for 0%

profile of v6, /device:TPU:1, one launch (start us, length us, event | category | flops | bytes accessed | tf_op | source)
XLA Modules:
  0.0 143.5 jit_solution(10584269601969952505)
XLA Ops:
  0.7 2.2 %columns.1 = bf16[8,64,512]{2,1,0:T(8,128)(2,1)} custom-call(s32[1]{0:T(128)} %bitcast.2.prompt_ref, bf16[2,64,4096]{2,1,0:T(8,128)(2,1)} %tokens_ref.1), custom_call_target="tpu_custom_call" | custom-call | tf_op jit(solution)/shard_map/columns/pallas_call | solution.py:49
  2.9 7.7 %all-to-all-start = ((bf16[8,64,512]{2,1,0:T(8,128)(2,1)}), bf16[8,64,512]{2,1,0:T(8,128)(2,1)S(1)}, u32[]{:S(2)}, u32[]{:S(2)}) async-start(bf16[8,64,512]{2,1,0:T(8,128)(2,1)} %columns.1), calls=%async_computation | async-start | bytes 1048576 | tf_op jit(solution)/shard_map/all_to_all | solution.py:21
  10.5 0.0 copy-start.13
  10.6 4.0 %collective-permute-start = (bf16[64,512]{1,0:T(8,128)(2,1)S(1)}, bf16[64,512]{1,0:T(8,128)(2,1)S(1)}, u32[]{:S(2)}, u32[]{:S(2)}) collective-permute-start(bf16[64,512]{1,0:T(8,128)(2,1)S(1)} %pad_maximum_fusion.1), channel_id=1, source_target_pairs={{0,64},{64,0},{1,65},{65,1},{2,66},{66,2},{3,67},{67,3},{4,68},{68... | collective-permute-start | bytes 196616 | tf_op jit(solution)/shard_map/ppermute | solution.py:347
  14.6 0.4 fusion.1
  15.1 0.1 reshape.82
  15.2 0.1 reduce-precision_convert_fusion.1
  15.3 0.1 fusion.15
  15.4 1.1 collective-permute-done
  16.6 18.8 %all_gather.3.weights_ref = bf16[512,512]{1,0:T(8,128)(2,1)S(1)} all-gather(bf16[128,512]{1,0:T(8,128)(2,1)S(1)} %pad_maximum_fusion), channel_id=1, replica_groups=mesh['zh'=4,'zl'=2,'y'=8,'tp'=8] {'zh'}, dimensions={0}, use_global_device_ids=true | all-gather | bytes 655360 | tf_op jit(solution)/shard_map/all_gather | solution.py:350
  35.4 6.1 %collective-permute-start.1 = (bf16[8,64,512]{2,1,0:T(8,128)(2,1)S(1)}, bf16[8,64,512]{2,1,0:T(8,128)(2,1)S(1)}, u32[]{:S(2)}, u32[]{:S(2)}) collective-permute-start(bf16[8,64,512]{2,1,0:T(8,128)(2,1)S(1)} %all-to-all-done.mine_ref), channel_id=1, source_target_pairs={{0,1},{1,0},{2,3},{3,2},{4,5},{5,4},{6,7},{7,6},{8,9},{9,8},{10,11... | collective-permute-start | bytes 1572872 | tf_op jit(solution)/shard_map/ppermute | solution.py:352
  41.6 1.4 %collective-permute-done.1.other_ref = bf16[8,64,512]{2,1,0:T(8,128)(2,1)S(1)} collective-permute-done((bf16[8,64,512]{2,1,0:T(8,128)(2,1)S(1)}, bf16[8,64,512]{2,1,0:T(8,128)(2,1)S(1)}, u32[]{:S(2)}, u32[]{:S(2)}) %collective-permute-start.1) | collective-permute-done | bytes 524320 | tf_op jit(solution)/shard_map/ppermute | solution.py:352
  43.0 1.7 %partials.1 = bf16[2,2,2,264,256]{4,3,2,1,0:T(8,128)(2,1)} custom-call(s32[1]{0:T(128)} %bitcast.2.prompt_ref, bf16[8,64,512]{2,1,0:T(8,128)(2,1)S(1)} %all-to-all-done.mine_ref, bf16[8,64,512]{2,1,0:T(8,128)(2,1)S(1)} %collective-permute-done.1.other_ref, bf16[512,512]{1,0:T(8,128)(2,1)S(1)} %all_gather.3.weights_ref, ...), custom_call_target="tpu_custom_call" | custom-call | tf_op jit(solution)/shard_map/partials/pallas_call | solution.py:84
  44.8 8.4 %all-to-all-start.1 = ((bf16[8,264,256]{2,1,0:T(8,128)(2,1)}), bf16[8,264,256]{2,1,0:T(8,128)(2,1)S(1)}, u32[]{:S(2)}, u32[]{:S(2)}) async-start(bf16[8,264,256]{2,1,0:T(8,128)(2,1)} %bitcast.10), calls=%async_computation.1 | async-start | bytes 2162688 | tf_op jit(solution)/shard_map/all_to_all | solution.py:21
  53.2 29.9 %all-to-all-done.1.got_ref = bf16[8,264,256]{2,1,0:T(8,128)(2,1)S(1)} async-done(((bf16[8,264,256]{2,1,0:T(8,128)(2,1)}), bf16[8,264,256]{2,1,0:T(8,128)(2,1)S(1)}, u32[]{:S(2)}, u32[]{:S(2)}) %all-to-all-start.1) | async-done | bytes 1081376 | tf_op jit(solution)/shard_map/all_to_all | solution.py:21
  83.1 3.6 %ranges.1 = (bf16[768,128]{1,0:T(8,128)(2,1)S(1)}, bf16[768,128]{1,0:T(8,128)(2,1)S(1)}) custom-call(s32[1]{0:T(128)} %bitcast.1.half_ref, bf16[8,264,256]{2,1,0:T(8,128)(2,1)S(1)} %all-to-all-done.1.got_ref), custom_call_target="tpu_custom_call" | custom-call | tf_op jit(solution)/shard_map/ranges/pallas_call | solution.py:300
  86.7 1.9 %collective-permute-start.2 = (bf16[768,128]{1,0:T(8,128)(2,1)S(1)}, bf16[768,128]{1,0:T(8,128)(2,1)S(1)}, u32[]{:S(2)}, u32[]{:S(2)}) collective-permute-start(bf16[768,128]{1,0:T(8,128)(2,1)S(1)} %get-tuple-element.10), channel_id=1, source_target_pairs={{0,8},{8,0},{16,24},{24,16},{32,40},{40,32},{48,56},{56,48},{1,9},... | collective-permute-start | bytes 589832 | tf_op jit(solution)/shard_map/ppermute | solution.py:372
  88.7 5.9 %collective-permute-done.2.other_ref = bf16[768,128]{1,0:T(8,128)(2,1)S(1)} collective-permute-done((bf16[768,128]{1,0:T(8,128)(2,1)S(1)}, bf16[768,128]{1,0:T(8,128)(2,1)S(1)}, u32[]{:S(2)}, u32[]{:S(2)}) %collective-permute-start.2) | collective-permute-done | bytes 196640 | tf_op jit(solution)/shard_map/ppermute | solution.py:372
  94.6 0.9 line.1
  95.5 4.7 %all-to-all-start.2 = ((bf16[8,192,128]{2,1,0:T(8,128)(2,1)}), bf16[8,192,128]{2,1,0:T(8,128)(2,1)S(1)}, u32[]{:S(2)}, u32[]{:S(2)}) async-start(bf16[8,192,128]{2,1,0:T(8,128)(2,1)} %line.1), calls=%async_computation.2 | async-start | bytes 786432 | tf_op jit(solution)/shard_map/all_to_all | solution.py:21
  100.2 0.1 pad_add_fusion.place_ref
  100.4 12.6 %all-to-all-done.2.lines_ref = bf16[8,192,128]{2,1,0:T(8,128)(2,1)S(1)} async-done(((bf16[8,192,128]{2,1,0:T(8,128)(2,1)}), bf16[8,192,128]{2,1,0:T(8,128)(2,1)S(1)}, u32[]{:S(2)}, u32[]{:S(2)}) %all-to-all-start.2) | async-done | bytes 393248 | tf_op jit(solution)/shard_map/all_to_all | solution.py:21
  112.9 2.4 %scan.1 = bf16[8,128,128]{2,1,0:T(8,128)(2,1)} custom-call(s32[2]{0:T(128)S(1)} %pad_add_fusion.place_ref, bf16[8,192,128]{2,1,0:T(8,128)(2,1)S(1)} %all-to-all-done.2.lines_ref, bf16[768,128]{1,0:T(8,128)(2,1)S(1)} %get-tuple-element.9.kept_ref, bf16[768,128]{1,0:T(8,128)(2,1)S(1)} %collective-permute-done.2.other_ref), custom_call_target="tpu_custom_call" | custom-call | tf_op jit(solution)/shard_map/scan/pallas_call | solution.py:300
  115.3 3.4 %all-to-all-start.3 = ((bf16[8,128,128]{2,1,0:T(8,128)(2,1)}), bf16[8,128,128]{2,1,0:T(8,128)(2,1)S(1)}, u32[]{:S(2)}, u32[]{:S(2)}) async-start(bf16[8,128,128]{2,1,0:T(8,128)(2,1)} %scan.1), calls=%async_computation.3 | async-start | bytes 524288 | tf_op jit(solution)/shard_map/all_to_all | solution.py:21
  118.7 0.1 copy.26.readout_ref
  118.8 9.1 %all-to-all-done.3.back_ref = bf16[8,128,128]{2,1,0:T(8,128)(2,1)S(1)} async-done(((bf16[8,128,128]{2,1,0:T(8,128)(2,1)}), bf16[8,128,128]{2,1,0:T(8,128)(2,1)S(1)}, u32[]{:S(2)}, u32[]{:S(2)}) %all-to-all-start.3) | async-done | bytes 262176 | tf_op jit(solution)/shard_map/all_to_all | solution.py:21
  128.1 2.0 %read.1 = bf16[8,2,64]{2,1,0:T(2,128)(2,1)} custom-call(f32[2,2]{1,0:T(2,128)S(1)} %copy-done, bf16[8,128,128]{2,1,0:T(8,128)(2,1)S(1)} %all-to-all-done.3.back_ref, bf16[2,256]{1,0:T(2,128)(2,1)S(1)} %copy-done.1, bf16[2,256]{1,0:T(2,128)(2,1)S(1)} %copy-done.2, bf16[2,256]{1,0:T(2,128)(2,1)S(1)} %copy-done.3, bf16[2,256]{1,0:T(2,128)(2,1)S(1)} %copy-done.4, ...), custom_call_target="tpu_custom_call" | custom-call | tf_op jit(solution)/shard_map/read/pallas_call | solution.py:300
  130.0 8.4 %all-to-all-start.4 = ((bf16[8,2,64]{2,1,0:T(2,128)(2,1)}), bf16[8,2,64]{2,1,0:T(2,128)(2,1)S(1)}, u32[]{:S(2)}, u32[]{:S(2)}) async-start(bf16[8,2,64]{2,1,0:T(2,128)(2,1)} %read.1), calls=%async_computation.4 | async-start | bytes 8192 | tf_op jit(solution)/shard_map/all_to_all | solution.py:21
  138.4 0.8 copy.27
  139.2 0.8 copy.28
  140.0 3.0 %all-to-all-done.4 = bf16[8,2,64]{2,1,0:T(2,128)(2,1)S(1)} async-done(((bf16[8,2,64]{2,1,0:T(2,128)(2,1)}), bf16[8,2,64]{2,1,0:T(2,128)(2,1)S(1)}, u32[]{:S(2)}, u32[]{:S(2)}) %all-to-all-start.4) | async-done | bytes 2080 | tf_op jit(solution)/shard_map/all_to_all | solution.py:21
  143.0 0.5 reduce_sum.12
  (43 shorter events, 0.2 us)
Async XLA Ops:
  0.6 9.9 %copy-start.10 = (bf16[64,256]{1,0:T(8,128)(2,1)S(1)}, bf16[64,256]{1,0:T(8,128)(2,1)}, u32[]{:S(2)}) copy-start(bf16[64,256]{1,0:T(8,128)(2,1)} %param.16) | copy-start | bytes 98308
  0.7 9.9 %copy-start.11 = (bf16[64,256]{1,0:T(8,128)(2,1)S(1)}, bf16[64,256]{1,0:T(8,128)(2,1)}, u32[]{:S(2)}) copy-start(bf16[64,256]{1,0:T(8,128)(2,1)} %param.17) | copy-start | bytes 98308
  0.7 14.0 %copy-start.6 = (bf16[2,64,4096]{2,1,0:T(8,128)(2,1)S(1)}, bf16[2,64,4096]{2,1,0:T(8,128)(2,1)}, u32[]{:S(2)}) copy-start(bf16[2,64,4096]{2,1,0:T(8,128)(2,1)} %tokens_ref.1) | copy-start | bytes 3145732
  0.7 14.0 %copy-start.7 = (bf16[4096,16]{0,1:T(8,128)(2,1)S(1)}, bf16[4096,16]{0,1:T(8,128)(2,1)}, u32[]{:S(2)}) copy-start(bf16[4096,16]{0,1:T(8,128)(2,1)} %param.19) | copy-start | bytes 393220
  0.7 14.0 %copy-start.8 = (bf16[4096,16]{0,1:T(8,128)(2,1)S(1)}, bf16[4096,16]{0,1:T(8,128)(2,1)}, u32[]{:S(2)}) copy-start(bf16[4096,16]{0,1:T(8,128)(2,1)} %param.18) | copy-start | bytes 393220
  2.9 32.6 %all-to-all-start = ((bf16[8,64,512]{2,1,0:T(8,128)(2,1)}), bf16[8,64,512]{2,1,0:T(8,128)(2,1)S(1)}, u32[]{:S(2)}, u32[]{:S(2)}) async-start(bf16[8,64,512]{2,1,0:T(8,128)(2,1)} %columns.1), calls=%async_computation | async-start | bytes 1048576 | tf_op jit(solution)/shard_map/all_to_all | solution.py:21
  10.5 4.7 %copy-start.13 = (f32[2]{0:T(128)S(1)}, f32[2]{0:T(128)}, u32[]{:S(2)}) copy-start(f32[2]{0:T(128)} %param.20) | copy-start | bytes 28
  10.5 4.8 %copy-start.12 = (f32[2,64,2]{1,2,0:T(2,128)S(1)}, f32[2,64,2]{1,2,0:T(2,128)}, u32[]{:S(2)}) copy-start(f32[2,64,2]{1,2,0:T(2,128)} %param.22) | copy-start | bytes 3076
  10.5 4.8 %copy-start.14 = (f32[2]{0:T(128)S(1)}, f32[2]{0:T(128)}, u32[]{:S(2)}) copy-start(f32[2]{0:T(128)} %param.21) | copy-start | bytes 28
  10.6 5.9 %collective-permute-start = (bf16[64,512]{1,0:T(8,128)(2,1)S(1)}, bf16[64,512]{1,0:T(8,128)(2,1)S(1)}, u32[]{:S(2)}, u32[]{:S(2)}) collective-permute-start(bf16[64,512]{1,0:T(8,128)(2,1)S(1)} %pad_maximum_fusion.1), channel_id=1, source_target_pairs={{0,64},{64,0},{1,65},{65,1},{2,66},{66,2},{3,67},{67,3},{4,68},{68... | collective-permute-start | bytes 196616 | tf_op jit(solution)/shard_map/ppermute | solution.py:347
  35.4 7.6 %collective-permute-start.1 = (bf16[8,64,512]{2,1,0:T(8,128)(2,1)S(1)}, bf16[8,64,512]{2,1,0:T(8,128)(2,1)S(1)}, u32[]{:S(2)}, u32[]{:S(2)}) collective-permute-start(bf16[8,64,512]{2,1,0:T(8,128)(2,1)S(1)} %all-to-all-done.mine_ref), channel_id=1, source_target_pairs={{0,1},{1,0},{2,3},{3,2},{4,5},{5,4},{6,7},{7,6},{8,9},{9,8},{10,11... | collective-permute-start | bytes 1572872 | tf_op jit(solution)/shard_map/ppermute | solution.py:352
  44.8 38.4 %all-to-all-start.1 = ((bf16[8,264,256]{2,1,0:T(8,128)(2,1)}), bf16[8,264,256]{2,1,0:T(8,128)(2,1)S(1)}, u32[]{:S(2)}, u32[]{:S(2)}) async-start(bf16[8,264,256]{2,1,0:T(8,128)(2,1)} %bitcast.10), calls=%async_computation.1 | async-start | bytes 2162688 | tf_op jit(solution)/shard_map/all_to_all | solution.py:21
  86.7 7.9 %collective-permute-start.2 = (bf16[768,128]{1,0:T(8,128)(2,1)S(1)}, bf16[768,128]{1,0:T(8,128)(2,1)S(1)}, u32[]{:S(2)}, u32[]{:S(2)}) collective-permute-start(bf16[768,128]{1,0:T(8,128)(2,1)S(1)} %get-tuple-element.10), channel_id=1, source_target_pairs={{0,8},{8,0},{16,24},{24,16},{32,40},{40,32},{48,56},{56,48},{1,9},... | collective-permute-start | bytes 589832 | tf_op jit(solution)/shard_map/ppermute | solution.py:372
  95.5 23.2 %copy-start.9 = (bf16[256,64]{0,1:T(8,128)(2,1)S(1)}, bf16[256,64]{0,1:T(8,128)(2,1)}, u32[]{:S(2)}) copy-start(bf16[256,64]{0,1:T(8,128)(2,1)} %param.29) | copy-start | bytes 98308
  95.5 17.4 %all-to-all-start.2 = ((bf16[8,192,128]{2,1,0:T(8,128)(2,1)}), bf16[8,192,128]{2,1,0:T(8,128)(2,1)S(1)}, u32[]{:S(2)}, u32[]{:S(2)}) async-start(bf16[8,192,128]{2,1,0:T(8,128)(2,1)} %line.1), calls=%async_computation.2 | async-start | bytes 786432 | tf_op jit(solution)/shard_map/all_to_all | solution.py:21
  100.3 27.7 %copy-start = (f32[2,2]{1,0:T(2,128)S(1)}, f32[2,2]{1,0:T(2,128)}, u32[]{:S(2)}) copy-start(f32[2,2]{1,0:T(2,128)} %strength_ref.1) | copy-start | bytes 52
  100.3 27.7 %copy-start.1 = (bf16[2,256]{1,0:T(2,128)(2,1)S(1)}, bf16[2,256]{1,0:T(2,128)(2,1)}, u32[]{:S(2)}) copy-start(bf16[2,256]{1,0:T(2,128)(2,1)} %probe_ref.1) | copy-start | bytes 3076
  100.3 27.7 %copy-start.2 = (bf16[2,256]{1,0:T(2,128)(2,1)S(1)}, bf16[2,256]{1,0:T(2,128)(2,1)}, u32[]{:S(2)}) copy-start(bf16[2,256]{1,0:T(2,128)(2,1)} %address_ref.1) | copy-start | bytes 3076
  100.3 27.7 %copy-start.3 = (bf16[2,256]{1,0:T(2,128)(2,1)S(1)}, bf16[2,256]{1,0:T(2,128)(2,1)}, u32[]{:S(2)}) copy-start(bf16[2,256]{1,0:T(2,128)(2,1)} %content_ref.1) | copy-start | bytes 3076
  100.3 27.7 %copy-start.4 = (bf16[2,256]{1,0:T(2,128)(2,1)S(1)}, bf16[2,256]{1,0:T(2,128)(2,1)}, u32[]{:S(2)}) copy-start(bf16[2,256]{1,0:T(2,128)(2,1)} %outgate_ref.1) | copy-start | bytes 3076
  100.3 27.7 %copy-start.5 = (f32[128]{0:T(128)S(1)}, f32[128]{0:T(128)}, u32[]{:S(2)}) copy-start(f32[128]{0:T(128)} %param.28) | copy-start | bytes 1540
  115.3 12.7 %all-to-all-start.3 = ((bf16[8,128,128]{2,1,0:T(8,128)(2,1)}), bf16[8,128,128]{2,1,0:T(8,128)(2,1)S(1)}, u32[]{:S(2)}, u32[]{:S(2)}) async-start(bf16[8,128,128]{2,1,0:T(8,128)(2,1)} %scan.1), calls=%async_computation.3 | async-start | bytes 524288 | tf_op jit(solution)/shard_map/all_to_all | solution.py:21
  130.0 13.0 %all-to-all-start.4 = ((bf16[8,2,64]{2,1,0:T(2,128)(2,1)}), bf16[8,2,64]{2,1,0:T(2,128)(2,1)S(1)}, u32[]{:S(2)}, u32[]{:S(2)}) async-start(bf16[8,2,64]{2,1,0:T(2,128)(2,1)} %read.1), calls=%async_computation.4 | async-start | bytes 8192 | tf_op jit(solution)/shard_map/all_to_all | solution.py:21

commit v7 on v4

--- a/solution.py
+++ b/solution.py
@@ -218,11 +218,29 @@
     rows = wide // 2
     ranges = sent_ref.shape[0] // 2
     z, mine_first = place_ref[0], place_ref[1] == 0
-    state = lines_ref[0, wide:, :].astype(jnp.float32)
-    entering = jnp.zeros_like(state)
-    for k in range(1, lines):
-        entering = jnp.where(z == k, state, entering)
-        state = times(state, lines_ref[k, :wide, :]) + lines_ref[k, wide:, :].astype(jnp.float32)
+    after, pairs = [], []
+    for k in range(0, lines, 2):
+        both = jnp.dot(
+            lines_ref[k], lines_ref[k + 1, :wide, :], preferred_element_type=jnp.float32
+        )
+        added = both[wide:] + lines_ref[k + 1, wide:, :].astype(jnp.float32)
+        pairs.append((parts(both[:wide]), added))
+    state = jnp.zeros((rows, wide), jnp.float32)
+    for k, ((high, low), added) in enumerate(pairs):
+        after.append(state)
+        if k:
+            ours = jnp.concatenate(parts(state), axis=0)
+            found = jnp.dot(ours, high, preferred_element_type=jnp.float32)
+            found = found[:rows] + found[rows:]
+            state = found + jnp.dot(ours[:rows], low, preferred_element_type=jnp.float32) + added
+        else:
+            state = added
+    begin = after[0]
+    for k in range(1, len(after)):
+        begin = jnp.where(z // 2 == k, after[k], begin)
+    before = lines_ref[(z // 2) * 2]
+    stepped = times(begin, before[:wide]) + before[wide:].astype(jnp.float32)
+    entering = jnp.where(z % 2 == 0, begin, stepped)
     final = state.astype(jnp.bfloat16)
     state = entering
     for h in range(2):
@@ -238,22 +256,13 @@
             sent_ref[h * ranges + j, rows:, :] = final
 
 
-def read_body(
-    strength_ref,
-    back_ref,
-    probe_ref,
-    address_ref,
-    content_ref,
-    outgate_ref,
-    gain_ref,
-    readout_ref,
-    sent_ref,
+def first_step_body(
+    strength_ref, probe_ref, address_ref, content_ref, outgate_ref, gain_ref, rows_ref
 ):
-    wide = back_ref.shape[2]
-    rows = wide // 2
     prompts, width = probe_ref.shape
-    heads = width // wide
-    each = [(p, h) for p in range(prompts) for h in range(heads)]
+    wide = gain_ref.shape[1]
+    each = [(p, h) for p in range(prompts) for h in range(width // wide)]
+    count = len(each)
 
     def gathered(ref):
         wanted = [ref[p : p + 1, h * wide : (h + 1) * wide] for p, h in each]
@@ -262,24 +271,41 @@
     query = silu(gathered(probe_ref))
     key = silu(gathered(address_ref))
     key = key * lax.rsqrt(jnp.sum(key * key, axis=-1, keepdims=True) + EPSILON)
-    value = silu(gathered(content_ref))
     strength = jnp.concatenate(
         [jnp.full((1, 1), strength_ref[p, h], jnp.float32) for p, h in each], axis=0
     )
     strength = 1.0 / (1.0 + jnp.exp(-strength))
-    pair = jnp.concatenate([key, query], axis=0)
+    along = jnp.sum(key * query, axis=-1, keepdims=True)
+    rest = jnp.concatenate([key, query], axis=0)
+    for k in range(3):
+        part = rest.astype(jnp.bfloat16).astype(jnp.float32)
+        rows_ref[2 * count * k : 2 * count * (k + 1), :] = part
+        rest = rest - part
+    rows_ref[6 * count : 7 * count, :] = silu(gathered(content_ref))
+    rows_ref[7 * count : 8 * count, :] = gain_ref[...] * silu(gathered(outgate_ref))
+    rows_ref[8 * count : 9 * count, :] = jnp.broadcast_to(strength * along, (count, wide))
+
+
+def read_body(back_ref, rows_ref, readout_ref, sent_ref):
+    wide = back_ref.shape[2]
+    half = wide // 2
+    count = back_ref.shape[0] // 2
+    prompts = sent_ref.shape[1]
+    heads = count // prompts
+    pair = rows_ref[: 6 * count, :].astype(jnp.bfloat16)
     recalled, probed = [], []
-    for n in range(len(each)):
-        state = jnp.concatenate([back_ref[2 * n, rows:, :], back_ref[2 * n + 1, rows:, :]], axis=0)
-        found = best(pair, state.astype(jnp.float32), ((1,), (1,)))
+    for n in range(count):
+        state = jnp.concatenate([back_ref[2 * n, half:, :], back_ref[2 * n + 1, half:, :]], axis=0)
+        found = lax.dot_general(
+            pair, state, (((1,), (1,)), ((), ())), preferred_element_type=jnp.float32
+        )
+        found = found[: 2 * count] + found[2 * count : 4 * count] + found[4 * count :]
         recalled.append(found[n : n + 1])
-        probed.append(found[len(each) + n : len(each) + n + 1])
-    along = jnp.sum(key * query, axis=-1, keepdims=True)
-    out = jnp.concatenate(probed, axis=0) + strength * along * (
-        value - jnp.concatenate(recalled, axis=0)
-    )
+        probed.append(found[count + n : count + n + 1])
+    value, gate, weight = (rows_ref[k * count : (k + 1) * count, :] for k in (6, 7, 8))
+    out = jnp.concatenate(probed, axis=0) + weight * (value - jnp.concatenate(recalled, axis=0))
     out = out * lax.rsqrt(jnp.mean(out * out, axis=-1, keepdims=True) + EPSILON)
-    read = out * gain_ref[...] * silu(gathered(outgate_ref))
+    read = out * gate
     rows_of = [
         jnp.concatenate([read[p * heads + h :][:1] for h in range(heads)], axis=1)
         for p in range(prompts)
@@ -293,11 +319,11 @@
 SMEM = pl.BlockSpec(memory_space=pltpu.SMEM)
 
 
-def local(body, name, shapes, *operands):
-    out = [jax.ShapeDtypeStruct(shape, jnp.bfloat16) for shape in shapes]
+def local(body, name, shapes, *operands, kind=jnp.bfloat16, scalars=1):
+    out = [jax.ShapeDtypeStruct(shape, kind) for shape in shapes]
     return pl.pallas_call(
         body,
-        in_specs=[SMEM] + [VMEM] * (len(operands) - 1),
+        in_specs=[SMEM] * scalars + [VMEM] * (len(operands) - scalars),
         out_specs=[VMEM] * len(out),
         out_shape=out,
         interpret=INTERPRET,
@@ -374,19 +400,20 @@
     (home,) = local(scan_body, "scan", [(SIDE, WIDTH, WIDTH)], place, lines, kept, other)
 
     back = exchange(home, "y")
-    (terms,) = local(
-        read_body,
-        "read",
-        [(lax.axis_size("tp"), prompts, readout_projection.shape[1])],
+    (first_step,) = local(
+        first_step_body,
+        "first_step",
+        [(9 * prompts * heads, WIDTH)],
         strength_raw,
-        back,
         probe,
         address,
         content,
         outgate,
         gain.reshape(1, WIDTH),
-        readout_projection,
-    )
+        kind=jnp.float32,
+    )
+    sizes = [(lax.axis_size("tp"), prompts, readout_projection.shape[1])]
+    (terms,) = local(read_body, "read", sizes, back, first_step, readout_projection, scalars=0)
     mixed = exchange(terms, "tp").astype(jnp.float32).sum(axis=0)
     states = back.reshape(prompts, heads, 2, 2, WIDTH // 2, WIDTH).transpose(3, 0, 1, 5, 2, 4)
     boundary, state_cache = states.reshape(2, prompts, heads, WIDTH, WIDTH)

time: 142 us -> 141 us (level)
    pallas_call x4 -> x5, Pallas kernels: 8.87 us -> 8.48 us  [local(): pl.pallas_call(body, in_specs=[SMEM] * scalars + [VMEM] * (len(operands)...]
  transfers between devices with their start and end apart: 6 -> 6, of which waited for: 5 -> 5; matrix products, arithmetic and copies ran while one was open for 2% -> 2% of each run, Pallas kernels for 0% -> 1%
where the time goes in v7:
time: 141 us; the launch traced here: 140 us
  waiting for transfers between devices  54.2 us (38%)
  starting transfers between devices  41.7 us (30%)
  blocking collectives  27.2 us (19%)
  Pallas kernels  12.7 us (9%)
  local copies, waits for them, and re-layouts  1.93 us (1%)
    all_to_all x5, waiting for transfers between devices, exchange(): lax.all_to_all(messages, axis, split_axis=0, concat_axis=0, tiled=True)  49.7 us
    all_to_all x5, starting transfers between devices, exchange(): lax.all_to_all(messages, axis, split_axis=0, concat_axis=0, tiled=True)  39.7 us
    all_gather x1, blocking collectives, per_device(): line_weights = lax.all_gather(weights, 'z', axis=0, tiled=True)  27.2 us
    pallas_call x5, Pallas kernels, local(): pl.pallas_call(body, in_specs=[SMEM] * scalars + [VMEM] * (len(operands)...  8.48 us
    ppermute x1, waiting for transfers between devices, per_device(): other = lax.ppermute(given, 'y', [(i, i ^ 1) for i in range(SIDE)])  4.49 us
  transfers between devices with their start and end apart: 6, of which 5 were waited for; matrix products, arithmetic and copies ran while one was open for 2% of the time, Pallas kernels for 1%

profile of v7, /device:TPU:1, one launch (start us, length us, event | category | flops | bytes accessed | tf_op | source)
XLA Modules:
  0.0 140.0 jit_solution(17946647024265484468)
XLA Ops:
  0.6 2.5 %columns.1 = bf16[8,128,512]{2,1,0:T(8,128)(2,1)} custom-call(bf16[128,4096]{1,0:T(8,128)(2,1)} %bitcast.43), custom_call_target="tpu_custom_call" | custom-call | tf_op jit(solution)/shard_map/columns/pallas_call | solution.py:46
  3.2 0.0 copy-start.6
  3.2 0.0 copy-start.7
  3.2 7.8 %all-to-all-start = ((bf16[8,128,512]{2,1,0:T(8,128)(2,1)}), bf16[8,128,512]{2,1,0:T(8,128)(2,1)S(1)}, u32[]{:S(2)}, u32[]{:S(2)}) async-start(bf16[8,128,512]{2,1,0:T(8,128)(2,1)} %columns.1), calls=%async_computation | async-start | bytes 2097152 | tf_op jit(solution)/shard_map/all_to_all | solution.py:20
  11.0 0.0 copy-start.10
  11.1 0.4 fusion.1
  11.5 0.1 reshape.81
  11.7 0.0 copy-done.12
  11.7 0.1 fusion.15
  11.8 0.1 reduce-precision_convert_fusion.1
  12.0 27.2 %all_gather.3.weights_ref = bf16[512,512]{1,0:T(8,128)(2,1)S(1)} all-gather(bf16[64,512]{1,0:T(8,128)(2,1)S(1)} %pad_maximum_fusion), channel_id=1, replica_groups=mesh['z'=8,'y'=8,'tp'=8] {'z'}, dimensions={0}, use_global_device_ids=true | all-gather | bytes 589824 | tf_op jit(solution)/shard_map/all_gather | solution.py:371
  39.2 1.7 %partials.1 = bf16[4,2,264,256]{3,2,1,0:T(8,128)(2,1)} custom-call(bf16[8,128,512]{2,1,0:T(8,128)(2,1)S(1)} %all-to-all-done.tokens_ref, bf16[512,512]{1,0:T(8,128)(2,1)S(1)} %all_gather.3.weights_ref, bf16[4,2,8,256]{3,2,1,0:T(8,128)(2,1)S(1)} %broadcast_in_dim.5.gates_ref), custom_call_target="tpu_custom_call" | custom-call | tf_op jit(solution)/shard_map/partials/pallas_call | solution.py:82
  40.9 6.3 %all-to-all-start.1 = ((bf16[8,264,256]{2,1,0:T(8,128)(2,1)}), bf16[8,264,256]{2,1,0:T(8,128)(2,1)S(1)}, u32[]{:S(2)}, u32[]{:S(2)}) async-start(bf16[8,264,256]{2,1,0:T(8,128)(2,1)} %bitcast.10), calls=%async_computation.1 | async-start | bytes 2162688 | tf_op jit(solution)/shard_map/all_to_all | solution.py:20
  47.3 25.8 %all-to-all-done.1.got_ref = bf16[8,264,256]{2,1,0:T(8,128)(2,1)S(1)} async-done(((bf16[8,264,256]{2,1,0:T(8,128)(2,1)}), bf16[8,264,256]{2,1,0:T(8,128)(2,1)S(1)}, u32[]{:S(2)}, u32[]{:S(2)}) %all-to-all-start.1) | async-done | bytes 1081376 | tf_op jit(solution)/shard_map/all_to_all | solution.py:20
  73.1 3.6 %ranges.1 = (bf16[768,128]{1,0:T(8,128)(2,1)S(1)}, bf16[768,128]{1,0:T(8,128)(2,1)S(1)}) custom-call(s32[1]{0:T(128)} %bitcast.1.half_ref, bf16[8,264,256]{2,1,0:T(8,128)(2,1)S(1)} %all-to-all-done.1.got_ref), custom_call_target="tpu_custom_call" | custom-call | tf_op jit(solution)/shard_map/ranges/pallas_call | solution.py:324
  76.7 1.9 %collective-permute-start = (bf16[768,128]{1,0:T(8,128)(2,1)S(1)}, bf16[768,128]{1,0:T(8,128)(2,1)S(1)}, u32[]{:S(2)}, u32[]{:S(2)}) collective-permute-start(bf16[768,128]{1,0:T(8,128)(2,1)S(1)} %get-tuple-element.6), channel_id=1, source_target_pairs={{0,8},{8,0},{16,24},{24,16},{32,40},{40,32},{48,56},{56,48},{1,9},... | collective-permute-start | bytes 589832 | tf_op jit(solution)/shard_map/ppermute | solution.py:396
  78.6 4.5 %collective-permute-done.other_ref = bf16[768,128]{1,0:T(8,128)(2,1)S(1)} collective-permute-done((bf16[768,128]{1,0:T(8,128)(2,1)S(1)}, bf16[768,128]{1,0:T(8,128)(2,1)S(1)}, u32[]{:S(2)}, u32[]{:S(2)}) %collective-permute-start) | collective-permute-done | bytes 196640 | tf_op jit(solution)/shard_map/ppermute | solution.py:396
  83.1 0.9 line.1
  84.1 13.9 %all-to-all-start.2 = ((bf16[8,192,128]{2,1,0:T(8,128)(2,1)}), bf16[8,192,128]{2,1,0:T(8,128)(2,1)S(1)}, u32[]{:S(2)}, u32[]{:S(2)}) async-start(bf16[8,192,128]{2,1,0:T(8,128)(2,1)} %line.1), calls=%async_computation.2 | async-start | bytes 786432 | tf_op jit(solution)/shard_map/all_to_all | solution.py:20
  97.9 0.1 pad_add_fusion.place_ref
  98.0 12.6 %all-to-all-done.2.lines_ref = bf16[8,192,128]{2,1,0:T(8,128)(2,1)S(1)} async-done(((bf16[8,192,128]{2,1,0:T(8,128)(2,1)}), bf16[8,192,128]{2,1,0:T(8,128)(2,1)S(1)}, u32[]{:S(2)}, u32[]{:S(2)}) %all-to-all-start.2) | async-done | bytes 393248 | tf_op jit(solution)/shard_map/all_to_all | solution.py:20
  110.6 2.2 %scan.1 = bf16[8,128,128]{2,1,0:T(8,128)(2,1)} custom-call(s32[2]{0:T(128)S(1)} %pad_add_fusion.place_ref, bf16[8,192,128]{2,1,0:T(8,128)(2,1)S(1)} %all-to-all-done.2.lines_ref, bf16[768,128]{1,0:T(8,128)(2,1)S(1)} %get-tuple-element.5.kept_ref, bf16[768,128]{1,0:T(8,128)(2,1)S(1)} %collective-permute-done.other_ref), custom_call_target="tpu_custom_call" | custom-call | tf_op jit(solution)/shard_map/scan/pallas_call | solution.py:324
  112.8 3.4 %all-to-all-start.3 = ((bf16[8,128,128]{2,1,0:T(8,128)(2,1)}), bf16[8,128,128]{2,1,0:T(8,128)(2,1)S(1)}, u32[]{:S(2)}, u32[]{:S(2)}) async-start(bf16[8,128,128]{2,1,0:T(8,128)(2,1)} %scan.1), calls=%async_computation.3 | async-start | bytes 524288 | tf_op jit(solution)/shard_map/all_to_all | solution.py:20
  116.2 0.1 copy.26.readout_ref
  116.4 0.8 first_step.1.rows_ref
  117.2 8.3 %all-to-all-done.3.back_ref = bf16[8,128,128]{2,1,0:T(8,128)(2,1)S(1)} async-done(((bf16[8,128,128]{2,1,0:T(8,128)(2,1)}), bf16[8,128,128]{2,1,0:T(8,128)(2,1)S(1)}, u32[]{:S(2)}, u32[]{:S(2)}) %all-to-all-start.3) | async-done | bytes 262176 | tf_op jit(solution)/shard_map/all_to_all | solution.py:20
  125.5 1.0 read.1
  126.5 8.4 %all-to-all-start.4 = ((bf16[8,2,64]{2,1,0:T(2,128)(2,1)}), bf16[8,2,64]{2,1,0:T(2,128)(2,1)S(1)}, u32[]{:S(2)}, u32[]{:S(2)}) async-start(bf16[8,2,64]{2,1,0:T(2,128)(2,1)} %read.1), calls=%async_computation.4 | async-start | bytes 8192 | tf_op jit(solution)/shard_map/all_to_all | solution.py:20
  134.9 0.8 copy.27
  135.7 0.8 copy.28
  136.4 3.0 %all-to-all-done.4 = bf16[8,2,64]{2,1,0:T(2,128)(2,1)S(1)} async-done(((bf16[8,2,64]{2,1,0:T(2,128)(2,1)}), bf16[8,2,64]{2,1,0:T(2,128)(2,1)S(1)}, u32[]{:S(2)}, u32[]{:S(2)}) %all-to-all-start.4) | async-done | bytes 2080 | tf_op jit(solution)/shard_map/all_to_all | solution.py:20
  139.5 0.5 reduce_sum.12
  (38 shorter events, 0.2 us)
Async XLA Ops:
  3.2 7.9 %copy-start.6 = (bf16[2,64,4096]{2,1,0:T(8,128)(2,1)S(1)}, bf16[2,64,4096]{2,1,0:T(8,128)(2,1)}, u32[]{:S(2)}) copy-start(bf16[2,64,4096]{2,1,0:T(8,128)(2,1)} %param.15) | copy-start | bytes 3145732
  3.2 7.9 %copy-start.7 = (bf16[4096,16]{0,1:T(8,128)(2,1)S(1)}, bf16[4096,16]{0,1:T(8,128)(2,1)}, u32[]{:S(2)}) copy-start(bf16[4096,16]{0,1:T(8,128)(2,1)} %param.19) | copy-start | bytes 393220
  3.2 7.9 %copy-start.8 = (bf16[4096,16]{0,1:T(8,128)(2,1)S(1)}, bf16[4096,16]{0,1:T(8,128)(2,1)}, u32[]{:S(2)}) copy-start(bf16[4096,16]{0,1:T(8,128)(2,1)} %param.18) | copy-start | bytes 393220
  3.2 36.0 %all-to-all-start = ((bf16[8,128,512]{2,1,0:T(8,128)(2,1)}), bf16[8,128,512]{2,1,0:T(8,128)(2,1)S(1)}, u32[]{:S(2)}, u32[]{:S(2)}) async-start(bf16[8,128,512]{2,1,0:T(8,128)(2,1)} %columns.1), calls=%async_computation | async-start | bytes 2097152 | tf_op jit(solution)/shard_map/all_to_all | solution.py:20
  11.0 0.7 copy-start.12
  11.0 0.7 copy-start.14
  11.0 0.7 copy-start.13
  11.0 0.9 copy-start.10
  11.0 0.9 copy-start.11
  40.9 32.1 %all-to-all-start.1 = ((bf16[8,264,256]{2,1,0:T(8,128)(2,1)}), bf16[8,264,256]{2,1,0:T(8,128)(2,1)S(1)}, u32[]{:S(2)}, u32[]{:S(2)}) async-start(bf16[8,264,256]{2,1,0:T(8,128)(2,1)} %bitcast.10), calls=%async_computation.1 | async-start | bytes 2162688 | tf_op jit(solution)/shard_map/all_to_all | solution.py:20
  76.7 6.4 %collective-permute-start = (bf16[768,128]{1,0:T(8,128)(2,1)S(1)}, bf16[768,128]{1,0:T(8,128)(2,1)S(1)}, u32[]{:S(2)}, u32[]{:S(2)}) collective-permute-start(bf16[768,128]{1,0:T(8,128)(2,1)S(1)} %get-tuple-element.6), channel_id=1, source_target_pairs={{0,8},{8,0},{16,24},{24,16},{32,40},{40,32},{48,56},{56,48},{1,9},... | collective-permute-start | bytes 589832 | tf_op jit(solution)/shard_map/ppermute | solution.py:396
  84.0 32.2 %copy-start.9 = (bf16[256,64]{0,1:T(8,128)(2,1)S(1)}, bf16[256,64]{0,1:T(8,128)(2,1)}, u32[]{:S(2)}) copy-start(bf16[256,64]{0,1:T(8,128)(2,1)} %param.29) | copy-start | bytes 98308
  84.0 32.3 %copy-start = (f32[2,2]{1,0:T(2,128)S(1)}, f32[2,2]{1,0:T(2,128)}, u32[]{:S(2)}) copy-start(f32[2,2]{1,0:T(2,128)} %strength_ref.1) | copy-start | bytes 52
  84.0 32.3 %copy-start.1 = (bf16[2,256]{1,0:T(2,128)(2,1)S(1)}, bf16[2,256]{1,0:T(2,128)(2,1)}, u32[]{:S(2)}) copy-start(bf16[2,256]{1,0:T(2,128)(2,1)} %probe_ref.1) | copy-start | bytes 3076
  84.0 32.3 %copy-start.2 = (bf16[2,256]{1,0:T(2,128)(2,1)S(1)}, bf16[2,256]{1,0:T(2,128)(2,1)}, u32[]{:S(2)}) copy-start(bf16[2,256]{1,0:T(2,128)(2,1)} %address_ref.1) | copy-start | bytes 3076
  84.0 32.3 %copy-start.3 = (bf16[2,256]{1,0:T(2,128)(2,1)S(1)}, bf16[2,256]{1,0:T(2,128)(2,1)}, u32[]{:S(2)}) copy-start(bf16[2,256]{1,0:T(2,128)(2,1)} %content_ref.1) | copy-start | bytes 3076
  84.0 32.3 %copy-start.4 = (bf16[2,256]{1,0:T(2,128)(2,1)S(1)}, bf16[2,256]{1,0:T(2,128)(2,1)}, u32[]{:S(2)}) copy-start(bf16[2,256]{1,0:T(2,128)(2,1)} %outgate_ref.1) | copy-start | bytes 3076
  84.0 32.3 %copy-start.5 = (f32[128]{0:T(128)S(1)}, f32[128]{0:T(128)}, u32[]{:S(2)}) copy-start(f32[128]{0:T(128)} %param.28) | copy-start | bytes 1540
  84.1 26.6 %all-to-all-start.2 = ((bf16[8,192,128]{2,1,0:T(8,128)(2,1)}), bf16[8,192,128]{2,1,0:T(8,128)(2,1)S(1)}, u32[]{:S(2)}, u32[]{:S(2)}) async-start(bf16[8,192,128]{2,1,0:T(8,128)(2,1)} %line.1), calls=%async_computation.2 | async-start | bytes 786432 | tf_op jit(solution)/shard_map/all_to_all | solution.py:20
  112.8 12.7 %all-to-all-start.3 = ((bf16[8,128,128]{2,1,0:T(8,128)(2,1)}), bf16[8,128,128]{2,1,0:T(8,128)(2,1)S(1)}, u32[]{:S(2)}, u32[]{:S(2)}) async-start(bf16[8,128,128]{2,1,0:T(8,128)(2,1)} %scan.1), calls=%async_computation.3 | async-start | bytes 524288 | tf_op jit(solution)/shard_map/all_to_all | solution.py:20
  126.5 13.0 %all-to-all-start.4 = ((bf16[8,2,64]{2,1,0:T(2,128)(2,1)}), bf16[8,2,64]{2,1,0:T(2,128)(2,1)S(1)}, u32[]{:S(2)}, u32[]{:S(2)}) async-start(bf16[8,2,64]{2,1,0:T(2,128)(2,1)} %read.1), calls=%async_computation.4 | async-start | bytes 8192 | tf_op jit(solution)/shard_map/all_to_all | solution.py:20

commit v8 on v7

--- a/solution.py
+++ b/solution.py
@@ -57,13 +57,18 @@
     )(flat)
 
 
-def partial_body(tokens_ref, weights_ref, gates_ref, sent_ref):
+def partial_body(tokens_ref, weights_ref, gates_ref, out_ref, sent_ref, done):
     line, rows, _ = tokens_ref.shape
     owners, halves, sent_rows, width = sent_ref.shape
     ranges = line // halves
     positions = (sent_rows - gates_ref.shape[2]) // ranges
     prompts = rows // positions
     heads = owners // prompts
+    sent_ref[:, :, ranges * positions :, :] = gates_ref[...]
+    writes = [
+        pltpu.make_async_copy(sent_ref.at[:, half], out_ref.at[:, half], done.at[half])
+        for half in range(halves)
+    ]
     for k in range(line):
         half, j = k // ranges, k % ranges
         part = jnp.dot(tokens_ref[k], weights_ref[...], preferred_element_type=jnp.float32)
@@ -73,17 +78,21 @@
                 sent_ref[p * heads + h, half, j * positions : (j + 1) * positions, :] = part[
                     p * positions : (p + 1) * positions, h * width : (h + 1) * width
                 ]
-    sent_ref[:, :, ranges * positions :, :] = gates_ref[...]
+        if j == ranges - 1:
+            writes[half].start()
+    for write in writes:
+        write.wait()
 
 
 def partial_projections(tokens, weights, gates, positions):
     owners, halves, extra, width = gates.shape
-    sent_rows = tokens.shape[0] // halves * positions + extra
+    shape = (owners, halves, tokens.shape[0] // halves * positions + extra, width)
     return pl.pallas_call(
         partial_body,
         in_specs=[VMEM, VMEM, VMEM],
-        out_specs=VMEM,
-        out_shape=jax.ShapeDtypeStruct((owners, halves, sent_rows, width), tokens.dtype),
+        out_specs=pl.BlockSpec(memory_space=pltpu.MemorySpace.HBM),
+        out_shape=jax.ShapeDtypeStruct(shape, tokens.dtype),
+        scratch_shapes=[pltpu.VMEM(shape, tokens.dtype), pltpu.SemaphoreType.DMA((halves,))],
         interpret=INTERPRET,
         compiler_params=SMALL,
         name="partials",

time: 141 us -> 141 us (level)
  no operation moved by 1% of the time
where the time goes in v8:
time: 141 us; the launch traced here: 140 us
  waiting for transfers between devices  54.2 us (38%)
  starting transfers between devices  41.7 us (30%)
  blocking collectives  27.2 us (19%)
  Pallas kernels  12.6 us (9%)
  local copies, waits for them, and re-layouts  1.93 us (1%)
    all_to_all x5, waiting for transfers between devices, exchange(): lax.all_to_all(messages, axis, split_axis=0, concat_axis=0, tiled=True)  49.8 us
    all_to_all x5, starting transfers between devices, exchange(): lax.all_to_all(messages, axis, split_axis=0, concat_axis=0, tiled=True)  39.8 us
    all_gather x1, blocking collectives, per_device(): line_weights = lax.all_gather(weights, 'z', axis=0, tiled=True)  27.2 us
    pallas_call x5, Pallas kernels, local(): pl.pallas_call(body, in_specs=[SMEM] * scalars + [VMEM] * (len(operands)...  8.48 us
    ppermute x1, waiting for transfers between devices, per_device(): other = lax.ppermute(given, 'y', [(i, i ^ 1) for i in range(SIDE)])  4.49 us
  transfers between devices with their start and end apart: 6, of which 5 were waited for; matrix products, arithmetic and copies ran while one was open for 2% of the time, Pallas kernels for 1%

profile of v8, /device:TPU:1, one launch (start us, length us, event | category | flops | bytes accessed | tf_op | source)
XLA Modules:
  0.0 139.9 jit_solution(958068513286240857)
XLA Ops:
  0.6 2.5 %columns.1 = bf16[8,128,512]{2,1,0:T(8,128)(2,1)} custom-call(bf16[128,4096]{1,0:T(8,128)(2,1)} %bitcast.43), custom_call_target="tpu_custom_call" | custom-call | tf_op jit(solution)/shard_map/columns/pallas_call | solution.py:46
  3.2 0.0 copy-start.6
  3.2 0.0 copy-start.7
  3.2 7.8 %all-to-all-start = ((bf16[8,128,512]{2,1,0:T(8,128)(2,1)}), bf16[8,128,512]{2,1,0:T(8,128)(2,1)S(1)}, u32[]{:S(2)}, u32[]{:S(2)}) async-start(bf16[8,128,512]{2,1,0:T(8,128)(2,1)} %columns.1), calls=%async_computation | async-start | bytes 2097152 | tf_op jit(solution)/shard_map/all_to_all | solution.py:20
  11.0 0.0 copy-start.10
  11.1 0.4 fusion.1
  11.5 0.1 reshape.81
  11.7 0.0 copy-done.12
  11.7 0.1 fusion.15
  11.8 0.1 reduce-precision_convert_fusion.1
  12.0 27.2 %all_gather.3.weights_ref = bf16[512,512]{1,0:T(8,128)(2,1)S(1)} all-gather(bf16[64,512]{1,0:T(8,128)(2,1)S(1)} %pad_maximum_fusion), channel_id=1, replica_groups=mesh['z'=8,'y'=8,'tp'=8] {'z'}, dimensions={0}, use_global_device_ids=true | all-gather | bytes 589824 | tf_op jit(solution)/shard_map/all_gather | solution.py:380
  39.2 1.6 %partials.1 = bf16[4,2,264,256]{3,2,1,0:T(8,128)(2,1)} custom-call(bf16[8,128,512]{2,1,0:T(8,128)(2,1)S(1)} %all-to-all-done.tokens_ref, bf16[512,512]{1,0:T(8,128)(2,1)S(1)} %all_gather.3.weights_ref, bf16[4,2,8,256]{3,2,1,0:T(8,128)(2,1)S(1)} %broadcast_in_dim.5.gates_ref), custom_call_target="tpu_custom_call" | custom-call | tf_op jit(solution)/shard_map/partials/pallas_call | solution.py:90
  40.8 6.3 %all-to-all-start.1 = ((bf16[8,264,256]{2,1,0:T(8,128)(2,1)}), bf16[8,264,256]{2,1,0:T(8,128)(2,1)S(1)}, u32[]{:S(2)}, u32[]{:S(2)}) async-start(bf16[8,264,256]{2,1,0:T(8,128)(2,1)} %bitcast.10), calls=%async_computation.1 | async-start | bytes 2162688 | tf_op jit(solution)/shard_map/all_to_all | solution.py:20
  47.1 25.8 %all-to-all-done.1.got_ref = bf16[8,264,256]{2,1,0:T(8,128)(2,1)S(1)} async-done(((bf16[8,264,256]{2,1,0:T(8,128)(2,1)}), bf16[8,264,256]{2,1,0:T(8,128)(2,1)S(1)}, u32[]{:S(2)}, u32[]{:S(2)}) %all-to-all-start.1) | async-done | bytes 1081376 | tf_op jit(solution)/shard_map/all_to_all | solution.py:20
  72.9 3.6 %ranges.1 = (bf16[768,128]{1,0:T(8,128)(2,1)S(1)}, bf16[768,128]{1,0:T(8,128)(2,1)S(1)}) custom-call(s32[1]{0:T(128)} %bitcast.1.half_ref, bf16[8,264,256]{2,1,0:T(8,128)(2,1)S(1)} %all-to-all-done.1.got_ref), custom_call_target="tpu_custom_call" | custom-call | tf_op jit(solution)/shard_map/ranges/pallas_call | solution.py:333
  76.6 1.9 %collective-permute-start = (bf16[768,128]{1,0:T(8,128)(2,1)S(1)}, bf16[768,128]{1,0:T(8,128)(2,1)S(1)}, u32[]{:S(2)}, u32[]{:S(2)}) collective-permute-start(bf16[768,128]{1,0:T(8,128)(2,1)S(1)} %get-tuple-element.6), channel_id=1, source_target_pairs={{0,8},{8,0},{16,24},{24,16},{32,40},{40,32},{48,56},{56,48},{1,9},... | collective-permute-start | bytes 589832 | tf_op jit(solution)/shard_map/ppermute | solution.py:405
  78.5 4.5 %collective-permute-done.other_ref = bf16[768,128]{1,0:T(8,128)(2,1)S(1)} collective-permute-done((bf16[768,128]{1,0:T(8,128)(2,1)S(1)}, bf16[768,128]{1,0:T(8,128)(2,1)S(1)}, u32[]{:S(2)}, u32[]{:S(2)}) %collective-permute-start) | collective-permute-done | bytes 196640 | tf_op jit(solution)/shard_map/ppermute | solution.py:405
  83.0 0.9 line.1
  83.9 13.9 %all-to-all-start.2 = ((bf16[8,192,128]{2,1,0:T(8,128)(2,1)}), bf16[8,192,128]{2,1,0:T(8,128)(2,1)S(1)}, u32[]{:S(2)}, u32[]{:S(2)}) async-start(bf16[8,192,128]{2,1,0:T(8,128)(2,1)} %line.1), calls=%async_computation.2 | async-start | bytes 786432 | tf_op jit(solution)/shard_map/all_to_all | solution.py:20
  97.8 0.1 pad_add_fusion.place_ref
  97.9 12.6 %all-to-all-done.2.lines_ref = bf16[8,192,128]{2,1,0:T(8,128)(2,1)S(1)} async-done(((bf16[8,192,128]{2,1,0:T(8,128)(2,1)}), bf16[8,192,128]{2,1,0:T(8,128)(2,1)S(1)}, u32[]{:S(2)}, u32[]{:S(2)}) %all-to-all-start.2) | async-done | bytes 393248 | tf_op jit(solution)/shard_map/all_to_all | solution.py:20
  110.5 2.2 %scan.1 = bf16[8,128,128]{2,1,0:T(8,128)(2,1)} custom-call(s32[2]{0:T(128)S(1)} %pad_add_fusion.place_ref, bf16[8,192,128]{2,1,0:T(8,128)(2,1)S(1)} %all-to-all-done.2.lines_ref, bf16[768,128]{1,0:T(8,128)(2,1)S(1)} %get-tuple-element.5.kept_ref, bf16[768,128]{1,0:T(8,128)(2,1)S(1)} %collective-permute-done.other_ref), custom_call_target="tpu_custom_call" | custom-call | tf_op jit(solution)/shard_map/scan/pallas_call | solution.py:333
  112.7 3.4 %all-to-all-start.3 = ((bf16[8,128,128]{2,1,0:T(8,128)(2,1)}), bf16[8,128,128]{2,1,0:T(8,128)(2,1)S(1)}, u32[]{:S(2)}, u32[]{:S(2)}) async-start(bf16[8,128,128]{2,1,0:T(8,128)(2,1)} %scan.1), calls=%async_computation.3 | async-start | bytes 524288 | tf_op jit(solution)/shard_map/all_to_all | solution.py:20
  116.1 0.1 copy.26.readout_ref
  116.3 0.8 first_step.1.rows_ref
  117.1 8.3 %all-to-all-done.3.back_ref = bf16[8,128,128]{2,1,0:T(8,128)(2,1)S(1)} async-done(((bf16[8,128,128]{2,1,0:T(8,128)(2,1)}), bf16[8,128,128]{2,1,0:T(8,128)(2,1)S(1)}, u32[]{:S(2)}, u32[]{:S(2)}) %all-to-all-start.3) | async-done | bytes 262176 | tf_op jit(solution)/shard_map/all_to_all | solution.py:20
  125.4 1.0 read.1
  126.4 8.4 %all-to-all-start.4 = ((bf16[8,2,64]{2,1,0:T(2,128)(2,1)}), bf16[8,2,64]{2,1,0:T(2,128)(2,1)S(1)}, u32[]{:S(2)}, u32[]{:S(2)}) async-start(bf16[8,2,64]{2,1,0:T(2,128)(2,1)} %read.1), calls=%async_computation.4 | async-start | bytes 8192 | tf_op jit(solution)/shard_map/all_to_all | solution.py:20
  134.8 0.8 copy.27
  135.6 0.8 copy.28
  136.3 3.0 %all-to-all-done.4 = bf16[8,2,64]{2,1,0:T(2,128)(2,1)S(1)} async-done(((bf16[8,2,64]{2,1,0:T(2,128)(2,1)}), bf16[8,2,64]{2,1,0:T(2,128)(2,1)S(1)}, u32[]{:S(2)}, u32[]{:S(2)}) %all-to-all-start.4) | async-done | bytes 2080 | tf_op jit(solution)/shard_map/all_to_all | solution.py:20
  139.4 0.5 reduce_sum.12
  (38 shorter events, 0.2 us)
Async XLA Ops:
  3.2 7.9 %copy-start.6 = (bf16[2,64,4096]{2,1,0:T(8,128)(2,1)S(1)}, bf16[2,64,4096]{2,1,0:T(8,128)(2,1)}, u32[]{:S(2)}) copy-start(bf16[2,64,4096]{2,1,0:T(8,128)(2,1)} %param.15) | copy-start | bytes 3145732
  3.2 7.9 %copy-start.7 = (bf16[4096,16]{0,1:T(8,128)(2,1)S(1)}, bf16[4096,16]{0,1:T(8,128)(2,1)}, u32[]{:S(2)}) copy-start(bf16[4096,16]{0,1:T(8,128)(2,1)} %param.19) | copy-start | bytes 393220
  3.2 7.9 %copy-start.8 = (bf16[4096,16]{0,1:T(8,128)(2,1)S(1)}, bf16[4096,16]{0,1:T(8,128)(2,1)}, u32[]{:S(2)}) copy-start(bf16[4096,16]{0,1:T(8,128)(2,1)} %param.18) | copy-start | bytes 393220
  3.2 36.0 %all-to-all-start = ((bf16[8,128,512]{2,1,0:T(8,128)(2,1)}), bf16[8,128,512]{2,1,0:T(8,128)(2,1)S(1)}, u32[]{:S(2)}, u32[]{:S(2)}) async-start(bf16[8,128,512]{2,1,0:T(8,128)(2,1)} %columns.1), calls=%async_computation | async-start | bytes 2097152 | tf_op jit(solution)/shard_map/all_to_all | solution.py:20
  11.0 0.7 copy-start.12
  11.0 0.7 copy-start.14
  11.0 0.7 copy-start.13
  11.0 0.9 copy-start.10
  11.0 0.9 copy-start.11
  40.8 32.1 %all-to-all-start.1 = ((bf16[8,264,256]{2,1,0:T(8,128)(2,1)}), bf16[8,264,256]{2,1,0:T(8,128)(2,1)S(1)}, u32[]{:S(2)}, u32[]{:S(2)}) async-start(bf16[8,264,256]{2,1,0:T(8,128)(2,1)} %bitcast.10), calls=%async_computation.1 | async-start | bytes 2162688 | tf_op jit(solution)/shard_map/all_to_all | solution.py:20
  76.6 6.4 %collective-permute-start = (bf16[768,128]{1,0:T(8,128)(2,1)S(1)}, bf16[768,128]{1,0:T(8,128)(2,1)S(1)}, u32[]{:S(2)}, u32[]{:S(2)}) collective-permute-start(bf16[768,128]{1,0:T(8,128)(2,1)S(1)} %get-tuple-element.6), channel_id=1, source_target_pairs={{0,8},{8,0},{16,24},{24,16},{32,40},{40,32},{48,56},{56,48},{1,9},... | collective-permute-start | bytes 589832 | tf_op jit(solution)/shard_map/ppermute | solution.py:405
  83.9 32.2 %copy-start.9 = (bf16[256,64]{0,1:T(8,128)(2,1)S(1)}, bf16[256,64]{0,1:T(8,128)(2,1)}, u32[]{:S(2)}) copy-start(bf16[256,64]{0,1:T(8,128)(2,1)} %param.29) | copy-start | bytes 98308
  83.9 32.3 %copy-start = (f32[2,2]{1,0:T(2,128)S(1)}, f32[2,2]{1,0:T(2,128)}, u32[]{:S(2)}) copy-start(f32[2,2]{1,0:T(2,128)} %strength_ref.1) | copy-start | bytes 52
  83.9 32.3 %copy-start.1 = (bf16[2,256]{1,0:T(2,128)(2,1)S(1)}, bf16[2,256]{1,0:T(2,128)(2,1)}, u32[]{:S(2)}) copy-start(bf16[2,256]{1,0:T(2,128)(2,1)} %probe_ref.1) | copy-start | bytes 3076
  83.9 32.3 %copy-start.2 = (bf16[2,256]{1,0:T(2,128)(2,1)S(1)}, bf16[2,256]{1,0:T(2,128)(2,1)}, u32[]{:S(2)}) copy-start(bf16[2,256]{1,0:T(2,128)(2,1)} %address_ref.1) | copy-start | bytes 3076
  83.9 32.3 %copy-start.3 = (bf16[2,256]{1,0:T(2,128)(2,1)S(1)}, bf16[2,256]{1,0:T(2,128)(2,1)}, u32[]{:S(2)}) copy-start(bf16[2,256]{1,0:T(2,128)(2,1)} %content_ref.1) | copy-start | bytes 3076
  83.9 32.3 %copy-start.4 = (bf16[2,256]{1,0:T(2,128)(2,1)S(1)}, bf16[2,256]{1,0:T(2,128)(2,1)}, u32[]{:S(2)}) copy-start(bf16[2,256]{1,0:T(2,128)(2,1)} %outgate_ref.1) | copy-start | bytes 3076
  83.9 32.3 %copy-start.5 = (f32[128]{0:T(128)S(1)}, f32[128]{0:T(128)}, u32[]{:S(2)}) copy-start(f32[128]{0:T(128)} %param.28) | copy-start | bytes 1540
  83.9 26.6 %all-to-all-start.2 = ((bf16[8,192,128]{2,1,0:T(8,128)(2,1)}), bf16[8,192,128]{2,1,0:T(8,128)(2,1)S(1)}, u32[]{:S(2)}, u32[]{:S(2)}) async-start(bf16[8,192,128]{2,1,0:T(8,128)(2,1)} %line.1), calls=%async_computation.2 | async-start | bytes 786432 | tf_op jit(solution)/shard_map/all_to_all | solution.py:20
  112.7 12.7 %all-to-all-start.3 = ((bf16[8,128,128]{2,1,0:T(8,128)(2,1)}), bf16[8,128,128]{2,1,0:T(8,128)(2,1)S(1)}, u32[]{:S(2)}, u32[]{:S(2)}) async-start(bf16[8,128,128]{2,1,0:T(8,128)(2,1)} %scan.1), calls=%async_computation.3 | async-start | bytes 524288 | tf_op jit(solution)/shard_map/all_to_all | solution.py:20
  126.4 13.0 %all-to-all-start.4 = ((bf16[8,2,64]{2,1,0:T(2,128)(2,1)}), bf16[8,2,64]{2,1,0:T(2,128)(2,1)S(1)}, u32[]{:S(2)}, u32[]{:S(2)}) async-start(bf16[8,2,64]{2,1,0:T(2,128)(2,1)} %read.1), calls=%async_computation.4 | async-start | bytes 8192 | tf_op jit(solution)/shard_map/all_to_all | solution.py:20
